TPU v7x, 512 devices: a whole 4x4x16 slice. The times are simulated.
512 devices in a mesh: ep: 32 (over z, core), tp: 16 (over y, x).
Axes of the slice: x: 4, y: 4, z: 16, core: 2. Of those that a mesh axis runs over, the one named last changes fastest.
Arguments:
- query_proj: bfloat16 [16384, 1024], P('ep', 'tp'), may hold values from -6 to 6
- key_proj: bfloat16 [16384, 256], P('ep'), may hold values from -6 to 6
- value_proj: bfloat16 [16384, 256], P('ep'), may hold values from -24 to 24
- sink_logit: float32 [16], P('tp'), may hold values from 2 to 6
- out_weight: bfloat16 [1024, 2048], P(None, 'tp'), may hold values from -0.1875 to 0.1875
- expert_input: bfloat16 [8192, 2048], P('ep'), may hold values from -6 to 6
- norm_gain: float32 [2048], replicated, may hold values from 0.1 to 1.9
- routes: int32 [8192, 2], P('ep'), may hold values from 0 to 31, as said below
- route_weights: float32 [8192, 2], P('ep'), may hold values from 0.2 to 1
- gate_weight: bfloat16 [32, 2048, 4096], P('ep', None, 'tp'), may hold values from -0.125 to 0.125
- up_weight: bfloat16 [32, 2048, 4096], P('ep', None, 'tp'), may hold values from -0.125 to 0.125
- down_weight: bfloat16 [32, 4096, 2048], P('ep', 'tp'), may hold values from -0.09375 to 0.09375
Outputs:
- mixer_out: bfloat16 [16384, 2048], P('ep', 'tp')
- expert_out: bfloat16 [8192, 2048], P('ep', 'tp')
Inputs may be any that keep to these rules, and one draw needn't show every extreme that they name: `routes`: experts form 4 groups of consecutive numbers of equal size. Each row names 2 different experts of one group. In each aligned block of 256 rows no expert is named by more than 32 rows, and in every block some expert is named by exactly 32 rows.
All inputs are finite; a program needn't handle non-finite values.
Results may differ from a plain program's by a relative error of at most 0.017.
Values may be sent and summed in bfloat16 or wider, within the bound.
No kernel may reach another device: no remote copies, remote signals or barrier semaphores. Data moves between devices by JAX's collectives and lax.ppermute only.
A program may use at most 64 MiB of HBM per device.

v0:
```python
import jax
import jax.numpy as jnp
from jax import lax
from jax.sharding import Mesh
from jax.sharding import PartitionSpec as P

D = 2048
HEADS = 16
KV_HEADS = 4
HEAD_DIM = 64
HALF_WIN = 128
GROUPS = 4
TOP_K = 2
TP = ("tp_0", "tp_1")


NORM_EPS = 1e-06
ROPE_BASE = 10000.0
NEG_BIG = -1e30


def padded(block, sides, width):
    for axis, dim in sides:
        count = lax.axis_size(axis)
        forward = [(i, i + 1) for i in range(count - 1)]
        backward = [(target, source) for source, target in forward]
        low = lax.ppermute(
            lax.slice_in_dim(block, block.shape[dim] - width, None, axis=dim), axis, forward
        )
        high = lax.ppermute(lax.slice_in_dim(block, 0, width, axis=dim), axis, backward)
        block = jnp.concatenate([low, block, high], axis=dim)
    return block


def in_order(blocks, dim):
    dims = list(blocks.shape[1:])
    dims[dim] *= blocks.shape[0]
    return jnp.moveaxis(blocks, 0, dim).reshape(dims)


def copy_for_each(x, axis):
    devices = lax.axis_size(axis)
    return lax.all_to_all(jnp.broadcast_to(x[None], (devices, *x.shape)), axis, 0, 0, tiled=True)


def collect(x, axis, dim):
    return in_order(copy_for_each(x, axis), dim)


def own_rows(terms, axes):
    so_far = terms.astype(jnp.bfloat16)
    for axis in axes:
        so_far = lax.psum_scatter(so_far, axis, scatter_dimension=0, tiled=True)
    return so_far.astype(jnp.float32)


def rotate(features, position_start):
    count = features.shape[0]
    half_dim = features.shape[-1] // 2
    inverse_freq = 1.0 / ROPE_BASE ** (
        jnp.arange(half_dim, dtype=jnp.float32) * 2.0 / features.shape[-1]
    )
    position = (jnp.arange(count, dtype=jnp.int32) + position_start).astype(jnp.float32)
    angles = position[:, None] * inverse_freq[None, :]
    cosine = jnp.cos(angles)[:, None, :]
    sine_part = jnp.sin(angles)[:, None, :]
    lower_half = features[..., :half_dim]
    upper_half = features[..., half_dim:]
    return jnp.concatenate(
        [
            lower_half * cosine - upper_half * sine_part,
            upper_half * cosine + lower_half * sine_part,
        ],
        axis=-1,
    )


def mixer_half(query_proj, key_proj, value_proj, sink_logit, out_weight):
    row_count = query_proj.shape[0]
    local_heads = query_proj.shape[1] // HEAD_DIM
    per_kv = HEADS // KV_HEADS
    kv_local = max(1, local_heads // per_kv)
    group_size = local_heads // kv_local
    tp_index = lax.axis_index(TP)
    offset = lax.axis_index("ep") * row_count
    seq_total = row_count * lax.axis_size("ep")
    first_kv = tp_index * local_heads // per_kv
    own_keys = lax.dynamic_slice_in_dim(key_proj, first_kv * HEAD_DIM, kv_local * HEAD_DIM, 1)
    own_values = lax.dynamic_slice_in_dim(value_proj, first_kv * HEAD_DIM, kv_local * HEAD_DIM, 1)
    rot_q = rotate(
        query_proj.reshape(row_count, local_heads, HEAD_DIM).astype(jnp.float32), offset
    ).astype(jnp.bfloat16)
    rot_k = rotate(
        own_keys.reshape(row_count, kv_local, HEAD_DIM).astype(jnp.float32), offset
    ).astype(jnp.bfloat16)
    stacked = jnp.stack([rot_k, own_values.reshape(row_count, kv_local, HEAD_DIM)])
    extended = padded(stacked, (("ep", 1),), HALF_WIN)
    own_sink = sink_logit.reshape(kv_local, group_size)
    block_rows = min(512, row_count)
    key_rows = block_rows + 2 * HALF_WIN
    key_offset = jnp.arange(key_rows, dtype=jnp.int32) - HALF_WIN
    key_gap = key_offset[None, :] - jnp.arange(block_rows, dtype=jnp.int32)[:, None]
    query_block = rot_q.reshape(block_rows, kv_local, group_size, HEAD_DIM)
    key_block = extended[0, 0:key_rows]
    value_block = extended[1, 0:key_rows]
    scores = jnp.einsum(
        "qngd,knd->ngqk", query_block, key_block, preferred_element_type=jnp.float32
    ) * HEAD_DIM ** (-0.5)
    global_key = offset + 0 + key_offset
    allowed = (
        (jnp.abs(key_gap) <= HALF_WIN)
        & (global_key >= 0)[None, :]
        & (global_key < seq_total)[None, :]
    )
    scores = jnp.where(allowed[None, None], scores, NEG_BIG)
    row_peak = jnp.maximum(jnp.max(scores, axis=-1), own_sink[:, :, None])
    lifted = jnp.exp(scores - row_peak[..., None])
    norm_total = jnp.sum(lifted, axis=-1) + jnp.exp(own_sink[:, :, None] - row_peak)
    probs = (lifted / norm_total[..., None]).astype(jnp.bfloat16)
    weighted = jnp.einsum("ngqk,knd->qngd", probs, value_block, preferred_element_type=jnp.float32)
    pieces = weighted.astype(jnp.bfloat16).reshape(block_rows, local_heads * HEAD_DIM)
    projected = jnp.dot(collect(pieces, TP, 1), out_weight, preferred_element_type=jnp.float32)
    return projected.astype(jnp.bfloat16)


def expert_half(
    expert_input, norm_gain, routes, route_weights, gate_weight, up_weight, down_weight
):
    row_count = expert_input.shape[0]
    widened = expert_input.astype(jnp.float32)
    normed = (
        widened
        * lax.rsqrt(jnp.mean(widened * widened, axis=1, keepdims=True) + NORM_EPS)
        * norm_gain
    ).astype(jnp.bfloat16)
    local_experts = gate_weight.shape[0]
    ep_count = lax.axis_size("ep")
    expert_count = local_experts * ep_count
    capacity = row_count * GROUPS // expert_count
    col_count = D // lax.axis_size(TP)
    flat_routes = routes.reshape(-1)
    onehot = (flat_routes[:, None] == jnp.arange(expert_count, dtype=jnp.int32)[None, :]).astype(
        jnp.int32
    )
    slot_rank = jnp.sum((jnp.cumsum(onehot, axis=0) - onehot) * onehot, axis=1)
    slot_index = flat_routes * capacity + slot_rank
    source_rows = jnp.arange(row_count * TOP_K, dtype=jnp.int32) // TOP_K
    own_cols = lax.dynamic_slice_in_dim(normed, lax.axis_index(TP) * col_count, col_count, 1)
    outgoing = (
        jnp.zeros((expert_count * capacity, col_count), jnp.bfloat16)
        .at[slot_index]
        .set(own_cols[source_rows])
    )
    arrived = lax.all_to_all(
        outgoing.reshape(expert_count, capacity, col_count),
        "ep",
        split_axis=0,
        concat_axis=1,
        tiled=True,
    )
    shard_piece = collect(arrived, TP, 2)
    gate_sum = jnp.einsum(
        "esd,edh->esh", shard_piece, gate_weight, preferred_element_type=jnp.float32
    )
    up_sum = jnp.einsum("esd,edh->esh", shard_piece, up_weight, preferred_element_type=jnp.float32)
    hidden = (jax.nn.silu(gate_sum) * up_sum).astype(jnp.bfloat16)
    slot_total = hidden.shape[1]
    term = jnp.einsum("esh,ehc->ces", hidden, down_weight, preferred_element_type=jnp.float32)
    summed = own_rows(term.reshape(col_count * lax.axis_size(TP), local_experts * slot_total), TP)
    result = summed.astype(jnp.bfloat16).reshape(col_count, local_experts, ep_count, capacity)
    returned = lax.all_to_all(result, "ep", split_axis=2, concat_axis=1, tiled=True)
    returned = returned.reshape(col_count, expert_count * capacity)
    picked = (
        jnp.take(returned, slot_index, axis=1)
        .reshape(col_count, row_count, TOP_K)
        .astype(jnp.float32)
    )
    combined = jnp.sum(picked * route_weights[None, :, :], axis=2)
    return combined.T.astype(jnp.bfloat16)


def local(
    query_proj,
    key_proj,
    value_proj,
    sink_logit,
    out_weight,
    expert_input,
    norm_gain,
    routes,
    route_weights,
    gate_weight,
    up_weight,
    down_weight,
):
    mixer_out = mixer_half(query_proj, key_proj, value_proj, sink_logit, out_weight)
    expert_out = expert_half(
        expert_input, norm_gain, routes, route_weights, gate_weight, up_weight, down_weight
    )
    return (mixer_out, expert_out)


def solution(mesh):
    finer = Mesh(mesh.devices.reshape(mesh.shape["ep"], 4, 4), ("ep", "tp_0", "tp_1"))
    in_specs = (
        P("ep", TP),
        P("ep", None),
        P("ep", None),
        P(TP),
        P(None, TP),
        P("ep", None),
        P(),
        P("ep", None),
        P("ep", None),
        P("ep", None, TP),
        P("ep", None, TP),
        P("ep", TP, None),
    )
    out_specs = (P("ep", TP), P("ep", TP))
    return jax.shard_map(local, mesh=finer, in_specs=in_specs, out_specs=out_specs, check_vma=False)
```

profile of v0, /device:TPU:1, one launch (start us, length us, event | category | flops | bytes accessed | tf_op | source)
XLA Modules:
  0.0 251.4 jit_solution(438518287984373368)
XLA Ops:
  7.2 1.6 convert_element_type.96
  8.9 0.3 multiply_reduce_fusion
  9.1 0.1 copy.41
  9.3 0.1 eq.26
  9.4 0.1 reshape.472
  9.6 1.2 reduce-window.6
  10.8 0.2 slice_reduce_fusion
  11.1 0.1 copy.46
  11.2 0.1 mul.163
  11.4 0.8 dynamic-slice
  12.2 0.1 fusion.47
  12.3 0.1 fusion.34
  12.4 3.1 %scatter_custom_fusion = bf16[1024,128]{1,0:T(8,128)(2,1)S(1)} fusion(s32[512]{0:T(512)S(1)} %bitcast.108, bf16[256,128]{1,0:T(8,128)(2,1)S(1)} %fusion.34, s32[1024]{0:T(1024)S(1)} %pad_clamp_fusion.1, bf16[]{:T(256)} %constant.105.clone.1), kind=kCustom, calls=%fused_computation.59 | custom fusion | bytes 262146 | tf_op jit(solution)/shard_map/scatter | solution.py:152
  15.4 38.8 %all_to_all.28 = bf16[32,32,128]{2,1,0:T(8,128)(2,1)S(1)} all-to-all(bf16[32,32,128]{2,1,0:T(8,128)(2,1)S(1)} %bitcast.103), channel_id=1, replica_groups=mesh['ep'=32,'tp_0'=4,'tp_1'=4] {'ep'}, dimensions={0} | all-to-all | bytes 524288 | tf_op jit(solution)/shard_map/all_to_all | solution.py:154
  54.2 0.1 copy.47
  54.4 0.5 broadcast_in_dim.27
  54.9 56.5 %all_to_all.29 = bf16[16,1,1024,128]{2,3,1,0:T(8,128)(2,1)S(1)} all-to-all(bf16[16,1,1024,128]{2,3,1,0:T(8,128)(2,1)S(1)} %broadcast_in_dim.27), channel_id=1, replica_groups=mesh['ep'=32,'tp_0'=4,'tp_1'=4] {'tp_0','tp_1'}, dimensions={0} | all-to-all | bytes 8388608 | tf_op jit(solution)/shard_map/all_to_all | solution.py:43
  111.4 2.0 copy-done.2
  113.4 1.3 fusion.8
  114.7 8.5 %convert_bitcast_fusion = bf16[2048,1024]{0,1:T(8,128)(2,1)} fusion(bf16[1024,2048]{0,1:T(8,128)(2,1)} %bitcast.101, bf16[1,256,2048]{2,1,0:T(8,128)(2,1)S(1)} %copy-done, bf16[1,2048,256]{2,1,0:T(8,128)(2,1)S(1)} %copy-done.10, f32[1024,256]{1,0:T(8,128)S(1)} %fusion.8), kind=kOutput, calls=%fused_computation.3 | convolution fusion | flops 2151153664 | bytes 11534336 | tf_op jit(solution)/shard_map/esh,ehc->ces/dot_general | solution.py:168
  123.2 0.7 copy-done.4
  124.0 0.1 copy.40
  124.2 0.1 dynamic-slice_bitcast_fusion
  124.3 0.1 bitcast_convert_fusion
  124.4 1.3 fusion.42
  125.7 0.1 pad_maximum_fusion.3
  125.8 3.3 %collective-permute-start = (bf16[2,128,1,64]{3,1,2,0:T(8,128)(2,1)S(1)}, bf16[2,128,1,64]{3,1,2,0:T(8,128)(2,1)S(1)}, u32[]{:S(2)}, u32[]{:S(2)}) collective-permute-start(bf16[2,128,1,64]{3,1,2,0:T(8,128)(2,1)S(1)} %get-tuple-element.2), channel_id=1, source_target_pairs={{0,16},{16,32},{32,48},{48,64},{64,80},{80,96},{96,112},{112,128},... | collective-permute-start | bytes 98312 | tf_op jit(solution)/shard_map/ppermute | solution.py:27
  129.1 2.2 collective-permute-start.1
  131.9 3.1 %collective-permute-done.1 = bf16[2,128,1,64]{3,1,2,0:T(8,128)(2,1)S(1)} collective-permute-done((bf16[2,128,1,64]{3,1,2,0:T(8,128)(2,1)S(1)}, bf16[2,128,1,64]{3,1,2,0:T(8,128)(2,1)S(1)}, u32[]{:S(2)}, u32[]{:S(2)}) %collective-permute-start.1) | collective-permute-done | bytes 32800 | tf_op jit(solution)/shard_map/ppermute | solution.py:30
  135.1 0.1 pad_maximum_fusion
  135.2 32.8 %reduce-scatter.5.cloned.1.call-done = bf16[512,1024]{0,1:T(8,128)(2,1)} async-done(((bf16[2048,1024]{0,1:T(8,128)(2,1)}), bf16[512,1024]{0,1:T(8,128)(2,1)}) %reduce-scatter.5.cloned.1.call-update) | async-done | bytes 1048592 | tf_op jit(solution)/shard_map/reduce_scatter | solution.py:53
  168.0 2.3 copy.51
  170.3 0.8 fusion.51
  171.2 0.3 fusion.2
  171.4 0.4 fusion.4
  171.8 1.1 broadcast_in_dim.23
  172.9 5.1 %all-to-all-start = ((bf16[16,512,64]{1,2,0:T(8,128)(2,1)}), bf16[16,512,64]{1,2,0:T(8,128)(2,1)S(1)}, u32[]{:S(2)}, u32[]{:S(2)}) async-start(bf16[16,512,64]{1,2,0:T(8,128)(2,1)} %broadcast_in_dim.23), calls=%async_computation | async-start | bytes 2097152 | tf_op jit(solution)/shard_map/all_to_all | solution.py:43
  178.1 25.0 %reduce-scatter.7.cloned.1.call-done = bf16[128,1024]{1,0:T(8,128)(2,1)} async-done(((bf16[512,1024]{1,0:T(8,128)(2,1)}), bf16[128,1024]{1,0:T(8,128)(2,1)}) %reduce-scatter.7.cloned.1.call-update) | async-done | bytes 262160
  203.0 1.8 copy.52
  204.8 14.1 %all-to-all-start.3 = ((bf16[128,1,32,32]{0,3,1,2:T(8,128)(2,1)}), bf16[128,1,32,32]{0,3,1,2:T(8,128)(2,1)S(1)}, u32[]{:S(2)}, u32[]{:S(2)}) async-start(bf16[128,1,32,32]{0,3,1,2:T(8,128)(2,1)} %bitcast.36), calls=%async_computation.4 | async-start | bytes 524288 | tf_op jit(solution)/shard_map/all_to_all | solution.py:171
  218.9 0.1 reduce_sum.42
  219.1 0.1 copy.44
  219.1 0.2 copy.45
  219.3 0.1 copy.50
  219.5 1.1 convolution_convert_fusion
  220.7 20.5 %all-to-all-done.3 = bf16[128,1,32,32]{0,3,1,2:T(8,128)(2,1)S(1)} async-done(((bf16[128,1,32,32]{0,3,1,2:T(8,128)(2,1)}), bf16[128,1,32,32]{0,3,1,2:T(8,128)(2,1)S(1)}, u32[]{:S(2)}, u32[]{:S(2)}) %all-to-all-start.3) | async-done | bytes 262176 | tf_op jit(solution)/shard_map/all_to_all | solution.py:171
  241.2 1.3 gather_fusion
  242.5 2.1 multiply_reduce_fusion.1
  (42 shorter events, 0.3 us)
Async XLA Ops:
  7.2 107.5 %copy-start = (bf16[1,256,2048]{2,1,0:T(8,128)(2,1)S(1)}, bf16[1,256,2048]{2,1,0:T(8,128)(2,1)}, u32[]{:S(2)}) copy-start(bf16[1,256,2048]{2,1,0:T(8,128)(2,1)} %param.23) | copy-start | bytes 3145732
  7.2 160.8 %reduce-scatter.5.cloned.1.call-start = ((), (), s32[]{:S(2)}) async-start(), calls=%async_computation.6 | async-start | bytes 5242880 | tf_op jit(solution)/shard_map/reduce_scatter | solution.py:53
  7.2 1.6 copy-start.1
  7.2 1.9 copy-start.7
  54.9 58.4 %copy-start.9 = (bf16[1,2048,256]{2,1,0:T(8,128)(2,1)S(1)}, bf16[1,2048,256]{2,1,0:T(8,128)(2,1)}, u32[]{:S(2)}) copy-start(bf16[1,2048,256]{2,1,0:T(8,128)(2,1)} %param.21) | copy-start | bytes 3145732
  111.4 2.0 copy-start.2
  113.4 1.3 copy-start.10
  123.2 0.8 copy-start.4
  123.2 1.0 copy-start.5
  123.2 1.1 copy-start.6
  123.2 79.8 %reduce-scatter.7.cloned.1.call-start = ((), (), s32[]{:S(2)}) async-start(), calls=%async_computation.7 | async-start | bytes 1310720
  125.8 6.1 %collective-permute-start = (bf16[2,128,1,64]{3,1,2,0:T(8,128)(2,1)S(1)}, bf16[2,128,1,64]{3,1,2,0:T(8,128)(2,1)S(1)}, u32[]{:S(2)}, u32[]{:S(2)}) collective-permute-start(bf16[2,128,1,64]{3,1,2,0:T(8,128)(2,1)S(1)} %get-tuple-element.2), channel_id=1, source_target_pairs={{0,16},{16,32},{32,48},{48,64},{64,80},{80,96},{96,112},{112,128},... | collective-permute-start | bytes 98312 | tf_op jit(solution)/shard_map/ppermute | solution.py:27
  129.1 6.0 %collective-permute-start.1 = (bf16[2,128,1,64]{3,1,2,0:T(8,128)(2,1)S(1)}, bf16[2,128,1,64]{3,1,2,0:T(8,128)(2,1)S(1)}, u32[]{:S(2)}, u32[]{:S(2)}) collective-permute-start(bf16[2,128,1,64]{3,1,2,0:T(8,128)(2,1)S(1)} %get-tuple-element.3), channel_id=1, source_target_pairs={{16,0},{32,16},{48,32},{64,48},{80,64},{96,80},{112,96},{128,112},... | collective-permute-start | bytes 98312 | tf_op jit(solution)/shard_map/ppermute | solution.py:30
  172.9 46.4 %copy-start.8 = (f32[256,2]{0,1:T(2,128)S(1)}, f32[256,2]{0,1:T(2,128)}, u32[]{:S(2)}) copy-start(f32[256,2]{0,1:T(2,128)} %param.20) | copy-start | bytes 6148
  172.9 46.6 %copy-start.3 = (bf16[1024,128]{1,0:T(8,128)(2,1)S(1)}, bf16[1024,128]{1,0:T(8,128)(2,1)}, u32[]{:S(2)}) copy-start(bf16[1024,128]{1,0:T(8,128)(2,1)} %param.16) | copy-start | bytes 786436
  172.9 31.9 %all-to-all-start = ((bf16[16,512,64]{1,2,0:T(8,128)(2,1)}), bf16[16,512,64]{1,2,0:T(8,128)(2,1)S(1)}, u32[]{:S(2)}, u32[]{:S(2)}) async-start(bf16[16,512,64]{1,2,0:T(8,128)(2,1)} %broadcast_in_dim.23), calls=%async_computation | async-start | bytes 2097152 | tf_op jit(solution)/shard_map/all_to_all | solution.py:43
  204.8 36.3 %all-to-all-start.3 = ((bf16[128,1,32,32]{0,3,1,2:T(8,128)(2,1)}), bf16[128,1,32,32]{0,3,1,2:T(8,128)(2,1)S(1)}, u32[]{:S(2)}, u32[]{:S(2)}) async-start(bf16[128,1,32,32]{0,3,1,2:T(8,128)(2,1)} %bitcast.36), calls=%async_computation.4 | async-start | bytes 524288 | tf_op jit(solution)/shard_map/all_to_all | solution.py:171
Sparse Core Ops, SparseCore 0:
  123.3 44.6 reduce-scatter.4
  170.8 32.1 reduce-scatter.6
where the time goes:
time: 252 us; the launch traced here: 251 us
  blocking collectives  95.3 us (38%)
  waiting for transfers between devices  81.4 us (32%)
  starting transfers between devices  24.7 us (10%)
  local copies, waits for them, and re-layouts  15.5 us (6%)
  between operations  15.1 us (6%)
  matrix products  12.1 us (5%)
  other arithmetic  7.36 us (3%)
    all_to_all x1, blocking collectives, copy_for_each(): lax.all_to_all(jnp.broadcast_to(x[None], (devices, *x.shape)), axis, 0, 0...  56.5 us
    all_to_all x1, blocking collectives, expert_half(): lax.all_to_all(outgoing.reshape(expert_count, capacity, col_count), 'ep',...  38.8 us
    reduce_scatter x1, waiting for transfers between devices, own_rows(): so_far = lax.psum_scatter(so_far, axis, scatter_dimension=0, tiled=True)  32.8 us
    unnamed x3, waiting for transfers between devices  25 us
    all_to_all x1, waiting for transfers between devices, expert_half(): lax.all_to_all(result, 'ep', split_axis=2, concat_axis=1, tiled=True)  20.5 us
    all_to_all x1, starting transfers between devices, expert_half(): lax.all_to_all(result, 'ep', split_axis=2, concat_axis=1, tiled=True)  14.1 us
    dot_general x1, matrix products, expert_half(): jnp.einsum('esh,ehc->ces', hidden, down_weight, preferred_element_type=jn...  8.49 us
    unnamed x27, local copies, waits for them, and re-layouts  7.23 us
  transfers between devices with their start and end apart: 6, of which 4 were waited for; matrix products, arithmetic and copies ran while one was open for 3% of the time, Pallas kernels for 0%

commit v1 on v0

v1 whole, which is shorter than its diff:
```python
import functools

import jax
import jax.numpy as jnp
from jax import lax
from jax.experimental import pallas as pl
from jax.experimental.pallas import tpu as pltpu
from jax.sharding import Mesh
from jax.sharding import PartitionSpec as P

D = 2048
HEADS = 16
KV_HEADS = 4
HEAD_DIM = 64
HALF_WIN = 128
ROWS_B = 256
EXPERTS = 32
CAP = 32
EP = ("z", "co")
TP = ("y", "x")
PLANE = ("co", "y", "x")

NORM_EPS = 1e-06
ROPE_BASE = 10000.0
NEG_BIG = -1e30

LINE_L = [[y * 4 + x for x in range(4)] for y in range(4)] + [
    [16 + y * 4 + x for y in range(4)] for x in range(4)
]
LINE_M = [[y * 4 + x for y in range(4)] for x in range(4)] + [
    [16 + y * 4 + x for x in range(4)] for y in range(4)
]
WHOLE = [list(range(16)), [16 + (p % 4) * 4 + p // 4 for p in range(16)]]

ANY = pl.BlockSpec(memory_space=pl.ANY)
VMEM = pl.BlockSpec(memory_space=pltpu.VMEM)
HALF_W = 3072


def line_shift(x, step):
    pairs = [(line[i], line[(i + step) % 4]) for line in LINE_L for i in range(4)]
    return lax.ppermute(x, PLANE, pairs)


def prep_kernel(
    x_ref, gain_ref, routes_ref, gate_ref, up_ref, down_ref,
    out_ref, slot_ref, wa_ref, wb_ref, normed_ref, sems,
):
    copies = [
        (gate_ref.at[0], wa_ref.at[pl.ds(0, 2048)]),
        (up_ref.at[0, pl.ds(0, 1024)], wa_ref.at[pl.ds(2048, 1024)]),
        (up_ref.at[0, pl.ds(1024, 1024)], wb_ref.at[pl.ds(0, 1024)]),
    ] + [
        (down_ref.at[0, :, pl.ds(c * 256, 256)], wb_ref.at[pl.ds(1024 + c * 256, 256)])
        for c in range(8)
    ]
    copies = [pltpu.make_async_copy(s, d, sems.at[i]) for i, (s, d) in enumerate(copies)]
    for copy in copies:
        copy.start()

    def norm_rows(i, carry):
        rows = pl.ds(pl.multiple_of(i * 32, 32), 32)
        wide = x_ref[rows, :].astype(jnp.float32)
        scale = lax.rsqrt(jnp.mean(wide * wide, axis=1, keepdims=True) + NORM_EPS)
        normed_ref[rows, :] = (wide * scale * gain_ref[...]).astype(jnp.bfloat16)
        return carry

    lax.fori_loop(0, ROWS_B // 32, norm_rows, 0)

    first = routes_ref[:, 0:1]
    second = routes_ref[:, 1:2]
    expert = lax.broadcasted_iota(jnp.int32, (ROWS_B, 128), 1)
    named = jnp.where((first == expert) | (second == expert), 1.0, 0.0)
    row = lax.broadcasted_iota(jnp.int32, (ROWS_B, ROWS_B), 0)
    col = lax.broadcasted_iota(jnp.int32, (ROWS_B, ROWS_B), 1)
    below = jnp.where(col < row, 1.0, 0.0).astype(jnp.bfloat16)
    above = jnp.where(row < col, 1.0, 0.0).astype(jnp.bfloat16)
    rank = jnp.dot(below, named.astype(jnp.bfloat16), preferred_element_type=jnp.float32)
    rank_a = jnp.sum(jnp.where(first == expert, rank, 0.0), axis=1, keepdims=True)
    rank_b = jnp.sum(jnp.where(second == expert, rank, 0.0), axis=1, keepdims=True)
    slot_a = first * CAP + rank_a.astype(jnp.int32)
    slot_b = second * CAP + rank_b.astype(jnp.int32)
    pair = lax.broadcasted_iota(jnp.int32, (ROWS_B, 2), 1)
    slot_ref[...] = jnp.where(pair == 0, slot_a, slot_b)

    named_t = named.T
    rank_t = jnp.dot(named_t.astype(jnp.bfloat16), above, preferred_element_type=jnp.float32)
    mark = jnp.where(named_t > 0.5, rank_t, -1.0).astype(jnp.bfloat16)
    spread = jnp.where(
        (lax.broadcasted_iota(jnp.int32, (ROWS_B, 128), 0) >> 3) == expert, 1.0, 0.0
    ).astype(jnp.bfloat16)
    mark_rows = jnp.dot(spread, mark, preferred_element_type=jnp.float32)
    xi = lax.axis_index("x")
    yi = lax.axis_index("y")
    even = ((row >> 3) & 1) == 0
    wanted = jnp.where(even, xi, yi) * 8 + (row & 7)
    pick = jnp.where(mark_rows.astype(jnp.int32) == wanted, 1.0, 0.0).astype(jnp.bfloat16)
    from_y = jnp.dot(
        pick, normed_ref[:, pl.ds(pl.multiple_of(yi * 512, 512), 512)],
        preferred_element_type=jnp.float32,
    )
    from_x = jnp.dot(
        pick, normed_ref[:, pl.ds(pl.multiple_of(xi * 512, 512), 512)],
        preferred_element_type=jnp.float32,
    )
    even_row = ((lax.broadcasted_iota(jnp.int32, (ROWS_B, 512), 0) >> 3) & 1) == 0
    out_ref[...] = jnp.where(even_row, from_y, from_x).astype(jnp.bfloat16)
    for copy in copies:
        copy.wait()


def prepare(expert_input, norm_gain, routes, gate, up, down):
    half = jax.ShapeDtypeStruct((HALF_W, 256), jnp.bfloat16)
    return pl.pallas_call(
        prep_kernel,
        out_shape=(
            jax.ShapeDtypeStruct((ROWS_B, 512), jnp.bfloat16),
            jax.ShapeDtypeStruct((ROWS_B, 2), jnp.int32),
            half,
            half,
        ),
        in_specs=[VMEM, VMEM, VMEM, ANY, ANY, ANY],
        out_specs=(VMEM, VMEM, ANY, ANY),
        scratch_shapes=[pltpu.VMEM((ROWS_B, D), jnp.bfloat16), pltpu.SemaphoreType.DMA((11,))],
        name="prep",
    )(expert_input, norm_gain.reshape(1, D), routes, gate, up, down)


def slice_hidden(x_ref, wa, wb):
    def part(m, ref, start):
        return jnp.dot(x_ref[m], ref[pl.ds(start, 512), :], preferred_element_type=jnp.float32)

    gate = part(0, wa, 0) + part(1, wa, 512) + part(2, wa, 1024) + part(3, wa, 1536)
    up = part(0, wa, 2048) + part(1, wa, 2560) + part(2, wb, 0) + part(3, wb, 512)
    return (gate / (1.0 + jnp.exp(-gate)) * up).astype(jnp.bfloat16)


def ffn_most_kernel(x_ref, *refs):
    weights, acc_ref, bufs, sems = refs[:6], refs[6], refs[7], refs[8]
    copies = [
        pltpu.make_async_copy(w, bufs.at[i], sems.at[i]) for i, w in enumerate(weights)
    ]
    for copy in copies:
        copy.start()
    for s in range(3):
        copies[2 * s].wait()
        copies[2 * s + 1].wait()
        wa, wb = bufs.at[2 * s], bufs.at[2 * s + 1]
        hidden = slice_hidden(x_ref, wa, wb)
        for c in range(8):
            cols = pl.ds(c * 256, 256)
            term = jnp.dot(
                hidden, wb[pl.ds(1024 + c * 256, 256), :], preferred_element_type=jnp.float32
            )
            acc_ref[:, cols] = term if s == 0 else acc_ref[:, cols] + term


def ffn_most(x, *weights):
    return pl.pallas_call(
        ffn_most_kernel,
        out_shape=jax.ShapeDtypeStruct((ROWS_B, D), jnp.float32),
        in_specs=[VMEM] + [ANY] * 6,
        out_specs=VMEM,
        scratch_shapes=[
            pltpu.VMEM((6, HALF_W, 256), jnp.bfloat16), pltpu.SemaphoreType.DMA((6,))
        ],
        name="ffn_most",
    )(x, *weights)


def ffn_last_kernel(x_ref, acc_ref, wa_ref, wb_ref, out_ref):
    core = lax.axis_index("co")
    hidden = slice_hidden(x_ref, wa_ref, wb_ref)
    for c in range(8):
        total = acc_ref[:, pl.ds(c * 256, 256)] + jnp.dot(
            hidden, wb_ref[pl.ds(1024 + c * 256, 256), :], preferred_element_type=jnp.float32
        )
        for k in range(2):
            t = 2 * c + k
            place = jnp.where(core == 0, t, (t % 4) * 4 + t // 4)
            out_ref[place] = total[:, k * 128 : (k + 1) * 128].astype(jnp.bfloat16)


def ffn_last(x, acc, wa, wb):
    return pl.pallas_call(
        ffn_last_kernel,
        out_shape=jax.ShapeDtypeStruct((16, ROWS_B, 128), jnp.bfloat16),
        in_specs=[VMEM] * 4,
        out_specs=VMEM,
        name="ffn_last",
    )(x, acc, wa, wb)


def combine_kernel(ret_ref, slot_ref, weight_ref, out_ref):
    place = lax.broadcasted_iota(jnp.int32, (ROWS_B, EXPERTS * CAP), 1)
    total = None
    for k in range(2):
        pick = jnp.where(place == slot_ref[:, k : k + 1], 1.0, 0.0).astype(jnp.bfloat16)
        rows = jnp.dot(pick, ret_ref[...], preferred_element_type=jnp.float32)
        term = rows * weight_ref[:, k : k + 1]
        total = term if total is None else total + term
    out_ref[...] = total.astype(jnp.bfloat16)


def combine(returned, slots, route_weights):
    return pl.pallas_call(
        combine_kernel,
        out_shape=jax.ShapeDtypeStruct((ROWS_B, 128), jnp.bfloat16),
        in_specs=[VMEM] * 3,
        out_specs=VMEM,
        name="combine",
    )(returned, slots, route_weights)


def padded(block, axis, dim, width):
    count = lax.axis_size(axis)
    forward = [(i, i + 1) for i in range(count - 1)]
    backward = [(target, source) for source, target in forward]
    low = lax.ppermute(
        lax.slice_in_dim(block, block.shape[dim] - width, None, axis=dim), axis, forward
    )
    high = lax.ppermute(lax.slice_in_dim(block, 0, width, axis=dim), axis, backward)
    return jnp.concatenate([low, block, high], axis=dim)


def collect(x, axis, dim):
    devices = lax.axis_size(axis)
    blocks = lax.all_to_all(
        jnp.broadcast_to(x[None], (devices, *x.shape)), axis, 0, 0, tiled=True
    )
    dims = list(x.shape)
    dims[dim] *= devices
    return jnp.moveaxis(blocks, 0, dim).reshape(dims)


def rotate(features, position_start):
    count = features.shape[0]
    half_dim = features.shape[-1] // 2
    inverse_freq = 1.0 / ROPE_BASE ** (
        jnp.arange(half_dim, dtype=jnp.float32) * 2.0 / features.shape[-1]
    )
    position = (jnp.arange(count, dtype=jnp.int32) + position_start).astype(jnp.float32)
    angles = position[:, None] * inverse_freq[None, :]
    cosine = jnp.cos(angles)[:, None, :]
    sine_part = jnp.sin(angles)[:, None, :]
    lower_half = features[..., :half_dim]
    upper_half = features[..., half_dim:]
    return jnp.concatenate(
        [
            lower_half * cosine - upper_half * sine_part,
            upper_half * cosine + lower_half * sine_part,
        ],
        axis=-1,
    )


def attend(query_proj, key_proj, value_proj, sink_logit):
    row_count = query_proj.shape[0]
    local_heads = query_proj.shape[1] // HEAD_DIM
    per_kv = HEADS // KV_HEADS
    kv_local = max(1, local_heads // per_kv)
    group_size = local_heads // kv_local
    tp_index = lax.axis_index(TP)
    offset = lax.axis_index(EP) * row_count
    seq_total = row_count * lax.axis_size(EP)
    first_kv = tp_index * local_heads // per_kv
    own_keys = lax.dynamic_slice_in_dim(key_proj, first_kv * HEAD_DIM, kv_local * HEAD_DIM, 1)
    own_values = lax.dynamic_slice_in_dim(value_proj, first_kv * HEAD_DIM, kv_local * HEAD_DIM, 1)
    rot_q = rotate(
        query_proj.reshape(row_count, local_heads, HEAD_DIM).astype(jnp.float32), offset
    ).astype(jnp.bfloat16)
    rot_k = rotate(
        own_keys.reshape(row_count, kv_local, HEAD_DIM).astype(jnp.float32), offset
    ).astype(jnp.bfloat16)
    stacked = jnp.stack([rot_k, own_values.reshape(row_count, kv_local, HEAD_DIM)])
    extended = padded(stacked, EP, 1, HALF_WIN)
    own_sink = sink_logit.reshape(kv_local, group_size)
    block_rows = row_count
    key_rows = block_rows + 2 * HALF_WIN
    key_offset = jnp.arange(key_rows, dtype=jnp.int32) - HALF_WIN
    key_gap = key_offset[None, :] - jnp.arange(block_rows, dtype=jnp.int32)[:, None]
    query_block = rot_q.reshape(block_rows, kv_local, group_size, HEAD_DIM)
    scores = jnp.einsum(
        "qngd,knd->ngqk", query_block, extended[0], preferred_element_type=jnp.float32
    ) * HEAD_DIM ** (-0.5)
    global_key = offset + key_offset
    allowed = (
        (jnp.abs(key_gap) <= HALF_WIN)
        & (global_key >= 0)[None, :]
        & (global_key < seq_total)[None, :]
    )
    scores = jnp.where(allowed[None, None], scores, NEG_BIG)
    row_peak = jnp.maximum(jnp.max(scores, axis=-1), own_sink[:, :, None])
    lifted = jnp.exp(scores - row_peak[..., None])
    norm_total = jnp.sum(lifted, axis=-1) + jnp.exp(own_sink[:, :, None] - row_peak)
    probs = (lifted / norm_total[..., None]).astype(jnp.bfloat16)
    weighted = jnp.einsum("ngqk,knd->qngd", probs, extended[1], preferred_element_type=jnp.float32)
    return weighted.astype(jnp.bfloat16).reshape(block_rows, local_heads * HEAD_DIM)


def local(
    query_proj,
    key_proj,
    value_proj,
    sink_logit,
    out_weight,
    expert_input,
    norm_gain,
    routes,
    route_weights,
    gate_weight,
    up_weight,
    down_weight,
):
    outgoing, slots, wa, wb = prepare(
        expert_input, norm_gain, routes, gate_weight, up_weight, down_weight
    )
    prev_a = line_shift(wa, 1)
    next_b = line_shift(wb, -1)
    next_a = line_shift(wa, -1)
    prev_b = line_shift(wb, 1)
    arrived = lax.all_to_all(outgoing, EP, 0, 0, tiled=True)
    prev_a, next_b, arrived = lax.optimization_barrier((prev_a, next_b, arrived))
    far_a = line_shift(prev_a, 1)
    far_b = line_shift(next_b, -1)

    attended = attend(query_proj, key_proj, value_proj, sink_logit)

    rows = lax.all_to_all(
        jnp.broadcast_to(arrived[None], (4, *arrived.shape)),
        PLANE, 0, 0, tiled=True, axis_index_groups=LINE_M,
    )
    acc = ffn_most(rows, wa, wb, prev_a, prev_b, next_a, next_b)
    partial = ffn_last(rows, acc, far_a, far_b)
    parts = lax.all_to_all(partial, PLANE, 0, 0, tiled=True, axis_index_groups=WHOLE)
    result = jnp.sum(parts.reshape(4, 4, EXPERTS, 8, 128).astype(jnp.float32), axis=0)
    result = jnp.moveaxis(result.astype(jnp.bfloat16), 0, 1).reshape(EXPERTS, CAP, 128)
    returned = lax.all_to_all(result, EP, 0, 0, tiled=True)
    expert_out = combine(returned.reshape(EXPERTS * CAP, 128), slots, route_weights)

    gathered = collect(attended, TP, 1)
    mixer_out = jnp.dot(gathered, out_weight, preferred_element_type=jnp.float32)
    return (mixer_out.astype(jnp.bfloat16), expert_out)


def solution(mesh):
    finer = Mesh(mesh.devices.reshape(16, 2, 4, 4), ("z", "co", "y", "x"))
    in_specs = (
        P(EP, TP),
        P(EP, None),
        P(EP, None),
        P(TP),
        P(None, TP),
        P(EP, None),
        P(),
        P(EP, None),
        P(EP, None),
        P(EP, None, TP),
        P(EP, None, TP),
        P(EP, TP, None),
    )
    out_specs = (P(EP, TP), P(EP, TP))
    return jax.shard_map(local, mesh=finer, in_specs=in_specs, out_specs=out_specs, check_vma=False)
```

time: 252 us -> 263 us (1.044)
  Pallas kernels: 0 us -> 113 us
  blocking collectives: 95.3 us -> 0 us
  starting transfers between devices: 24.7 us -> 63.1 us
  between operations: 15.1 us -> 1.6 us
  waiting for transfers between devices: 81.4 us -> 71.6 us
  matrix products: 12.1 us -> 2.38 us
  local copies, waits for them, and re-layouts: 15.5 us -> 7.21 us
  other arithmetic: 7.36 us -> 2.79 us
    pallas_call x0 -> x4, Pallas kernels: none -> 113 us  [the longest x1 98.6 us: prepare(): pl.pallas_call(prep_kernel, out_shape=(jax.ShapeDtypeStruct((ROWS_B, 512)...]
    all_to_all x2 -> x0, blocking collectives: 95.3 us -> none  [the longest x1 56.5 us: copy_for_each(): lax.all_to_all(jnp.broadcast_to(x[None], (devices, *x.shape)), axis, 0, 0...]
    all_to_all x2 -> x5, waiting for transfers between devices: 20.5 us -> 66.2 us  [the longest x1 20.3 us: local(): returned = lax.all_to_all(result, EP, 0, 0, tiled=True)]
    reduce_scatter x1 -> x0, waiting for transfers between devices: 32.8 us -> none  [own_rows(): so_far = lax.psum_scatter(so_far, axis, scatter_dimension=0, tiled=True)]
    unnamed x3 -> x0, waiting for transfers between devices: 25 us -> none
    ppermute x0 -> x6, starting transfers between devices: none -> 20.5 us  [line_shift(): return lax.ppermute(x, PLANE, pairs)]
    all_to_all x2 -> x5, starting transfers between devices: 19.2 us -> 37.1 us  [the longest x1 16.4 us: local(): arrived = lax.all_to_all(outgoing, EP, 0, 0, tiled=True)]
    dot_general x5 -> x3, matrix products: 12.1 us -> 2.38 us  [the longest x1 1.14 us: local(): jnp.dot(gathered, out_weight, preferred_element_type=jnp.float32)]
  transfers between devices with their start and end apart: 6 -> 13, of which waited for: 4 -> 7; matrix products, arithmetic and copies ran while one was open for 3% -> 3% of each run, Pallas kernels for 0% -> 3%
where the time goes in v1:
time: 263 us; the launch traced here: 262 us
  Pallas kernels  113 us (43%)
  waiting for transfers between devices  71.6 us (27%)
  starting transfers between devices  63.1 us (24%)
  local copies, waits for them, and re-layouts  7.21 us (3%)
  other arithmetic  2.79 us (1%)
    pallas_call x1, Pallas kernels, prepare(): pl.pallas_call(prep_kernel, out_shape=(jax.ShapeDtypeStruct((ROWS_B, 512)...  98.6 us
    ppermute x6, starting transfers between devices, line_shift(): return lax.ppermute(x, PLANE, pairs)  20.5 us
    all_to_all x1, waiting for transfers between devices, local(): returned = lax.all_to_all(result, EP, 0, 0, tiled=True)  20.3 us
    all_to_all x1, starting transfers between devices, local(): arrived = lax.all_to_all(outgoing, EP, 0, 0, tiled=True)  16.4 us
    all_to_all x1, waiting for transfers between devices, local(): arrived = lax.all_to_all(outgoing, EP, 0, 0, tiled=True)  15.7 us
    all_to_all x1, waiting for transfers between devices, local(): lax.all_to_all(partial, PLANE, 0, 0, tiled=True, axis_index_groups=WHOLE)  14.4 us
    all_to_all x1, waiting for transfers between devices, collect(): lax.all_to_all(jnp.broadcast_to(x[None], (devices, *x.shape)), axis, 0, 0...  14 us
    all_to_all x1, starting transfers between devices, local(): returned = lax.all_to_all(result, EP, 0, 0, tiled=True)  9.68 us
  transfers between devices with their start and end apart: 13, of which 7 were waited for; matrix products, arithmetic and copies ran while one was open for 3% of the time, Pallas kernels for 3%

profile of v1, /device:TPU:1, one launch (start us, length us, event | category | flops | bytes accessed | tf_op | source)
XLA Modules:
  0.0 261.9 jit_solution(11382733862115779666)
XLA Ops:
  0.6 0.0 copy-start
  0.6 1.5 copy.25.routes_ref
  2.2 98.6 %prep.1 = (bf16[256,512]{1,0:T(8,128)(2,1)}, s32[256,2]{1,0:T(8,128)}, bf16[3072,256]{1,0:T(8,128)(2,1)}, bf16[3072,256]{1,0:T(8,128)(2,1)}) custom-call(bf16[256,2048]{1,0:T(8,128)(2,1)} %x_ref.1, f32[1,2048]{1,0:T(1,128)} %bitcast.60, s32[256,2]{1,0:T(8,128)} %copy.25.routes_ref, bf16[1,2048,256]{2,1,0:T(8,128)(2,1)} %gate_ref.1, ...), custom_call_target="tpu_custom_call" | custom-call | tf_op jit(solution)/shard_map/prep/pallas_call | solution.py:114
  100.7 4.0 %collective-permute-start.2 = (bf16[3072,256]{1,0:T(8,128)(2,1)}, bf16[3072,256]{1,0:T(8,128)(2,1)S(1)}, u32[]{:S(2)}, u32[]{:S(2)}) collective-permute-start(bf16[3072,256]{1,0:T(8,128)(2,1)} %get-tuple-element.9.refs_0_), channel_id=1, source_target_pairs={{0,1},{1,2},{2,3},{3,0},{4,5},{5,6},{6,7},{7,4},{8,9},{9,10},{10,1... | collective-permute-start | bytes 4718600 | tf_op jit(solution)/shard_map/ppermute | solution.py:42
  104.8 3.4 %collective-permute-start.3 = (bf16[3072,256]{1,0:T(8,128)(2,1)}, bf16[3072,256]{1,0:T(8,128)(2,1)}, u32[]{:S(2)}, u32[]{:S(2)}) collective-permute-start(bf16[3072,256]{1,0:T(8,128)(2,1)} %get-tuple-element.10.refs_1_), channel_id=1, source_target_pairs={{0,3},{1,0},{2,1},{3,2},{4,7},{5,4},{6,5},{7,6},{8,11},{9,8},{10,9... | collective-permute-start | bytes 4718600 | tf_op jit(solution)/shard_map/ppermute | solution.py:42
  108.1 16.4 %all-to-all-start.1 = ((bf16[32,8,512]{2,1,0:T(8,128)(2,1)}), bf16[32,8,512]{2,1,0:T(8,128)(2,1)S(1)}, u32[]{:S(2)}, u32[]{:S(2)}) async-start(bf16[32,8,512]{2,1,0:T(8,128)(2,1)} %bitcast.59), calls=%async_computation.1 | async-start | bytes 524288 | tf_op jit(solution)/shard_map/all_to_all | solution.py:322
  124.6 3.2 %collective-permute-start.4 = (bf16[3072,256]{1,0:T(8,128)(2,1)}, bf16[3072,256]{1,0:T(8,128)(2,1)}, u32[]{:S(2)}, u32[]{:S(2)}) collective-permute-start(bf16[3072,256]{1,0:T(8,128)(2,1)} %get-tuple-element.10.refs_1_), channel_id=1, source_target_pairs={{0,1},{1,2},{2,3},{3,0},{4,5},{5,6},{6,7},{7,4},{8,9},{9,10},{10,1... | collective-permute-start | bytes 4718600 | tf_op jit(solution)/shard_map/ppermute | solution.py:42
  127.8 3.4 %collective-permute-start.5 = (bf16[3072,256]{1,0:T(8,128)(2,1)}, bf16[3072,256]{1,0:T(8,128)(2,1)}, u32[]{:S(2)}, u32[]{:S(2)}) collective-permute-start(bf16[3072,256]{1,0:T(8,128)(2,1)} %get-tuple-element.9.refs_0_), channel_id=1, source_target_pairs={{0,3},{1,0},{2,1},{3,2},{4,7},{5,4},{6,5},{7,6},{8,11},{9,8},{10,9... | collective-permute-start | bytes 4718600 | tf_op jit(solution)/shard_map/ppermute | solution.py:42
  131.1 15.7 %all-to-all-done.1 = bf16[32,8,512]{2,1,0:T(8,128)(2,1)S(1)} async-done(((bf16[32,8,512]{2,1,0:T(8,128)(2,1)}), bf16[32,8,512]{2,1,0:T(8,128)(2,1)S(1)}, u32[]{:S(2)}, u32[]{:S(2)}) %all-to-all-start.1) | async-done | bytes 262176 | tf_op jit(solution)/shard_map/all_to_all | solution.py:322
  146.8 0.0 collective-permute-done.2.refs_2_
  146.8 0.0 collective-permute-done.3.refs_5_
  146.8 3.2 %collective-permute-start.6 = (bf16[3072,256]{1,0:T(8,128)(2,1)S(1)}, bf16[3072,256]{1,0:T(8,128)(2,1)}, u32[]{:S(2)}, u32[]{:S(2)}) collective-permute-start(bf16[3072,256]{1,0:T(8,128)(2,1)S(1)} %collective-permute-done.2.refs_2_), channel_id=1, source_target_pairs={{0,1},{1,2},{2,3},{3,0},{4,5},{5,6},{6,7},{7,4},{8,9},{9,10},{10,1... | collective-permute-start | bytes 4718600 | tf_op jit(solution)/shard_map/ppermute | solution.py:42
  150.0 3.4 %collective-permute-start.7 = (bf16[3072,256]{1,0:T(8,128)(2,1)}, bf16[3072,256]{1,0:T(8,128)(2,1)}, u32[]{:S(2)}, u32[]{:S(2)}) collective-permute-start(bf16[3072,256]{1,0:T(8,128)(2,1)} %collective-permute-done.3.refs_5_), channel_id=1, source_target_pairs={{0,3},{1,0},{2,1},{3,2},{4,7},{5,4},{6,5},{7,6},{8,11},{9,8},{10,9... | collective-permute-start | bytes 4718600 | tf_op jit(solution)/shard_map/ppermute | solution.py:42
  153.4 0.1 copy.24
  153.6 0.1 dynamic-slice_bitcast_fusion
  153.7 0.1 bitcast_convert_fusion
  153.8 1.1 broadcast_in_dim.12
  154.9 3.5 %all-to-all-start.2 = ((bf16[4,256,512]{2,1,0:T(8,128)(2,1)}), bf16[4,256,512]{2,1,0:T(8,128)(2,1)S(1)}, u32[]{:S(2)}, u32[]{:S(2)}) async-start(bf16[4,256,512]{2,1,0:T(8,128)(2,1)} %broadcast_in_dim.12), calls=%async_computation.2 | async-start | bytes 2097152 | tf_op jit(solution)/shard_map/all_to_all | solution.py:329
  158.5 1.9 fusion.25
  160.4 0.1 pad_maximum_fusion.3
  160.5 3.7 %collective-permute-start = (bf16[2,128,1,64]{3,1,2,0:T(8,128)(2,1)S(1)}, bf16[2,128,1,64]{3,1,2,0:T(8,128)(2,1)S(1)}, u32[]{:S(2)}, u32[]{:S(2)}) collective-permute-start(bf16[2,128,1,64]{3,1,2,0:T(8,128)(2,1)S(1)} %get-tuple-element.16), channel_id=1, source_target_pairs={{0,16},{16,32},{32,48},{48,64},{64,80},{80,96},{96,112},{112,128},... | collective-permute-start | bytes 98312 | tf_op jit(solution)/shard_map/ppermute | solution.py:219
  164.2 1.3 collective-permute-done
  165.5 1.9 collective-permute-start.1
  168.0 4.0 %collective-permute-done.1 = bf16[2,128,1,64]{3,1,2,0:T(8,128)(2,1)S(1)} collective-permute-done((bf16[2,128,1,64]{3,1,2,0:T(8,128)(2,1)S(1)}, bf16[2,128,1,64]{3,1,2,0:T(8,128)(2,1)S(1)}, u32[]{:S(2)}, u32[]{:S(2)}) %collective-permute-start.1) | collective-permute-done | bytes 32800 | tf_op jit(solution)/shard_map/ppermute | solution.py:222
  172.1 0.1 pad_maximum_fusion
  172.2 0.0 collective-permute-done.5.refs_4_
  172.2 1.9 all-to-all-done.2.x_ref
  174.1 1.0 copy-done.1
  175.1 7.6 %ffn_most.1.acc_ref = f32[256,2048]{1,0:T(8,128)} custom-call(bf16[4,256,512]{2,1,0:T(8,128)(2,1)} %copy-done.1, bf16[3072,256]{1,0:T(8,128)(2,1)} %get-tuple-element.9.refs_0_, bf16[3072,256]{1,0:T(8,128)(2,1)} %get-tuple-element.10.refs_1_, bf16[3072,256]{1,0:T(8,128)(2,1)} %copy-done.2, bf16[3072,256]{1,0:T(8,128)(2,1)} %collective-permute-done.4.refs_3_, ...), custom_call_target="tpu_custom_call" | custom-call | tf_op jit(solution)/shard_map/ffn_most/pallas_call | solution.py:159
  182.7 0.0 collective-permute-done.7.wb_ref
  182.7 4.9 %ffn_last.1 = bf16[16,256,128]{2,1,0:T(8,128)(2,1)} custom-call(bf16[4,256,512]{2,1,0:T(8,128)(2,1)} %copy-done.1, f32[256,2048]{1,0:T(8,128)} %ffn_most.1.acc_ref, bf16[3072,256]{1,0:T(8,128)(2,1)} %collective-permute-done.6.wa_ref, bf16[3072,256]{1,0:T(8,128)(2,1)} %collective-permute-done.7.wb_ref), custom_call_target="tpu_custom_call" | custom-call | tf_op jit(solution)/shard_map/ffn_last/pallas_call | solution.py:185
  187.6 3.8 %all-to-all-start.3 = ((bf16[16,256,128]{2,1,0:T(8,128)(2,1)}), bf16[16,256,128]{2,1,0:T(8,128)(2,1)S(1)}, u32[]{:S(2)}, u32[]{:S(2)}) async-start(bf16[16,256,128]{2,1,0:T(8,128)(2,1)} %ffn_last.1), calls=%async_computation.3 | async-start | bytes 2097152 | tf_op jit(solution)/shard_map/all_to_all | solution.py:335
  191.5 0.8 fusion.29
  192.3 0.3 fusion.2
  192.6 0.4 fusion.3
  193.0 14.4 %all-to-all-done.3 = bf16[16,256,128]{2,1,0:T(8,128)(2,1)S(1)} async-done(((bf16[16,256,128]{2,1,0:T(8,128)(2,1)}), bf16[16,256,128]{2,1,0:T(8,128)(2,1)S(1)}, u32[]{:S(2)}, u32[]{:S(2)}) %all-to-all-start.3) | async-done | bytes 1048608 | tf_op jit(solution)/shard_map/all_to_all | solution.py:335
  207.4 1.1 broadcast_in_dim.11
  208.5 3.7 %all-to-all-start = ((bf16[16,512,64]{1,2,0:T(8,128)(2,1)}), bf16[16,512,64]{1,2,0:T(8,128)(2,1)S(1)}, u32[]{:S(2)}, u32[]{:S(2)}) async-start(bf16[16,512,64]{1,2,0:T(8,128)(2,1)} %broadcast_in_dim.11), calls=%async_computation | async-start | bytes 2097152 | tf_op jit(solution)/shard_map/all_to_all | solution.py:228
  212.2 0.0 copy-start.9
  212.2 0.2 reduce_sum.22
  212.4 0.7 copy_bitcast_fusion
  213.2 14.0 %all-to-all-done = bf16[16,512,64]{1,2,0:T(8,128)(2,1)S(1)} async-done(((bf16[16,512,64]{1,2,0:T(8,128)(2,1)}), bf16[16,512,64]{1,2,0:T(8,128)(2,1)S(1)}, u32[]{:S(2)}, u32[]{:S(2)}) %all-to-all-start) | async-done | bytes 1048608 | tf_op jit(solution)/shard_map/all_to_all | solution.py:228
  227.1 9.7 %all-to-all-start.4 = ((bf16[32,32,128]{2,1,0:T(8,128)(2,1)}), bf16[32,32,128]{2,1,0:T(8,128)(2,1)S(1)}, u32[]{:S(2)}, u32[]{:S(2)}) async-start(bf16[32,32,128]{2,1,0:T(8,128)(2,1)} %copy_bitcast_fusion), calls=%async_computation.4 | async-start | bytes 524288 | tf_op jit(solution)/shard_map/all_to_all | solution.py:338
  236.8 0.8 copy.27.weight_ref
  237.6 1.1 convolution_convert_fusion
  238.8 20.3 %all-to-all-done.4 = bf16[32,32,128]{2,1,0:T(8,128)(2,1)S(1)} async-done(((bf16[32,32,128]{2,1,0:T(8,128)(2,1)}), bf16[32,32,128]{2,1,0:T(8,128)(2,1)S(1)}, u32[]{:S(2)}, u32[]{:S(2)}) %all-to-all-start.4) | async-done | bytes 262176 | tf_op jit(solution)/shard_map/all_to_all | solution.py:338
  259.1 0.7 copy-done.3
  259.8 2.2 combine.1
  (24 shorter events, 0.1 us)
Async XLA Ops:
  0.6 237.0 %copy-start = (bf16[1024,128]{1,0:T(8,128)(2,1)S(1)}, bf16[1024,128]{1,0:T(8,128)(2,1)}, u32[]{:S(2)}) copy-start(bf16[1024,128]{1,0:T(8,128)(2,1)} %param.16) | copy-start | bytes 786436
  2.2 151.3 %copy-start.6 = (bf16[512,64]{0,1:T(8,128)(2,1)S(1)}, bf16[512,64]{0,1:T(8,128)(2,1)}, u32[]{:S(2)}) copy-start(bf16[512,64]{0,1:T(8,128)(2,1)} %param.12) | copy-start | bytes 196612
  2.2 151.4 %copy-start.7 = (bf16[512,256]{1,0:T(8,128)(2,1)S(1)}, bf16[512,256]{1,0:T(8,128)(2,1)}, u32[]{:S(2)}) copy-start(bf16[512,256]{1,0:T(8,128)(2,1)} %param.14) | copy-start | bytes 786436
  2.2 151.5 %copy-start.8 = (bf16[512,256]{1,0:T(8,128)(2,1)S(1)}, bf16[512,256]{1,0:T(8,128)(2,1)}, u32[]{:S(2)}) copy-start(bf16[512,256]{1,0:T(8,128)(2,1)} %param.13) | copy-start | bytes 786436
  100.7 46.1 %collective-permute-start.2 = (bf16[3072,256]{1,0:T(8,128)(2,1)}, bf16[3072,256]{1,0:T(8,128)(2,1)S(1)}, u32[]{:S(2)}, u32[]{:S(2)}) collective-permute-start(bf16[3072,256]{1,0:T(8,128)(2,1)} %get-tuple-element.9.refs_0_), channel_id=1, source_target_pairs={{0,1},{1,2},{2,3},{3,0},{4,5},{5,6},{6,7},{7,4},{8,9},{9,10},{10,1... | collective-permute-start | bytes 4718600 | tf_op jit(solution)/shard_map/ppermute | solution.py:42
  104.8 42.1 %collective-permute-start.3 = (bf16[3072,256]{1,0:T(8,128)(2,1)}, bf16[3072,256]{1,0:T(8,128)(2,1)}, u32[]{:S(2)}, u32[]{:S(2)}) collective-permute-start(bf16[3072,256]{1,0:T(8,128)(2,1)} %get-tuple-element.10.refs_1_), channel_id=1, source_target_pairs={{0,3},{1,0},{2,1},{3,2},{4,7},{5,4},{6,5},{7,6},{8,11},{9,8},{10,9... | collective-permute-start | bytes 4718600 | tf_op jit(solution)/shard_map/ppermute | solution.py:42
  108.1 38.7 %all-to-all-start.1 = ((bf16[32,8,512]{2,1,0:T(8,128)(2,1)}), bf16[32,8,512]{2,1,0:T(8,128)(2,1)S(1)}, u32[]{:S(2)}, u32[]{:S(2)}) async-start(bf16[32,8,512]{2,1,0:T(8,128)(2,1)} %bitcast.59), calls=%async_computation.1 | async-start | bytes 524288 | tf_op jit(solution)/shard_map/all_to_all | solution.py:322
  124.6 47.6 %collective-permute-start.4 = (bf16[3072,256]{1,0:T(8,128)(2,1)}, bf16[3072,256]{1,0:T(8,128)(2,1)}, u32[]{:S(2)}, u32[]{:S(2)}) collective-permute-start(bf16[3072,256]{1,0:T(8,128)(2,1)} %get-tuple-element.10.refs_1_), channel_id=1, source_target_pairs={{0,1},{1,2},{2,3},{3,0},{4,5},{5,6},{6,7},{7,4},{8,9},{9,10},{10,1... | collective-permute-start | bytes 4718600 | tf_op jit(solution)/shard_map/ppermute | solution.py:42
  127.8 44.4 %collective-permute-start.5 = (bf16[3072,256]{1,0:T(8,128)(2,1)}, bf16[3072,256]{1,0:T(8,128)(2,1)}, u32[]{:S(2)}, u32[]{:S(2)}) collective-permute-start(bf16[3072,256]{1,0:T(8,128)(2,1)} %get-tuple-element.9.refs_0_), channel_id=1, source_target_pairs={{0,3},{1,0},{2,1},{3,2},{4,7},{5,4},{6,5},{7,6},{8,11},{9,8},{10,9... | collective-permute-start | bytes 4718600 | tf_op jit(solution)/shard_map/ppermute | solution.py:42
  146.8 8.1 %copy-start.2 = (bf16[3072,256]{1,0:T(8,128)(2,1)}, bf16[3072,256]{1,0:T(8,128)(2,1)S(1)}, u32[]{:S(2)}) copy-start(bf16[3072,256]{1,0:T(8,128)(2,1)S(1)} %collective-permute-done.2.refs_2_) | copy-start | bytes 4718596
  146.8 35.9 %collective-permute-start.6 = (bf16[3072,256]{1,0:T(8,128)(2,1)S(1)}, bf16[3072,256]{1,0:T(8,128)(2,1)}, u32[]{:S(2)}, u32[]{:S(2)}) collective-permute-start(bf16[3072,256]{1,0:T(8,128)(2,1)S(1)} %collective-permute-done.2.refs_2_), channel_id=1, source_target_pairs={{0,1},{1,2},{2,3},{3,0},{4,5},{5,6},{6,7},{7,4},{8,9},{9,10},{10,1... | collective-permute-start | bytes 4718600 | tf_op jit(solution)/shard_map/ppermute | solution.py:42
  150.0 32.7 %collective-permute-start.7 = (bf16[3072,256]{1,0:T(8,128)(2,1)}, bf16[3072,256]{1,0:T(8,128)(2,1)}, u32[]{:S(2)}, u32[]{:S(2)}) collective-permute-start(bf16[3072,256]{1,0:T(8,128)(2,1)} %collective-permute-done.3.refs_5_), channel_id=1, source_target_pairs={{0,3},{1,0},{2,1},{3,2},{4,7},{5,4},{6,5},{7,6},{8,11},{9,8},{10,9... | collective-permute-start | bytes 4718600 | tf_op jit(solution)/shard_map/ppermute | solution.py:42
  154.9 19.1 %all-to-all-start.2 = ((bf16[4,256,512]{2,1,0:T(8,128)(2,1)}), bf16[4,256,512]{2,1,0:T(8,128)(2,1)S(1)}, u32[]{:S(2)}, u32[]{:S(2)}) async-start(bf16[4,256,512]{2,1,0:T(8,128)(2,1)} %broadcast_in_dim.12), calls=%async_computation.2 | async-start | bytes 2097152 | tf_op jit(solution)/shard_map/all_to_all | solution.py:329
  160.5 5.0 %collective-permute-start = (bf16[2,128,1,64]{3,1,2,0:T(8,128)(2,1)S(1)}, bf16[2,128,1,64]{3,1,2,0:T(8,128)(2,1)S(1)}, u32[]{:S(2)}, u32[]{:S(2)}) collective-permute-start(bf16[2,128,1,64]{3,1,2,0:T(8,128)(2,1)S(1)} %get-tuple-element.16), channel_id=1, source_target_pairs={{0,16},{16,32},{32,48},{48,64},{64,80},{80,96},{96,112},{112,128},... | collective-permute-start | bytes 98312 | tf_op jit(solution)/shard_map/ppermute | solution.py:219
  165.5 6.6 %collective-permute-start.1 = (bf16[2,128,1,64]{3,1,2,0:T(8,128)(2,1)S(1)}, bf16[2,128,1,64]{3,1,2,0:T(8,128)(2,1)S(1)}, u32[]{:S(2)}, u32[]{:S(2)}) collective-permute-start(bf16[2,128,1,64]{3,1,2,0:T(8,128)(2,1)S(1)} %get-tuple-element.17), channel_id=1, source_target_pairs={{16,0},{32,16},{48,32},{64,48},{80,64},{96,80},{112,96},{128,112},... | collective-permute-start | bytes 98312 | tf_op jit(solution)/shard_map/ppermute | solution.py:222
  174.1 1.0 copy-start.1
  187.6 3.8 %copy-start.4 = (bf16[512,32]{1,0:T(8,128)(2,1)S(1)}, bf16[512,32]{1,0:T(8,128)(2,1)}, u32[]{:S(2)}) copy-start(bf16[512,32]{1,0:T(8,128)(2,1)} %get-tuple-element.18) | copy-start | bytes 98308
  187.6 3.8 %copy-start.5 = (bf16[512,32]{1,0:T(8,128)(2,1)S(1)}, bf16[512,32]{1,0:T(8,128)(2,1)}, u32[]{:S(2)}) copy-start(bf16[512,32]{1,0:T(8,128)(2,1)} %get-tuple-element.19) | copy-start | bytes 98308
  187.6 19.8 %all-to-all-start.3 = ((bf16[16,256,128]{2,1,0:T(8,128)(2,1)}), bf16[16,256,128]{2,1,0:T(8,128)(2,1)S(1)}, u32[]{:S(2)}, u32[]{:S(2)}) async-start(bf16[16,256,128]{2,1,0:T(8,128)(2,1)} %ffn_last.1), calls=%async_computation.3 | async-start | bytes 2097152 | tf_op jit(solution)/shard_map/all_to_all | solution.py:335
  208.5 18.6 %all-to-all-start = ((bf16[16,512,64]{1,2,0:T(8,128)(2,1)}), bf16[16,512,64]{1,2,0:T(8,128)(2,1)S(1)}, u32[]{:S(2)}, u32[]{:S(2)}) async-start(bf16[16,512,64]{1,2,0:T(8,128)(2,1)} %broadcast_in_dim.11), calls=%async_computation | async-start | bytes 2097152 | tf_op jit(solution)/shard_map/all_to_all | solution.py:228
  212.2 24.6 %copy-start.9 = (f32[256,2]{0,1:T(2,128)S(1)}, f32[256,2]{0,1:T(2,128)}, u32[]{:S(2)}) copy-start(f32[256,2]{0,1:T(2,128)} %param.20) | copy-start | bytes 6148
  227.1 31.9 %all-to-all-start.4 = ((bf16[32,32,128]{2,1,0:T(8,128)(2,1)}), bf16[32,32,128]{2,1,0:T(8,128)(2,1)S(1)}, u32[]{:S(2)}, u32[]{:S(2)}) async-start(bf16[32,32,128]{2,1,0:T(8,128)(2,1)} %copy_bitcast_fusion), calls=%async_computation.4 | async-start | bytes 524288 | tf_op jit(solution)/shard_map/all_to_all | solution.py:338
  259.1 0.7 copy-start.3

commit v2 on v1

--- a/solution.py
+++ b/solution.py
@@ -44,14 +44,14 @@
 
 def prep_kernel(
     x_ref, gain_ref, routes_ref, gate_ref, up_ref, down_ref,
-    out_ref, slot_ref, wa_ref, wb_ref, normed_ref, sems,
+    out_ref, slot_ref, wa_ref, wb_ref, normed_ref, sa_ref, sb_ref, sems,
 ):
     copies = [
-        (gate_ref.at[0], wa_ref.at[pl.ds(0, 2048)]),
-        (up_ref.at[0, pl.ds(0, 1024)], wa_ref.at[pl.ds(2048, 1024)]),
-        (up_ref.at[0, pl.ds(1024, 1024)], wb_ref.at[pl.ds(0, 1024)]),
+        (gate_ref.at[0], sa_ref.at[pl.ds(0, 2048)]),
+        (up_ref.at[0, pl.ds(0, 1024)], sa_ref.at[pl.ds(2048, 1024)]),
+        (up_ref.at[0, pl.ds(1024, 1024)], sb_ref.at[pl.ds(0, 1024)]),
     ] + [
-        (down_ref.at[0, :, pl.ds(c * 256, 256)], wb_ref.at[pl.ds(1024 + c * 256, 256)])
+        (down_ref.at[0, :, pl.ds(c * 256, 256)], sb_ref.at[pl.ds(1024 + c * 256, 256)])
         for c in range(8)
     ]
     copies = [pltpu.make_async_copy(s, d, sems.at[i]) for i, (s, d) in enumerate(copies)]
@@ -66,28 +66,36 @@
         return carry
 
     lax.fori_loop(0, ROWS_B // 32, norm_rows, 0)
-
-    first = routes_ref[:, 0:1]
-    second = routes_ref[:, 1:2]
-    expert = lax.broadcasted_iota(jnp.int32, (ROWS_B, 128), 1)
-    named = jnp.where((first == expert) | (second == expert), 1.0, 0.0)
+    for copy in copies:
+        copy.wait()
+    leave = [
+        pltpu.make_async_copy(sa_ref, wa_ref, sems.at[11]),
+        pltpu.make_async_copy(sb_ref, wb_ref, sems.at[12]),
+    ]
+    for copy in leave:
+        copy.start()
+
+    first = routes_ref[0:1, :]
+    second = routes_ref[1:2, :]
+    expert = lax.broadcasted_iota(jnp.int32, (128, ROWS_B), 0)
     row = lax.broadcasted_iota(jnp.int32, (ROWS_B, ROWS_B), 0)
     col = lax.broadcasted_iota(jnp.int32, (ROWS_B, ROWS_B), 1)
-    below = jnp.where(col < row, 1.0, 0.0).astype(jnp.bfloat16)
     above = jnp.where(row < col, 1.0, 0.0).astype(jnp.bfloat16)
-    rank = jnp.dot(below, named.astype(jnp.bfloat16), preferred_element_type=jnp.float32)
-    rank_a = jnp.sum(jnp.where(first == expert, rank, 0.0), axis=1, keepdims=True)
-    rank_b = jnp.sum(jnp.where(second == expert, rank, 0.0), axis=1, keepdims=True)
+    named = jnp.where((first == expert) | (second == expert), 1.0, 0.0)
+    rank = jnp.dot(named.astype(jnp.bfloat16), above, preferred_element_type=jnp.float32)
+    rank_a = jnp.sum(jnp.where(first == expert, rank, 0.0), axis=0, keepdims=True)
+    rank_b = jnp.sum(jnp.where(second == expert, rank, 0.0), axis=0, keepdims=True)
     slot_a = first * CAP + rank_a.astype(jnp.int32)
     slot_b = second * CAP + rank_b.astype(jnp.int32)
-    pair = lax.broadcasted_iota(jnp.int32, (ROWS_B, 2), 1)
-    slot_ref[...] = jnp.where(pair == 0, slot_a, slot_b)
-
-    named_t = named.T
-    rank_t = jnp.dot(named_t.astype(jnp.bfloat16), above, preferred_element_type=jnp.float32)
-    mark = jnp.where(named_t > 0.5, rank_t, -1.0).astype(jnp.bfloat16)
+    both = jnp.where(expert == 0, slot_a, slot_b).astype(jnp.float32)
+    slot_ref[...] = both.T.astype(jnp.int32)
+
+    mark = jnp.where(named > 0.5, rank, -1.0).astype(jnp.bfloat16)
     spread = jnp.where(
-        (lax.broadcasted_iota(jnp.int32, (ROWS_B, 128), 0) >> 3) == expert, 1.0, 0.0
+        (lax.broadcasted_iota(jnp.int32, (ROWS_B, 128), 0) >> 3)
+        == lax.broadcasted_iota(jnp.int32, (ROWS_B, 128), 1),
+        1.0,
+        0.0,
     ).astype(jnp.bfloat16)
     mark_rows = jnp.dot(spread, mark, preferred_element_type=jnp.float32)
     xi = lax.axis_index("x")
@@ -105,7 +113,7 @@
     )
     even_row = ((lax.broadcasted_iota(jnp.int32, (ROWS_B, 512), 0) >> 3) & 1) == 0
     out_ref[...] = jnp.where(even_row, from_y, from_x).astype(jnp.bfloat16)
-    for copy in copies:
+    for copy in leave:
         copy.wait()
 
 
@@ -115,15 +123,20 @@
         prep_kernel,
         out_shape=(
             jax.ShapeDtypeStruct((ROWS_B, 512), jnp.bfloat16),
-            jax.ShapeDtypeStruct((ROWS_B, 2), jnp.int32),
+            jax.ShapeDtypeStruct((ROWS_B, 128), jnp.int32),
             half,
             half,
         ),
         in_specs=[VMEM, VMEM, VMEM, ANY, ANY, ANY],
         out_specs=(VMEM, VMEM, ANY, ANY),
-        scratch_shapes=[pltpu.VMEM((ROWS_B, D), jnp.bfloat16), pltpu.SemaphoreType.DMA((11,))],
+        scratch_shapes=[
+            pltpu.VMEM((ROWS_B, D), jnp.bfloat16),
+            pltpu.VMEM((HALF_W, 256), jnp.bfloat16),
+            pltpu.VMEM((HALF_W, 256), jnp.bfloat16),
+            pltpu.SemaphoreType.DMA((13,)),
+        ],
         name="prep",
-    )(expert_input, norm_gain.reshape(1, D), routes, gate, up, down)
+    )(expert_input, norm_gain.reshape(1, D), routes.T, gate, up, down)
 
 
 def slice_hidden(x_ref, wa, wb):
@@ -135,14 +148,17 @@
     return (gate / (1.0 + jnp.exp(-gate)) * up).astype(jnp.bfloat16)
 
 
-def ffn_most_kernel(x_ref, *refs):
-    weights, acc_ref, bufs, sems = refs[:6], refs[6], refs[7], refs[8]
+def ffn_kernel(x_ref, attended_ref, *refs):
+    weights, out_ref, acc_ref, bufs, sems = refs[:8], refs[8], refs[9], refs[10], refs[11]
     copies = [
         pltpu.make_async_copy(w, bufs.at[i], sems.at[i]) for i, w in enumerate(weights)
     ]
     for copy in copies:
         copy.start()
-    for s in range(3):
+    core = lax.axis_index("co")
+    for t in range(16):
+        out_ref[t, pl.ds(256, 256), :] = attended_ref[...]
+    for s in range(4):
         copies[2 * s].wait()
         copies[2 * s + 1].wait()
         wa, wb = bufs.at[2 * s], bufs.at[2 * s + 1]
@@ -152,43 +168,30 @@
             term = jnp.dot(
                 hidden, wb[pl.ds(1024 + c * 256, 256), :], preferred_element_type=jnp.float32
             )
-            acc_ref[:, cols] = term if s == 0 else acc_ref[:, cols] + term
-
-
-def ffn_most(x, *weights):
+            total = term if s == 0 else acc_ref[:, cols] + term
+            if s < 3:
+                acc_ref[:, cols] = total
+                continue
+            for k in range(2):
+                t = 2 * c + k
+                place = jnp.where(core == 0, t, (t % 4) * 4 + t // 4)
+                piece = total[:, k * 128 : (k + 1) * 128].astype(jnp.bfloat16)
+                out_ref[place, pl.ds(0, 256), :] = piece
+
+
+def ffn(x, attended, weights):
     return pl.pallas_call(
-        ffn_most_kernel,
-        out_shape=jax.ShapeDtypeStruct((ROWS_B, D), jnp.float32),
-        in_specs=[VMEM] + [ANY] * 6,
+        ffn_kernel,
+        out_shape=jax.ShapeDtypeStruct((16, 512, 128), jnp.bfloat16),
+        in_specs=[VMEM, VMEM] + [ANY] * 8,
         out_specs=VMEM,
         scratch_shapes=[
-            pltpu.VMEM((6, HALF_W, 256), jnp.bfloat16), pltpu.SemaphoreType.DMA((6,))
+            pltpu.VMEM((ROWS_B, D), jnp.float32),
+            pltpu.VMEM((8, HALF_W, 256), jnp.bfloat16),
+            pltpu.SemaphoreType.DMA((8,)),
         ],
-        name="ffn_most",
-    )(x, *weights)
-
-
-def ffn_last_kernel(x_ref, acc_ref, wa_ref, wb_ref, out_ref):
-    core = lax.axis_index("co")
-    hidden = slice_hidden(x_ref, wa_ref, wb_ref)
-    for c in range(8):
-        total = acc_ref[:, pl.ds(c * 256, 256)] + jnp.dot(
-            hidden, wb_ref[pl.ds(1024 + c * 256, 256), :], preferred_element_type=jnp.float32
-        )
-        for k in range(2):
-            t = 2 * c + k
-            place = jnp.where(core == 0, t, (t % 4) * 4 + t // 4)
-            out_ref[place] = total[:, k * 128 : (k + 1) * 128].astype(jnp.bfloat16)
-
-
-def ffn_last(x, acc, wa, wb):
-    return pl.pallas_call(
-        ffn_last_kernel,
-        out_shape=jax.ShapeDtypeStruct((16, ROWS_B, 128), jnp.bfloat16),
-        in_specs=[VMEM] * 4,
-        out_specs=VMEM,
-        name="ffn_last",
-    )(x, acc, wa, wb)
+        name="ffn",
+    )(x, attended, *weights)
 
 
 def combine_kernel(ret_ref, slot_ref, weight_ref, out_ref):
@@ -221,16 +224,6 @@
     )
     high = lax.ppermute(lax.slice_in_dim(block, 0, width, axis=dim), axis, backward)
     return jnp.concatenate([low, block, high], axis=dim)
-
-
-def collect(x, axis, dim):
-    devices = lax.axis_size(axis)
-    blocks = lax.all_to_all(
-        jnp.broadcast_to(x[None], (devices, *x.shape)), axis, 0, 0, tiled=True
-    )
-    dims = list(x.shape)
-    dims[dim] *= devices
-    return jnp.moveaxis(blocks, 0, dim).reshape(dims)
 
 
 def rotate(features, position_start):
@@ -320,26 +313,28 @@
     next_a = line_shift(wa, -1)
     prev_b = line_shift(wb, 1)
     arrived = lax.all_to_all(outgoing, EP, 0, 0, tiled=True)
-    prev_a, next_b, arrived = lax.optimization_barrier((prev_a, next_b, arrived))
     far_a = line_shift(prev_a, 1)
     far_b = line_shift(next_b, -1)
 
     attended = attend(query_proj, key_proj, value_proj, sink_logit)
+    packed = jnp.concatenate([attended[:256], attended[256:]], axis=1)
 
     rows = lax.all_to_all(
         jnp.broadcast_to(arrived[None], (4, *arrived.shape)),
         PLANE, 0, 0, tiled=True, axis_index_groups=LINE_M,
     )
-    acc = ffn_most(rows, wa, wb, prev_a, prev_b, next_a, next_b)
-    partial = ffn_last(rows, acc, far_a, far_b)
+    partial = ffn(rows, packed, (wa, wb, prev_a, prev_b, next_a, next_b, far_a, far_b))
     parts = lax.all_to_all(partial, PLANE, 0, 0, tiled=True, axis_index_groups=WHOLE)
-    result = jnp.sum(parts.reshape(4, 4, EXPERTS, 8, 128).astype(jnp.float32), axis=0)
-    result = jnp.moveaxis(result.astype(jnp.bfloat16), 0, 1).reshape(EXPERTS, CAP, 128)
+    parts = parts.reshape(4, 4, 512, 128)
+    result = jnp.sum(parts[:, :, :256].astype(jnp.float32), axis=0).astype(jnp.bfloat16)
+    result = jnp.moveaxis(result.reshape(4, EXPERTS, 8, 128), 0, 1).reshape(EXPERTS, CAP, 128)
     returned = lax.all_to_all(result, EP, 0, 0, tiled=True)
     expert_out = combine(returned.reshape(EXPERTS * CAP, 128), slots, route_weights)
 
-    gathered = collect(attended, TP, 1)
-    mixer_out = jnp.dot(gathered, out_weight, preferred_element_type=jnp.float32)
+    heads = parts[:, :, 256:]
+    heads = jnp.where(lax.axis_index("co") == 0, heads, jnp.swapaxes(heads, 0, 1))
+    heads = heads.reshape(16, 256, 2, HEAD_DIM).transpose(2, 1, 0, 3).reshape(512, 1024)
+    mixer_out = jnp.dot(heads, out_weight, preferred_element_type=jnp.float32)
     return (mixer_out.astype(jnp.bfloat16), expert_out)
 
 

time: 263 us -> 170 us (0.65)
  Pallas kernels: 113 us -> 16.5 us
  blocking collectives: 0 us -> 32.6 us
  waiting for transfers between devices: 71.6 us -> 43.9 us
    pallas_call x1, Pallas kernels: 98.6 us -> 5.68 us  [prepare(): pl.pallas_call(prep_kernel, out_shape=(jax.ShapeDtypeStruct((ROWS_B, 512)...]
    all_to_all x0 -> x1, blocking collectives: none -> 32.6 us  [local(): lax.all_to_all(partial, PLANE, 0, 0, tiled=True, axis_index_groups=WHOLE)]
    all_to_all x2 -> x0, waiting for transfers between devices: 28.4 us -> none  [the longest x1 14.4 us: local(): lax.all_to_all(partial, PLANE, 0, 0, tiled=True, axis_index_groups=WHOLE)]
    ppermute x6, waiting for transfers between devices: 0.02 us -> 8.17 us  [line_shift(): return lax.ppermute(x, PLANE, pairs)]
    all_to_all x2 -> x0, starting transfers between devices: 7.44 us -> none  [the longest x1 3.78 us: local(): lax.all_to_all(partial, PLANE, 0, 0, tiled=True, axis_index_groups=WHOLE)]
    all_to_all x1, waiting for transfers between devices: 1.85 us -> 8.77 us  [local(): lax.all_to_all(jnp.broadcast_to(arrived[None], (4, *arrived.shape)), PLAN...]
    all_to_all x1, waiting for transfers between devices: 15.7 us -> 9.12 us  [local(): arrived = lax.all_to_all(outgoing, EP, 0, 0, tiled=True)]
    all_to_all x1, starting transfers between devices: 9.68 us -> 15.8 us  [local(): returned = lax.all_to_all(result, EP, 0, 0, tiled=True)]
  transfers between devices with their start and end apart: 13 -> 11, of which waited for: 7 -> 4; matrix products, arithmetic and copies ran while one was open for 3% -> 6% of each run, Pallas kernels for 3% -> 0%
where the time goes in v2:
time: 170 us; the launch traced here: 169 us
  starting transfers between devices  63.7 us (37%)
  waiting for transfers between devices  43.9 us (26%)
  blocking collectives  32.6 us (19%)
  Pallas kernels  16.5 us (10%)
  local copies, waits for them, and re-layouts  5.23 us (3%)
  other arithmetic  2.97 us (2%)
  matrix products  2.49 us (1%)
    all_to_all x1, blocking collectives, local(): lax.all_to_all(partial, PLANE, 0, 0, tiled=True, axis_index_groups=WHOLE)  32.6 us
    ppermute x6, starting transfers between devices, line_shift(): return lax.ppermute(x, PLANE, pairs)  20.4 us
    all_to_all x1, waiting for transfers between devices, local(): returned = lax.all_to_all(result, EP, 0, 0, tiled=True)  17.8 us
    all_to_all x1, starting transfers between devices, local(): returned = lax.all_to_all(result, EP, 0, 0, tiled=True)  15.8 us
    all_to_all x1, starting transfers between devices, local(): arrived = lax.all_to_all(outgoing, EP, 0, 0, tiled=True)  13.8 us
    all_to_all x1, waiting for transfers between devices, local(): arrived = lax.all_to_all(outgoing, EP, 0, 0, tiled=True)  9.12 us
    all_to_all x1, waiting for transfers between devices, local(): lax.all_to_all(jnp.broadcast_to(arrived[None], (4, *arrived.shape)), PLAN...  8.77 us
    pallas_call x1, Pallas kernels, ffn(): pl.pallas_call(ffn_kernel, out_shape=jax.ShapeDtypeStruct((16, 512, 128),...  8.71 us
  transfers between devices with their start and end apart: 11, of which 4 were waited for; matrix products, arithmetic and copies ran while one was open for 6% of the time, Pallas kernels for 0%

profile of v2, /device:TPU:1, one launch (start us, length us, event | category | flops | bytes accessed | tf_op | source)
XLA Modules:
  0.0 169.1 jit_solution(3032584201101936784)
XLA Ops:
  0.6 0.0 copy-start
  0.7 5.7 %prep.1 = (bf16[256,512]{1,0:T(8,128)(2,1)}, s32[256,128]{1,0:T(8,128)}, bf16[3072,256]{1,0:T(8,128)(2,1)}, bf16[3072,256]{1,0:T(8,128)(2,1)}) custom-call(bf16[256,2048]{1,0:T(8,128)(2,1)} %x_ref.1, f32[1,2048]{1,0:T(1,128)} %bitcast.72, s32[2,256]{1,0:T(2,128)} %bitcast.73, bf16[1,2048,256]{2,1,0:T(8,128)(2,1)} %gate_ref.1, bf16[1,2048,256]{2,1,0:T(8,128)(2,1)} %up_ref.1, ...), custom_call_target="tpu_custom_call" | custom-call | tf_op jit(solution)/shard_map/prep/pallas_call | solution.py:122
  6.4 4.0 %collective-permute-start.2 = (bf16[3072,256]{1,0:T(8,128)(2,1)}, bf16[3072,256]{1,0:T(8,128)(2,1)}, u32[]{:S(2)}, u32[]{:S(2)}) collective-permute-start(bf16[3072,256]{1,0:T(8,128)(2,1)} %get-tuple-element.7.refs_0_), channel_id=1, source_target_pairs={{0,1},{1,2},{2,3},{3,0},{4,5},{5,6},{6,7},{7,4},{8,9},{9,10},{10,1... | collective-permute-start | bytes 4718600 | tf_op jit(solution)/shard_map/ppermute | solution.py:42
  10.4 3.4 %collective-permute-start.5 = (bf16[3072,256]{1,0:T(8,128)(2,1)}, bf16[3072,256]{1,0:T(8,128)(2,1)}, u32[]{:S(2)}, u32[]{:S(2)}) collective-permute-start(bf16[3072,256]{1,0:T(8,128)(2,1)} %get-tuple-element.8.refs_1_), channel_id=1, source_target_pairs={{0,3},{1,0},{2,1},{3,2},{4,7},{5,4},{6,5},{7,6},{8,11},{9,8},{10,9... | collective-permute-start | bytes 4718600 | tf_op jit(solution)/shard_map/ppermute | solution.py:42
  13.8 1.9 %collective-permute-start.3 = (bf16[3072,256]{1,0:T(8,128)(2,1)}, bf16[3072,256]{1,0:T(8,128)(2,1)}, u32[]{:S(2)}, u32[]{:S(2)}) collective-permute-start(bf16[3072,256]{1,0:T(8,128)(2,1)} %get-tuple-element.8.refs_1_), channel_id=1, source_target_pairs={{0,1},{1,2},{2,3},{3,0},{4,5},{5,6},{6,7},{7,4},{8,9},{9,10},{10,1... | collective-permute-start | bytes 4718600 | tf_op jit(solution)/shard_map/ppermute | solution.py:42
  15.7 0.0 copy-done.2
  15.7 0.1 copy.24
  15.9 0.1 dynamic-slice_bitcast_fusion
  16.0 0.1 bitcast_convert_fusion
  16.2 1.3 fusion.25
  17.4 0.1 pad_maximum_fusion.3
  17.5 4.9 %collective-permute-start = (bf16[2,128,1,64]{3,1,2,0:T(8,128)(2,1)S(1)}, bf16[2,128,1,64]{3,1,2,0:T(8,128)(2,1)S(1)}, u32[]{:S(2)}, u32[]{:S(2)}) collective-permute-start(bf16[2,128,1,64]{3,1,2,0:T(8,128)(2,1)S(1)} %get-tuple-element.12), channel_id=1, source_target_pairs={{0,16},{16,32},{32,48},{48,64},{64,80},{80,96},{96,112},{112,128},... | collective-permute-start | bytes 98312 | tf_op jit(solution)/shard_map/ppermute | solution.py:222
  22.4 4.8 %collective-permute-start.1 = (bf16[2,128,1,64]{3,1,2,0:T(8,128)(2,1)S(1)}, bf16[2,128,1,64]{3,1,2,0:T(8,128)(2,1)S(1)}, u32[]{:S(2)}, u32[]{:S(2)}) collective-permute-start(bf16[2,128,1,64]{3,1,2,0:T(8,128)(2,1)S(1)} %get-tuple-element.13), channel_id=1, source_target_pairs={{16,0},{32,16},{48,32},{64,48},{80,64},{96,80},{112,96},{128,112},... | collective-permute-start | bytes 98312 | tf_op jit(solution)/shard_map/ppermute | solution.py:225
  27.3 13.8 %all-to-all-start = ((bf16[32,8,512]{2,1,0:T(8,128)(2,1)}), bf16[32,8,512]{2,1,0:T(8,128)(2,1)S(1)}, u32[]{:S(2)}, u32[]{:S(2)}) async-start(bf16[32,8,512]{2,1,0:T(8,128)(2,1)} %bitcast.2), calls=%async_computation | async-start | bytes 524288 | tf_op jit(solution)/shard_map/all_to_all | solution.py:315
  41.7 0.0 collective-permute-done
  41.7 4.6 %collective-permute-start.4 = (bf16[3072,256]{1,0:T(8,128)(2,1)}, bf16[3072,256]{1,0:T(8,128)(2,1)}, u32[]{:S(2)}, u32[]{:S(2)}) collective-permute-start(bf16[3072,256]{1,0:T(8,128)(2,1)} %get-tuple-element.7.refs_0_), channel_id=1, source_target_pairs={{0,3},{1,0},{2,1},{3,2},{4,7},{5,4},{6,5},{7,6},{8,11},{9,8},{10,9... | collective-permute-start | bytes 4718600 | tf_op jit(solution)/shard_map/ppermute | solution.py:42
  46.4 0.0 collective-permute-done.2.refs_2_
  46.4 1.9 %collective-permute-start.6 = (bf16[3072,256]{1,0:T(8,128)(2,1)}, bf16[3072,256]{1,0:T(8,128)(2,1)}, u32[]{:S(2)}, u32[]{:S(2)}) collective-permute-start(bf16[3072,256]{1,0:T(8,128)(2,1)} %collective-permute-done.2.refs_2_), channel_id=1, source_target_pairs={{0,1},{1,2},{2,3},{3,0},{4,5},{5,6},{6,7},{7,4},{8,9},{9,10},{10,1... | collective-permute-start | bytes 4718600 | tf_op jit(solution)/shard_map/ppermute | solution.py:42
  48.3 0.0 collective-permute-done.5.refs_5_
  48.3 4.6 %collective-permute-start.7 = (bf16[3072,256]{1,0:T(8,128)(2,1)}, bf16[3072,256]{1,0:T(8,128)(2,1)}, u32[]{:S(2)}, u32[]{:S(2)}) collective-permute-start(bf16[3072,256]{1,0:T(8,128)(2,1)} %collective-permute-done.5.refs_5_), channel_id=1, source_target_pairs={{0,3},{1,0},{2,1},{3,2},{4,7},{5,4},{6,5},{7,6},{8,11},{9,8},{10,9... | collective-permute-start | bytes 4718600 | tf_op jit(solution)/shard_map/ppermute | solution.py:42
  52.9 0.0 collective-permute-done.1
  52.9 0.1 pad_maximum_fusion
  53.0 0.8 fusion.29
  53.9 0.3 fusion.2
  54.2 9.1 %all-to-all-done = bf16[32,8,512]{2,1,0:T(8,128)(2,1)S(1)} async-done(((bf16[32,8,512]{2,1,0:T(8,128)(2,1)}), bf16[32,8,512]{2,1,0:T(8,128)(2,1)S(1)}, u32[]{:S(2)}, u32[]{:S(2)}) %all-to-all-start) | async-done | bytes 262176 | tf_op jit(solution)/shard_map/all_to_all | solution.py:315
  63.3 1.1 broadcast_in_dim.8
  64.3 3.9 %all-to-all-start.1 = ((bf16[4,256,512]{2,1,0:T(8,128)(2,1)}), bf16[4,256,512]{2,1,0:T(8,128)(2,1)S(1)}, u32[]{:S(2)}, u32[]{:S(2)}) async-start(bf16[4,256,512]{2,1,0:T(8,128)(2,1)} %broadcast_in_dim.8), calls=%async_computation.1 | async-start | bytes 2097152 | tf_op jit(solution)/shard_map/all_to_all | solution.py:322
  68.3 0.5 fusion.3
  68.8 0.7 pad_maximum_fusion.4.attended_ref
  69.6 0.0 collective-permute-done.3.refs_3_
  69.6 0.0 collective-permute-done.4.refs_4_
  69.6 8.8 %all-to-all-done.1.x_ref = bf16[4,256,512]{2,1,0:T(8,128)(2,1)S(1)} async-done(((bf16[4,256,512]{2,1,0:T(8,128)(2,1)}), bf16[4,256,512]{2,1,0:T(8,128)(2,1)S(1)}, u32[]{:S(2)}, u32[]{:S(2)}) %all-to-all-start.1) | async-done | bytes 1048608 | tf_op jit(solution)/shard_map/all_to_all | solution.py:322
  78.3 0.0 collective-permute-done.6.refs_6_
  78.3 8.2 %collective-permute-done.7.refs_7_ = bf16[3072,256]{1,0:T(8,128)(2,1)} collective-permute-done((bf16[3072,256]{1,0:T(8,128)(2,1)}, bf16[3072,256]{1,0:T(8,128)(2,1)}, u32[]{:S(2)}, u32[]{:S(2)}) %collective-permute-start.7) | collective-permute-done | bytes 1572896 | tf_op jit(solution)/shard_map/ppermute | solution.py:42
  86.5 8.7 %ffn.1 = bf16[16,512,128]{2,1,0:T(8,128)(2,1)} custom-call(bf16[4,256,512]{2,1,0:T(8,128)(2,1)} %copy-done.1, bf16[256,128]{1,0:T(8,128)(2,1)} %pad_maximum_fusion.4.attended_ref, bf16[3072,256]{1,0:T(8,128)(2,1)} %get-tuple-element.7.refs_0_, bf16[3072,256]{1,0:T(8,128)(2,1)} %get-tuple-element.8.refs_1_, bf16[3072,256]{1,0:T(8,128)(2,1)} %collective-permute-done.2.refs_2_, ...), custom_call_target="tpu_custom_call" | custom-call | tf_op jit(solution)/shard_map/ffn/pallas_call | solution.py:183
  95.2 32.6 %all_to_all.24 = bf16[16,512,128]{2,1,0:T(8,128)(2,1)S(1)} all-to-all(bf16[16,512,128]{2,1,0:T(8,128)(2,1)} %ffn.1), channel_id=1, replica_groups={{0,1,2,3,4,5,6,7,8,9,10,11,12,13,14,15},{16,20,24,28,17,21,25,29,18,22,..., dimensions={0} | all-to-all | bytes 4194304 | tf_op jit(solution)/shard_map/all_to_all | solution.py:327
  127.9 0.2 slice_reduce_fusion
  128.0 0.7 copy_bitcast_fusion
  128.8 15.8 %all-to-all-start.3 = ((bf16[32,32,128]{2,1,0:T(8,128)(2,1)}), bf16[32,32,128]{2,1,0:T(8,128)(2,1)}, u32[]{:S(2)}, u32[]{:S(2)}) async-start(bf16[32,32,128]{2,1,0:T(8,128)(2,1)} %copy_bitcast_fusion), calls=%async_computation.3 | async-start | bytes 524288 | tf_op jit(solution)/shard_map/all_to_all | solution.py:331
  144.6 0.8 copy.30.weight_ref
  145.4 0.5 copy.27
  146.0 0.5 copy.32
  146.5 0.1 bitcast_select_fusion.1
  146.6 1.1 copy.28
  147.7 0.2 copy.34
  148.0 1.1 convolution_convert_fusion.1
  149.1 17.8 %all-to-all-done.3 = bf16[32,32,128]{2,1,0:T(8,128)(2,1)} async-done(((bf16[32,32,128]{2,1,0:T(8,128)(2,1)}), bf16[32,32,128]{2,1,0:T(8,128)(2,1)}, u32[]{:S(2)}, u32[]{:S(2)}) %all-to-all-start.3) | async-done | bytes 262176 | tf_op jit(solution)/shard_map/all_to_all | solution.py:331
  166.9 2.2 %combine.1 = bf16[256,128]{1,0:T(8,128)(2,1)} custom-call(bf16[1024,128]{1,0:T(8,128)(2,1)} %bitcast.31.ret_ref, s32[256,128]{1,0:T(8,128)} %get-tuple-element.9.slot_ref, f32[256,2]{1,0:T(8,128)} %copy.30.weight_ref), custom_call_target="tpu_custom_call" | custom-call | tf_op jit(solution)/shard_map/combine/pallas_call | solution.py:209
  (17 shorter events, 0.1 us)
Async XLA Ops:
  0.6 147.3 %copy-start = (bf16[1024,128]{1,0:T(8,128)(2,1)S(1)}, bf16[1024,128]{1,0:T(8,128)(2,1)}, u32[]{:S(2)}) copy-start(bf16[1024,128]{1,0:T(8,128)(2,1)} %param.16) | copy-start | bytes 786436
  0.6 15.1 %copy-start.2 = (bf16[512,64]{0,1:T(8,128)(2,1)S(1)}, bf16[512,64]{0,1:T(8,128)(2,1)}, u32[]{:S(2)}) copy-start(bf16[512,64]{0,1:T(8,128)(2,1)} %param.12) | copy-start | bytes 196612
  0.7 15.2 %copy-start.3 = (bf16[512,256]{1,0:T(8,128)(2,1)S(1)}, bf16[512,256]{1,0:T(8,128)(2,1)}, u32[]{:S(2)}) copy-start(bf16[512,256]{1,0:T(8,128)(2,1)} %param.14) | copy-start | bytes 786436
  0.7 15.4 %copy-start.4 = (bf16[512,256]{1,0:T(8,128)(2,1)S(1)}, bf16[512,256]{1,0:T(8,128)(2,1)}, u32[]{:S(2)}) copy-start(bf16[512,256]{1,0:T(8,128)(2,1)} %param.13) | copy-start | bytes 786436
  6.4 40.0 %collective-permute-start.2 = (bf16[3072,256]{1,0:T(8,128)(2,1)}, bf16[3072,256]{1,0:T(8,128)(2,1)}, u32[]{:S(2)}, u32[]{:S(2)}) collective-permute-start(bf16[3072,256]{1,0:T(8,128)(2,1)} %get-tuple-element.7.refs_0_), channel_id=1, source_target_pairs={{0,1},{1,2},{2,3},{3,0},{4,5},{5,6},{6,7},{7,4},{8,9},{9,10},{10,1... | collective-permute-start | bytes 4718600 | tf_op jit(solution)/shard_map/ppermute | solution.py:42
  10.4 37.9 %collective-permute-start.5 = (bf16[3072,256]{1,0:T(8,128)(2,1)}, bf16[3072,256]{1,0:T(8,128)(2,1)}, u32[]{:S(2)}, u32[]{:S(2)}) collective-permute-start(bf16[3072,256]{1,0:T(8,128)(2,1)} %get-tuple-element.8.refs_1_), channel_id=1, source_target_pairs={{0,3},{1,0},{2,1},{3,2},{4,7},{5,4},{6,5},{7,6},{8,11},{9,8},{10,9... | collective-permute-start | bytes 4718600 | tf_op jit(solution)/shard_map/ppermute | solution.py:42
  13.8 55.8 %collective-permute-start.3 = (bf16[3072,256]{1,0:T(8,128)(2,1)}, bf16[3072,256]{1,0:T(8,128)(2,1)}, u32[]{:S(2)}, u32[]{:S(2)}) collective-permute-start(bf16[3072,256]{1,0:T(8,128)(2,1)} %get-tuple-element.8.refs_1_), channel_id=1, source_target_pairs={{0,1},{1,2},{2,3},{3,0},{4,5},{5,6},{6,7},{7,4},{8,9},{9,10},{10,1... | collective-permute-start | bytes 4718600 | tf_op jit(solution)/shard_map/ppermute | solution.py:42
  17.5 24.2 %collective-permute-start = (bf16[2,128,1,64]{3,1,2,0:T(8,128)(2,1)S(1)}, bf16[2,128,1,64]{3,1,2,0:T(8,128)(2,1)S(1)}, u32[]{:S(2)}, u32[]{:S(2)}) collective-permute-start(bf16[2,128,1,64]{3,1,2,0:T(8,128)(2,1)S(1)} %get-tuple-element.12), channel_id=1, source_target_pairs={{0,16},{16,32},{32,48},{48,64},{64,80},{80,96},{96,112},{112,128},... | collective-permute-start | bytes 98312 | tf_op jit(solution)/shard_map/ppermute | solution.py:222
  22.4 30.5 %collective-permute-start.1 = (bf16[2,128,1,64]{3,1,2,0:T(8,128)(2,1)S(1)}, bf16[2,128,1,64]{3,1,2,0:T(8,128)(2,1)S(1)}, u32[]{:S(2)}, u32[]{:S(2)}) collective-permute-start(bf16[2,128,1,64]{3,1,2,0:T(8,128)(2,1)S(1)} %get-tuple-element.13), channel_id=1, source_target_pairs={{16,0},{32,16},{48,32},{64,48},{80,64},{96,80},{112,96},{128,112},... | collective-permute-start | bytes 98312 | tf_op jit(solution)/shard_map/ppermute | solution.py:225
  27.3 36.0 %all-to-all-start = ((bf16[32,8,512]{2,1,0:T(8,128)(2,1)}), bf16[32,8,512]{2,1,0:T(8,128)(2,1)S(1)}, u32[]{:S(2)}, u32[]{:S(2)}) async-start(bf16[32,8,512]{2,1,0:T(8,128)(2,1)} %bitcast.2), calls=%async_computation | async-start | bytes 524288 | tf_op jit(solution)/shard_map/all_to_all | solution.py:315
  41.7 27.8 %collective-permute-start.4 = (bf16[3072,256]{1,0:T(8,128)(2,1)}, bf16[3072,256]{1,0:T(8,128)(2,1)}, u32[]{:S(2)}, u32[]{:S(2)}) collective-permute-start(bf16[3072,256]{1,0:T(8,128)(2,1)} %get-tuple-element.7.refs_0_), channel_id=1, source_target_pairs={{0,3},{1,0},{2,1},{3,2},{4,7},{5,4},{6,5},{7,6},{8,11},{9,8},{10,9... | collective-permute-start | bytes 4718600 | tf_op jit(solution)/shard_map/ppermute | solution.py:42
  46.4 32.0 %collective-permute-start.6 = (bf16[3072,256]{1,0:T(8,128)(2,1)}, bf16[3072,256]{1,0:T(8,128)(2,1)}, u32[]{:S(2)}, u32[]{:S(2)}) collective-permute-start(bf16[3072,256]{1,0:T(8,128)(2,1)} %collective-permute-done.2.refs_2_), channel_id=1, source_target_pairs={{0,1},{1,2},{2,3},{3,0},{4,5},{5,6},{6,7},{7,4},{8,9},{9,10},{10,1... | collective-permute-start | bytes 4718600 | tf_op jit(solution)/shard_map/ppermute | solution.py:42
  48.3 38.2 %collective-permute-start.7 = (bf16[3072,256]{1,0:T(8,128)(2,1)}, bf16[3072,256]{1,0:T(8,128)(2,1)}, u32[]{:S(2)}, u32[]{:S(2)}) collective-permute-start(bf16[3072,256]{1,0:T(8,128)(2,1)} %collective-permute-done.5.refs_5_), channel_id=1, source_target_pairs={{0,3},{1,0},{2,1},{3,2},{4,7},{5,4},{6,5},{7,6},{8,11},{9,8},{10,9... | collective-permute-start | bytes 4718600 | tf_op jit(solution)/shard_map/ppermute | solution.py:42
  64.3 14.0 %all-to-all-start.1 = ((bf16[4,256,512]{2,1,0:T(8,128)(2,1)}), bf16[4,256,512]{2,1,0:T(8,128)(2,1)S(1)}, u32[]{:S(2)}, u32[]{:S(2)}) async-start(bf16[4,256,512]{2,1,0:T(8,128)(2,1)} %broadcast_in_dim.8), calls=%async_computation.1 | async-start | bytes 2097152 | tf_op jit(solution)/shard_map/all_to_all | solution.py:322
  78.3 8.2 %copy-start.1 = (bf16[4,256,512]{2,1,0:T(8,128)(2,1)}, bf16[4,256,512]{2,1,0:T(8,128)(2,1)S(1)}, u32[]{:S(2)}) copy-start(bf16[4,256,512]{2,1,0:T(8,128)(2,1)S(1)} %all-to-all-done.1.x_ref) | copy-start | bytes 3145732
  127.9 16.8 %copy-start.5 = (f32[256,2]{0,1:T(2,128)S(1)}, f32[256,2]{0,1:T(2,128)}, u32[]{:S(2)}) copy-start(f32[256,2]{0,1:T(2,128)} %param.20) | copy-start | bytes 6148
  128.8 38.1 %all-to-all-start.3 = ((bf16[32,32,128]{2,1,0:T(8,128)(2,1)}), bf16[32,32,128]{2,1,0:T(8,128)(2,1)}, u32[]{:S(2)}, u32[]{:S(2)}) async-start(bf16[32,32,128]{2,1,0:T(8,128)(2,1)} %copy_bitcast_fusion), calls=%async_computation.3 | async-start | bytes 524288 | tf_op jit(solution)/shard_map/all_to_all | solution.py:331

commit v3 on v2

--- a/solution.py
+++ b/solution.py
@@ -1,5 +1,3 @@
-import functools
-
 import jax
 import jax.numpy as jnp
 from jax import lax
@@ -7,6 +5,7 @@
 from jax.experimental.pallas import tpu as pltpu
 from jax.sharding import Mesh
 from jax.sharding import PartitionSpec as P
+
 
 D = 2048
 HEADS = 16
@@ -141,14 +140,17 @@
 
 def slice_hidden(x_ref, wa, wb):
     def part(m, ref, start):
-        return jnp.dot(x_ref[m], ref[pl.ds(start, 512), :], preferred_element_type=jnp.float32)
+        return jnp.dot(
+            x_ref[m, pl.ds(0, ROWS_B), :], ref[pl.ds(start, 512), :],
+            preferred_element_type=jnp.float32,
+        )
 
     gate = part(0, wa, 0) + part(1, wa, 512) + part(2, wa, 1024) + part(3, wa, 1536)
     up = part(0, wa, 2048) + part(1, wa, 2560) + part(2, wb, 0) + part(3, wb, 512)
     return (gate / (1.0 + jnp.exp(-gate)) * up).astype(jnp.bfloat16)
 
 
-def ffn_kernel(x_ref, attended_ref, *refs):
+def ffn_kernel(x_ref, *refs):
     weights, out_ref, acc_ref, bufs, sems = refs[:8], refs[8], refs[9], refs[10], refs[11]
     copies = [
         pltpu.make_async_copy(w, bufs.at[i], sems.at[i]) for i, w in enumerate(weights)
@@ -156,8 +158,6 @@
     for copy in copies:
         copy.start()
     core = lax.axis_index("co")
-    for t in range(16):
-        out_ref[t, pl.ds(256, 256), :] = attended_ref[...]
     for s in range(4):
         copies[2 * s].wait()
         copies[2 * s + 1].wait()
@@ -176,14 +176,14 @@
                 t = 2 * c + k
                 place = jnp.where(core == 0, t, (t % 4) * 4 + t // 4)
                 piece = total[:, k * 128 : (k + 1) * 128].astype(jnp.bfloat16)
-                out_ref[place, pl.ds(0, 256), :] = piece
-
-
-def ffn(x, attended, weights):
+                out_ref[place] = piece
+
+
+def ffn(x, weights):
     return pl.pallas_call(
         ffn_kernel,
-        out_shape=jax.ShapeDtypeStruct((16, 512, 128), jnp.bfloat16),
-        in_specs=[VMEM, VMEM] + [ANY] * 8,
+        out_shape=jax.ShapeDtypeStruct((16, ROWS_B, 128), jnp.bfloat16),
+        in_specs=[VMEM] + [ANY] * 8,
         out_specs=VMEM,
         scratch_shapes=[
             pltpu.VMEM((ROWS_B, D), jnp.float32),
@@ -191,7 +191,7 @@
             pltpu.SemaphoreType.DMA((8,)),
         ],
         name="ffn",
-    )(x, attended, *weights)
+    )(x, *weights)
 
 
 def combine_kernel(ret_ref, slot_ref, weight_ref, out_ref):
@@ -213,6 +213,38 @@
         out_specs=VMEM,
         name="combine",
     )(returned, slots, route_weights)
+
+
+def project_kernel(own_ref, prev_ref, next_ref, far_ref, weight_ref, out_ref, a_ref, w_ref):
+    core = lax.axis_index("co")
+    line = jnp.where(core == 0, lax.axis_index("x"), lax.axis_index("y"))
+    w_ref[...] = jnp.zeros_like(w_ref)
+    for j, (ref, step) in enumerate(((own_ref, 0), (prev_ref, 3), (next_ref, 1), (far_ref, 2))):
+        source = lax.rem(line + step, 4)
+        for m in range(4):
+            head = jnp.where(core == 0, m * 4 + source, source * 4 + m)
+            at = (4 * j + m) * 128
+            weight = weight_ref[pl.ds(pl.multiple_of(head * HEAD_DIM, HEAD_DIM), HEAD_DIM), :]
+            w_ref[pl.ds(at, 64), pl.ds(0, 128)] = weight
+            w_ref[pl.ds(at + 64, 64), pl.ds(128, 128)] = weight
+            for q in range(4):
+                a_ref[pl.ds(q * 64, 64), pl.ds(at, 128)] = ref[m, :, pl.ds(q * 128, 128)]
+    both = jnp.dot(a_ref[...], w_ref[...], preferred_element_type=jnp.float32)
+    out_ref[pl.ds(0, 256), :] = both[:, :128].astype(jnp.bfloat16)
+    out_ref[pl.ds(256, 256), :] = both[:, 128:].astype(jnp.bfloat16)
+
+
+def project(own, prev, nxt, far, out_weight):
+    return pl.pallas_call(
+        project_kernel,
+        out_shape=jax.ShapeDtypeStruct((512, 128), jnp.bfloat16),
+        in_specs=[VMEM] * 5,
+        out_specs=VMEM,
+        scratch_shapes=[
+            pltpu.VMEM((256, 2048), jnp.bfloat16), pltpu.VMEM((2048, 256), jnp.bfloat16)
+        ],
+        name="project",
+    )(own, prev, nxt, far, out_weight)
 
 
 def padded(block, axis, dim, width):
@@ -318,24 +350,26 @@
 
     attended = attend(query_proj, key_proj, value_proj, sink_logit)
     packed = jnp.concatenate([attended[:256], attended[256:]], axis=1)
-
+    packed = jnp.concatenate([packed[q * 64 : (q + 1) * 64] for q in range(4)], axis=1)
+
+    payload = jnp.concatenate([arrived, packed], axis=0)
     rows = lax.all_to_all(
-        jnp.broadcast_to(arrived[None], (4, *arrived.shape)),
+        jnp.broadcast_to(payload[None], (4, *payload.shape)),
         PLANE, 0, 0, tiled=True, axis_index_groups=LINE_M,
     )
-    partial = ffn(rows, packed, (wa, wb, prev_a, prev_b, next_a, next_b, far_a, far_b))
+    partial = ffn(rows, (wa, wb, prev_a, prev_b, next_a, next_b, far_a, far_b))
     parts = lax.all_to_all(partial, PLANE, 0, 0, tiled=True, axis_index_groups=WHOLE)
-    parts = parts.reshape(4, 4, 512, 128)
-    result = jnp.sum(parts[:, :, :256].astype(jnp.float32), axis=0).astype(jnp.bfloat16)
-    result = jnp.moveaxis(result.reshape(4, EXPERTS, 8, 128), 0, 1).reshape(EXPERTS, CAP, 128)
+    parts = parts.reshape(4, 4, 256, 128)
+    result = jnp.sum(parts.astype(jnp.float32), axis=0).astype(jnp.bfloat16)
+    result = jnp.moveaxis(result.reshape(4, EXPERTS, 8, 128), 0, 1)
+    result = result.reshape(EXPERTS, CAP, 128)
     returned = lax.all_to_all(result, EP, 0, 0, tiled=True)
     expert_out = combine(returned.reshape(EXPERTS * CAP, 128), slots, route_weights)
 
-    heads = parts[:, :, 256:]
-    heads = jnp.where(lax.axis_index("co") == 0, heads, jnp.swapaxes(heads, 0, 1))
-    heads = heads.reshape(16, 256, 2, HEAD_DIM).transpose(2, 1, 0, 3).reshape(512, 1024)
-    mixer_out = jnp.dot(heads, out_weight, preferred_element_type=jnp.float32)
-    return (mixer_out.astype(jnp.bfloat16), expert_out)
+    heads = rows[:, 256:]
+    around = [line_shift(heads, step) for step in (1, -1, 2)]
+    mixer_out = project(heads, *around, out_weight)
+    return (mixer_out, expert_out)
 
 
 def solution(mesh):

time: 170 us -> 161 us (0.947)
  blocking collectives: 32.6 us -> 24.5 us
  waiting for transfers between devices: 43.9 us -> 37.7 us
  starting transfers between devices: 63.7 us -> 68.3 us
  Pallas kernels: 16.5 us -> 18.7 us
    all_to_all x1, waiting for transfers between devices: 17.8 us -> 2.62 us  [local(): returned = lax.all_to_all(result, EP, 0, 0, tiled=True)]
    all_to_all x1, blocking collectives: 32.6 us -> 24.5 us  [local(): lax.all_to_all(partial, PLANE, 0, 0, tiled=True, axis_index_groups=WHOLE)]
    ppermute x6 -> x9, starting transfers between devices: 20.4 us -> 26.6 us  [line_shift(): return lax.ppermute(x, PLANE, pairs)]
    all_to_all x1, waiting for transfers between devices: 8.77 us -> 14.8 us  [local(): lax.all_to_all(jnp.broadcast_to(payload[None], (4, *payload.shape)), PLAN...]
    ppermute x6 -> x9, waiting for transfers between devices: 8.17 us -> 11.3 us  [line_shift(): return lax.ppermute(x, PLANE, pairs)]
    all_to_all x1, starting transfers between devices: 15.8 us -> 13.3 us  [local(): returned = lax.all_to_all(result, EP, 0, 0, tiled=True)]
    pallas_call x1 -> x2, Pallas kernels: 8.71 us -> 10.9 us  [the longest x1 8.42 us: ffn(): pl.pallas_call(ffn_kernel, out_shape=jax.ShapeDtypeStruct((16, ROWS_B, 12...]
  transfers between devices with their start and end apart: 11 -> 14, of which waited for: 4 -> 7; matrix products, arithmetic and copies ran while one was open for 6% -> 4% of each run, Pallas kernels for 0% -> 2%
where the time goes in v3:
time: 161 us; the launch traced here: 160 us
  starting transfers between devices  68.3 us (42%)
  waiting for transfers between devices  37.7 us (23%)
  blocking collectives  24.5 us (15%)
  Pallas kernels  18.7 us (12%)
  local copies, waits for them, and re-layouts  5.44 us (3%)
  other arithmetic  2.36 us (1%)
  between operations  1.66 us (1%)
    ppermute x9, starting transfers between devices, line_shift(): return lax.ppermute(x, PLANE, pairs)  26.6 us
    all_to_all x1, blocking collectives, local(): lax.all_to_all(partial, PLANE, 0, 0, tiled=True, axis_index_groups=WHOLE)  24.5 us
    all_to_all x1, starting transfers between devices, local(): arrived = lax.all_to_all(outgoing, EP, 0, 0, tiled=True)  15 us
    all_to_all x1, waiting for transfers between devices, local(): lax.all_to_all(jnp.broadcast_to(payload[None], (4, *payload.shape)), PLAN...  14.8 us
    all_to_all x1, starting transfers between devices, local(): returned = lax.all_to_all(result, EP, 0, 0, tiled=True)  13.3 us
    ppermute x9, waiting for transfers between devices, line_shift(): return lax.ppermute(x, PLANE, pairs)  11.3 us
    all_to_all x1, waiting for transfers between devices, local(): arrived = lax.all_to_all(outgoing, EP, 0, 0, tiled=True)  9.02 us
    pallas_call x1, Pallas kernels, ffn(): pl.pallas_call(ffn_kernel, out_shape=jax.ShapeDtypeStruct((16, ROWS_B, 12...  8.42 us
  transfers between devices with their start and end apart: 14, of which 7 were waited for; matrix products, arithmetic and copies ran while one was open for 4% of the time, Pallas kernels for 2%

profile of v3, /device:TPU:1, one launch (start us, length us, event | category | flops | bytes accessed | tf_op | source)
XLA Modules:
  0.0 159.9 jit_solution(13975888754052538146)
XLA Ops:
  0.6 0.0 copy-start
  0.7 5.6 %prep.1 = (bf16[256,512]{1,0:T(8,128)(2,1)}, s32[256,128]{1,0:T(8,128)}, bf16[3072,256]{1,0:T(8,128)(2,1)}, bf16[3072,256]{1,0:T(8,128)(2,1)}) custom-call(bf16[256,2048]{1,0:T(8,128)(2,1)} %x_ref.1, f32[1,2048]{1,0:T(1,128)} %bitcast.58, s32[2,256]{1,0:T(2,128)} %bitcast.59, bf16[1,2048,256]{2,1,0:T(8,128)(2,1)} %gate_ref.1, bf16[1,2048,256]{2,1,0:T(8,128)(2,1)} %up_ref.1, ...), custom_call_target="tpu_custom_call" | custom-call | tf_op jit(solution)/shard_map/prep/pallas_call | solution.py:121
  6.3 5.5 %collective-permute-start.8 = (bf16[3072,256]{1,0:T(8,128)(2,1)}, bf16[3072,256]{1,0:T(8,128)(2,1)}, u32[]{:S(2)}, u32[]{:S(2)}) collective-permute-start(bf16[3072,256]{1,0:T(8,128)(2,1)} %get-tuple-element.8.refs_1_), channel_id=1, source_target_pairs={{0,3},{1,0},{2,1},{3,2},{4,7},{5,4},{6,5},{7,6},{8,11},{9,8},{10,9... | collective-permute-start | bytes 4718600 | tf_op jit(solution)/shard_map/ppermute | solution.py:41
  11.8 1.9 %collective-permute-start.6 = (bf16[3072,256]{1,0:T(8,128)(2,1)}, bf16[3072,256]{1,0:T(8,128)(2,1)}, u32[]{:S(2)}, u32[]{:S(2)}) collective-permute-start(bf16[3072,256]{1,0:T(8,128)(2,1)} %get-tuple-element.8.refs_1_), channel_id=1, source_target_pairs={{0,1},{1,2},{2,3},{3,0},{4,5},{5,6},{6,7},{7,4},{8,9},{9,10},{10,1... | collective-permute-start | bytes 4718600 | tf_op jit(solution)/shard_map/ppermute | solution.py:41
  13.7 1.9 %collective-permute-start.5 = (bf16[3072,256]{1,0:T(8,128)(2,1)}, bf16[3072,256]{1,0:T(8,128)(2,1)}, u32[]{:S(2)}, u32[]{:S(2)}) collective-permute-start(bf16[3072,256]{1,0:T(8,128)(2,1)} %get-tuple-element.7.refs_0_), channel_id=1, source_target_pairs={{0,1},{1,2},{2,3},{3,0},{4,5},{5,6},{6,7},{7,4},{8,9},{9,10},{10,1... | collective-permute-start | bytes 4718600 | tf_op jit(solution)/shard_map/ppermute | solution.py:41
  15.7 0.1 copy.20
  15.8 0.1 dynamic-slice_bitcast_fusion
  16.0 0.1 bitcast_convert_fusion
  16.1 1.3 fusion.26
  17.4 0.1 pad_maximum_fusion.5
  17.5 4.9 %collective-permute-start = (bf16[2,128,1,64]{3,1,2,0:T(8,128)(2,1)S(1)}, bf16[2,128,1,64]{3,1,2,0:T(8,128)(2,1)S(1)}, u32[]{:S(2)}, u32[]{:S(2)}) collective-permute-start(bf16[2,128,1,64]{3,1,2,0:T(8,128)(2,1)S(1)} %get-tuple-element.10), channel_id=1, source_target_pairs={{0,16},{16,32},{32,48},{48,64},{64,80},{80,96},{96,112},{112,128},... | collective-permute-start | bytes 98312 | tf_op jit(solution)/shard_map/ppermute | solution.py:254
  22.4 3.6 %collective-permute-start.1 = (bf16[2,128,1,64]{3,1,2,0:T(8,128)(2,1)S(1)}, bf16[2,128,1,64]{3,1,2,0:T(8,128)(2,1)S(1)}, u32[]{:S(2)}, u32[]{:S(2)}) collective-permute-start(bf16[2,128,1,64]{3,1,2,0:T(8,128)(2,1)S(1)} %get-tuple-element.11), channel_id=1, source_target_pairs={{16,0},{32,16},{48,32},{64,48},{80,64},{96,80},{112,96},{128,112},... | collective-permute-start | bytes 98312 | tf_op jit(solution)/shard_map/ppermute | solution.py:257
  26.0 15.0 %all-to-all-start = ((bf16[32,8,512]{2,1,0:T(8,128)(2,1)}), bf16[32,8,512]{2,1,0:T(8,128)(2,1)S(1)}, u32[]{:S(2)}, u32[]{:S(2)}) async-start(bf16[32,8,512]{2,1,0:T(8,128)(2,1)} %bitcast.2), calls=%async_computation | async-start | bytes 524288 | tf_op jit(solution)/shard_map/all_to_all | solution.py:347
  41.7 4.6 %collective-permute-start.7 = (bf16[3072,256]{1,0:T(8,128)(2,1)S(1)}, bf16[3072,256]{1,0:T(8,128)(2,1)}, u32[]{:S(2)}, u32[]{:S(2)}) collective-permute-start(bf16[3072,256]{1,0:T(8,128)(2,1)S(1)} %copy-done.2), channel_id=1, source_target_pairs={{0,3},{1,0},{2,1},{3,2},{4,7},{5,4},{6,5},{7,6},{8,11},{9,8},{10,9... | collective-permute-start | bytes 4718600 | tf_op jit(solution)/shard_map/ppermute | solution.py:41
  46.3 0.0 collective-permute-done.1
  46.3 0.1 pad_maximum_fusion
  46.5 0.8 fusion.33
  47.3 0.3 fusion.2
  47.6 0.0 collective-permute-done.8.refs_5_
  47.6 2.4 %collective-permute-start.10 = (bf16[3072,256]{1,0:T(8,128)(2,1)}, bf16[3072,256]{1,0:T(8,128)(2,1)}, u32[]{:S(2)}, u32[]{:S(2)}) collective-permute-start(bf16[3072,256]{1,0:T(8,128)(2,1)} %collective-permute-done.8.refs_5_), channel_id=1, source_target_pairs={{0,3},{1,0},{2,1},{3,2},{4,7},{5,4},{6,5},{7,6},{8,11},{9,8},{10,9... | collective-permute-start | bytes 4718600 | tf_op jit(solution)/shard_map/ppermute | solution.py:41
  50.0 1.6 %collective-permute-done.5.refs_2_ = bf16[3072,256]{1,0:T(8,128)(2,1)} collective-permute-done((bf16[3072,256]{1,0:T(8,128)(2,1)}, bf16[3072,256]{1,0:T(8,128)(2,1)}, u32[]{:S(2)}, u32[]{:S(2)}) %collective-permute-start.5) | collective-permute-done | bytes 1572896 | tf_op jit(solution)/shard_map/ppermute | solution.py:41
  51.6 1.9 %collective-permute-start.9 = (bf16[3072,256]{1,0:T(8,128)(2,1)}, bf16[3072,256]{1,0:T(8,128)(2,1)}, u32[]{:S(2)}, u32[]{:S(2)}) collective-permute-start(bf16[3072,256]{1,0:T(8,128)(2,1)} %collective-permute-done.5.refs_2_), channel_id=1, source_target_pairs={{0,1},{1,2},{2,3},{3,0},{4,5},{5,6},{6,7},{7,4},{8,9},{9,10},{10,1... | collective-permute-start | bytes 4718600 | tf_op jit(solution)/shard_map/ppermute | solution.py:41
  53.5 0.4 fusion.3
  53.9 0.1 fusion.30
  54.0 0.1 fusion.21
  54.1 0.1 copy.21
  54.2 9.0 %all-to-all-done = bf16[32,8,512]{2,1,0:T(8,128)(2,1)S(1)} async-done(((bf16[32,8,512]{2,1,0:T(8,128)(2,1)}), bf16[32,8,512]{2,1,0:T(8,128)(2,1)S(1)}, u32[]{:S(2)}, u32[]{:S(2)}) %all-to-all-start) | async-done | bytes 262176 | tf_op jit(solution)/shard_map/all_to_all | solution.py:347
  63.3 1.2 broadcast_in_dim.6
  64.4 4.9 %all-to-all-start.1 = ((bf16[4,320,512]{2,1,0:T(8,128)(2,1)}), bf16[4,320,512]{2,1,0:T(8,128)(2,1)S(1)}, u32[]{:S(2)}, u32[]{:S(2)}) async-start(bf16[4,320,512]{2,1,0:T(8,128)(2,1)} %broadcast_in_dim.6), calls=%async_computation.1 | async-start | bytes 2621440 | tf_op jit(solution)/shard_map/all_to_all | solution.py:356
  69.4 14.8 %all-to-all-done.1.x_ref = bf16[4,320,512]{2,1,0:T(8,128)(2,1)S(1)} async-done(((bf16[4,320,512]{2,1,0:T(8,128)(2,1)}), bf16[4,320,512]{2,1,0:T(8,128)(2,1)S(1)}, u32[]{:S(2)}, u32[]{:S(2)}) %all-to-all-start.1) | async-done | bytes 1310752 | tf_op jit(solution)/shard_map/all_to_all | solution.py:356
  84.1 3.5 %collective-permute-done.10.refs_7_ = bf16[3072,256]{1,0:T(8,128)(2,1)} collective-permute-done((bf16[3072,256]{1,0:T(8,128)(2,1)}, bf16[3072,256]{1,0:T(8,128)(2,1)}, u32[]{:S(2)}, u32[]{:S(2)}) %collective-permute-start.10) | collective-permute-done | bytes 1572896 | tf_op jit(solution)/shard_map/ppermute | solution.py:41
  87.6 8.4 %ffn.1 = bf16[16,256,128]{2,1,0:T(8,128)(2,1)} custom-call(bf16[4,320,512]{2,1,0:T(8,128)(2,1)} %copy-done.1, bf16[3072,256]{1,0:T(8,128)(2,1)} %get-tuple-element.7.refs_0_, bf16[3072,256]{1,0:T(8,128)(2,1)} %get-tuple-element.8.refs_1_, bf16[3072,256]{1,0:T(8,128)(2,1)} %collective-permute-done.5.refs_2_, ...), custom_call_target="tpu_custom_call" | custom-call | tf_op jit(solution)/shard_map/ffn/pallas_call | solution.py:183
  96.1 24.5 %all_to_all.27 = bf16[16,256,128]{2,1,0:T(8,128)(2,1)S(1)} all-to-all(bf16[16,256,128]{2,1,0:T(8,128)(2,1)} %ffn.1), channel_id=1, replica_groups={{0,1,2,3,4,5,6,7,8,9,10,11,12,13,14,15},{16,20,24,28,17,21,25,29,18,22,..., dimensions={0} | all-to-all | bytes 2097152 | tf_op jit(solution)/shard_map/all_to_all | solution.py:361
  120.5 0.2 reduce_sum.22
  120.8 0.7 copy_bitcast_fusion
  121.5 13.3 %all-to-all-start.3 = ((bf16[32,32,128]{2,1,0:T(8,128)(2,1)}), bf16[32,32,128]{2,1,0:T(8,128)(2,1)S(1)}, u32[]{:S(2)}, u32[]{:S(2)}) async-start(bf16[32,32,128]{2,1,0:T(8,128)(2,1)} %copy_bitcast_fusion), calls=%async_computation.3 | async-start | bytes 524288 | tf_op jit(solution)/shard_map/all_to_all | solution.py:366
  134.8 1.0 slice.82.own_ref
  135.8 1.9 %collective-permute-start.2 = (bf16[4,64,512]{2,1,0:T(8,128)(2,1)S(1)}, bf16[4,64,512]{2,1,0:T(8,128)(2,1)S(1)}, u32[]{:S(2)}, u32[]{:S(2)}) collective-permute-start(bf16[4,64,512]{2,1,0:T(8,128)(2,1)S(1)} %slice.82.own_ref), channel_id=1, source_target_pairs={{0,1},{1,2},{2,3},{3,0},{4,5},{5,6},{6,7},{7,4},{8,9},{9,10},{10,1... | collective-permute-start | bytes 786440 | tf_op jit(solution)/shard_map/ppermute | solution.py:41
  137.7 4.6 %collective-permute-start.3 = (bf16[4,64,512]{2,1,0:T(8,128)(2,1)S(1)}, bf16[4,64,512]{2,1,0:T(8,128)(2,1)S(1)}, u32[]{:S(2)}, u32[]{:S(2)}) collective-permute-start(bf16[4,64,512]{2,1,0:T(8,128)(2,1)S(1)} %slice.82.own_ref), channel_id=1, source_target_pairs={{0,3},{1,0},{2,1},{3,2},{4,7},{5,4},{6,5},{7,6},{8,11},{9,8},{10,9... | collective-permute-start | bytes 786440 | tf_op jit(solution)/shard_map/ppermute | solution.py:41
  142.3 1.9 %collective-permute-start.4 = (bf16[4,64,512]{2,1,0:T(8,128)(2,1)S(1)}, bf16[4,64,512]{2,1,0:T(8,128)(2,1)S(1)}, u32[]{:S(2)}, u32[]{:S(2)}) collective-permute-start(bf16[4,64,512]{2,1,0:T(8,128)(2,1)S(1)} %slice.82.own_ref), channel_id=1, source_target_pairs={{0,2},{1,3},{2,0},{3,1},{4,6},{5,7},{6,4},{7,5},{8,10},{9,11},{10,... | collective-permute-start | bytes 786440 | tf_op jit(solution)/shard_map/ppermute | solution.py:41
  144.2 0.8 copy.23.weight_ref
  145.0 3.4 %collective-permute-done.3.next_ref = bf16[4,64,512]{2,1,0:T(8,128)(2,1)S(1)} collective-permute-done((bf16[4,64,512]{2,1,0:T(8,128)(2,1)S(1)}, bf16[4,64,512]{2,1,0:T(8,128)(2,1)S(1)}, u32[]{:S(2)}, u32[]{:S(2)}) %collective-permute-start.3) | collective-permute-done | bytes 262176 | tf_op jit(solution)/shard_map/ppermute | solution.py:41
  148.4 2.8 %collective-permute-done.4.far_ref = bf16[4,64,512]{2,1,0:T(8,128)(2,1)S(1)} collective-permute-done((bf16[4,64,512]{2,1,0:T(8,128)(2,1)S(1)}, bf16[4,64,512]{2,1,0:T(8,128)(2,1)S(1)}, u32[]{:S(2)}, u32[]{:S(2)}) %collective-permute-start.4) | collective-permute-done | bytes 262176 | tf_op jit(solution)/shard_map/ppermute | solution.py:41
  151.2 0.7 copy-done.7
  151.9 2.5 %project.1 = bf16[512,128]{1,0:T(8,128)(2,1)} custom-call(bf16[4,64,512]{2,1,0:T(8,128)(2,1)} %copy-done.4, bf16[4,64,512]{2,1,0:T(8,128)(2,1)} %copy-done.5, bf16[4,64,512]{2,1,0:T(8,128)(2,1)} %copy-done.6, bf16[4,64,512]{2,1,0:T(8,128)(2,1)} %copy-done.7, bf16[1024,128]{1,0:T(8,128)(2,1)} %weight_ref.2), custom_call_target="tpu_custom_call" | custom-call | tf_op jit(solution)/shard_map/project/pallas_call | solution.py:238
  154.4 2.6 %all-to-all-done.3 = bf16[32,32,128]{2,1,0:T(8,128)(2,1)S(1)} async-done(((bf16[32,32,128]{2,1,0:T(8,128)(2,1)}), bf16[32,32,128]{2,1,0:T(8,128)(2,1)S(1)}, u32[]{:S(2)}, u32[]{:S(2)}) %all-to-all-start.3) | async-done | bytes 262176 | tf_op jit(solution)/shard_map/all_to_all | solution.py:366
  157.0 0.7 copy-done.3
  157.7 2.2 %combine.1 = bf16[256,128]{1,0:T(8,128)(2,1)} custom-call(bf16[1024,128]{1,0:T(8,128)(2,1)} %bitcast.57, s32[256,128]{1,0:T(8,128)} %get-tuple-element.9.slot_ref, f32[256,2]{1,0:T(8,128)} %copy.23.weight_ref), custom_call_target="tpu_custom_call" | custom-call | tf_op jit(solution)/shard_map/combine/pallas_call | solution.py:209
  (32 shorter events, 0.1 us)
Async XLA Ops:
  0.6 15.2 %copy-start = (bf16[512,256]{1,0:T(8,128)(2,1)S(1)}, bf16[512,256]{1,0:T(8,128)(2,1)}, u32[]{:S(2)}) copy-start(bf16[512,256]{1,0:T(8,128)(2,1)} %param.14) | copy-start | bytes 786436
  0.6 15.0 %copy-start.8 = (bf16[512,64]{0,1:T(8,128)(2,1)S(1)}, bf16[512,64]{0,1:T(8,128)(2,1)}, u32[]{:S(2)}) copy-start(bf16[512,64]{0,1:T(8,128)(2,1)} %param.12) | copy-start | bytes 196612
  0.7 15.3 %copy-start.9 = (bf16[512,256]{1,0:T(8,128)(2,1)S(1)}, bf16[512,256]{1,0:T(8,128)(2,1)}, u32[]{:S(2)}) copy-start(bf16[512,256]{1,0:T(8,128)(2,1)} %param.13) | copy-start | bytes 786436
  6.3 41.3 %collective-permute-start.8 = (bf16[3072,256]{1,0:T(8,128)(2,1)}, bf16[3072,256]{1,0:T(8,128)(2,1)}, u32[]{:S(2)}, u32[]{:S(2)}) collective-permute-start(bf16[3072,256]{1,0:T(8,128)(2,1)} %get-tuple-element.8.refs_1_), channel_id=1, source_target_pairs={{0,3},{1,0},{2,1},{3,2},{4,7},{5,4},{6,5},{7,6},{8,11},{9,8},{10,9... | collective-permute-start | bytes 4718600 | tf_op jit(solution)/shard_map/ppermute | solution.py:41
  11.8 57.6 %collective-permute-start.6 = (bf16[3072,256]{1,0:T(8,128)(2,1)}, bf16[3072,256]{1,0:T(8,128)(2,1)}, u32[]{:S(2)}, u32[]{:S(2)}) collective-permute-start(bf16[3072,256]{1,0:T(8,128)(2,1)} %get-tuple-element.8.refs_1_), channel_id=1, source_target_pairs={{0,1},{1,2},{2,3},{3,0},{4,5},{5,6},{6,7},{7,4},{8,9},{9,10},{10,1... | collective-permute-start | bytes 4718600 | tf_op jit(solution)/shard_map/ppermute | solution.py:41
  13.7 37.9 %collective-permute-start.5 = (bf16[3072,256]{1,0:T(8,128)(2,1)}, bf16[3072,256]{1,0:T(8,128)(2,1)}, u32[]{:S(2)}, u32[]{:S(2)}) collective-permute-start(bf16[3072,256]{1,0:T(8,128)(2,1)} %get-tuple-element.7.refs_0_), channel_id=1, source_target_pairs={{0,1},{1,2},{2,3},{3,0},{4,5},{5,6},{6,7},{7,4},{8,9},{9,10},{10,1... | collective-permute-start | bytes 4718600 | tf_op jit(solution)/shard_map/ppermute | solution.py:41
  16.0 25.7 %copy-start.2 = (bf16[3072,256]{1,0:T(8,128)(2,1)S(1)}, bf16[3072,256]{1,0:T(8,128)(2,1)}, u32[]{:S(2)}) copy-start(bf16[3072,256]{1,0:T(8,128)(2,1)} %get-tuple-element.7.refs_0_) | copy-start | bytes 4718596
  17.5 24.2 %collective-permute-start = (bf16[2,128,1,64]{3,1,2,0:T(8,128)(2,1)S(1)}, bf16[2,128,1,64]{3,1,2,0:T(8,128)(2,1)S(1)}, u32[]{:S(2)}, u32[]{:S(2)}) collective-permute-start(bf16[2,128,1,64]{3,1,2,0:T(8,128)(2,1)S(1)} %get-tuple-element.10), channel_id=1, source_target_pairs={{0,16},{16,32},{32,48},{48,64},{64,80},{80,96},{96,112},{112,128},... | collective-permute-start | bytes 98312 | tf_op jit(solution)/shard_map/ppermute | solution.py:254
  22.4 24.0 %collective-permute-start.1 = (bf16[2,128,1,64]{3,1,2,0:T(8,128)(2,1)S(1)}, bf16[2,128,1,64]{3,1,2,0:T(8,128)(2,1)S(1)}, u32[]{:S(2)}, u32[]{:S(2)}) collective-permute-start(bf16[2,128,1,64]{3,1,2,0:T(8,128)(2,1)S(1)} %get-tuple-element.11), channel_id=1, source_target_pairs={{16,0},{32,16},{48,32},{64,48},{80,64},{96,80},{112,96},{128,112},... | collective-permute-start | bytes 98312 | tf_op jit(solution)/shard_map/ppermute | solution.py:257
  26.0 37.2 %all-to-all-start = ((bf16[32,8,512]{2,1,0:T(8,128)(2,1)}), bf16[32,8,512]{2,1,0:T(8,128)(2,1)S(1)}, u32[]{:S(2)}, u32[]{:S(2)}) async-start(bf16[32,8,512]{2,1,0:T(8,128)(2,1)} %bitcast.2), calls=%async_computation | async-start | bytes 524288 | tf_op jit(solution)/shard_map/all_to_all | solution.py:347
  41.7 27.7 %collective-permute-start.7 = (bf16[3072,256]{1,0:T(8,128)(2,1)S(1)}, bf16[3072,256]{1,0:T(8,128)(2,1)}, u32[]{:S(2)}, u32[]{:S(2)}) collective-permute-start(bf16[3072,256]{1,0:T(8,128)(2,1)S(1)} %copy-done.2), channel_id=1, source_target_pairs={{0,3},{1,0},{2,1},{3,2},{4,7},{5,4},{6,5},{7,6},{8,11},{9,8},{10,9... | collective-permute-start | bytes 4718600 | tf_op jit(solution)/shard_map/ppermute | solution.py:41
  47.6 40.0 %collective-permute-start.10 = (bf16[3072,256]{1,0:T(8,128)(2,1)}, bf16[3072,256]{1,0:T(8,128)(2,1)}, u32[]{:S(2)}, u32[]{:S(2)}) collective-permute-start(bf16[3072,256]{1,0:T(8,128)(2,1)} %collective-permute-done.8.refs_5_), channel_id=1, source_target_pairs={{0,3},{1,0},{2,1},{3,2},{4,7},{5,4},{6,5},{7,6},{8,11},{9,8},{10,9... | collective-permute-start | bytes 4718600 | tf_op jit(solution)/shard_map/ppermute | solution.py:41
  51.6 36.0 %collective-permute-start.9 = (bf16[3072,256]{1,0:T(8,128)(2,1)}, bf16[3072,256]{1,0:T(8,128)(2,1)}, u32[]{:S(2)}, u32[]{:S(2)}) collective-permute-start(bf16[3072,256]{1,0:T(8,128)(2,1)} %collective-permute-done.5.refs_2_), channel_id=1, source_target_pairs={{0,1},{1,2},{2,3},{3,0},{4,5},{5,6},{6,7},{7,4},{8,9},{9,10},{10,1... | collective-permute-start | bytes 4718600 | tf_op jit(solution)/shard_map/ppermute | solution.py:41
  64.4 19.7 %all-to-all-start.1 = ((bf16[4,320,512]{2,1,0:T(8,128)(2,1)}), bf16[4,320,512]{2,1,0:T(8,128)(2,1)S(1)}, u32[]{:S(2)}, u32[]{:S(2)}) async-start(bf16[4,320,512]{2,1,0:T(8,128)(2,1)} %broadcast_in_dim.6), calls=%async_computation.1 | async-start | bytes 2621440 | tf_op jit(solution)/shard_map/all_to_all | solution.py:356
  84.1 3.5 %copy-start.1 = (bf16[4,320,512]{2,1,0:T(8,128)(2,1)}, bf16[4,320,512]{2,1,0:T(8,128)(2,1)S(1)}, u32[]{:S(2)}) copy-start(bf16[4,320,512]{2,1,0:T(8,128)(2,1)S(1)} %all-to-all-done.1.x_ref) | copy-start | bytes 3932164
  120.5 23.7 %copy-start.10 = (f32[256,2]{0,1:T(2,128)S(1)}, f32[256,2]{0,1:T(2,128)}, u32[]{:S(2)}) copy-start(f32[256,2]{0,1:T(2,128)} %param.20) | copy-start | bytes 6148
  121.5 35.5 %all-to-all-start.3 = ((bf16[32,32,128]{2,1,0:T(8,128)(2,1)}), bf16[32,32,128]{2,1,0:T(8,128)(2,1)S(1)}, u32[]{:S(2)}, u32[]{:S(2)}) async-start(bf16[32,32,128]{2,1,0:T(8,128)(2,1)} %copy_bitcast_fusion), calls=%async_computation.3 | async-start | bytes 524288 | tf_op jit(solution)/shard_map/all_to_all | solution.py:366
  135.8 15.4 %copy-start.4 = (bf16[4,64,512]{2,1,0:T(8,128)(2,1)}, bf16[4,64,512]{2,1,0:T(8,128)(2,1)S(1)}, u32[]{:S(2)}) copy-start(bf16[4,64,512]{2,1,0:T(8,128)(2,1)S(1)} %slice.82.own_ref) | copy-start | bytes 786436
  135.8 9.3 %collective-permute-start.2 = (bf16[4,64,512]{2,1,0:T(8,128)(2,1)S(1)}, bf16[4,64,512]{2,1,0:T(8,128)(2,1)S(1)}, u32[]{:S(2)}, u32[]{:S(2)}) collective-permute-start(bf16[4,64,512]{2,1,0:T(8,128)(2,1)S(1)} %slice.82.own_ref), channel_id=1, source_target_pairs={{0,1},{1,2},{2,3},{3,0},{4,5},{5,6},{6,7},{7,4},{8,9},{9,10},{10,1... | collective-permute-start | bytes 786440 | tf_op jit(solution)/shard_map/ppermute | solution.py:41
  137.7 10.7 %collective-permute-start.3 = (bf16[4,64,512]{2,1,0:T(8,128)(2,1)S(1)}, bf16[4,64,512]{2,1,0:T(8,128)(2,1)S(1)}, u32[]{:S(2)}, u32[]{:S(2)}) collective-permute-start(bf16[4,64,512]{2,1,0:T(8,128)(2,1)S(1)} %slice.82.own_ref), channel_id=1, source_target_pairs={{0,3},{1,0},{2,1},{3,2},{4,7},{5,4},{6,5},{7,6},{8,11},{9,8},{10,9... | collective-permute-start | bytes 786440 | tf_op jit(solution)/shard_map/ppermute | solution.py:41
  142.3 8.9 %collective-permute-start.4 = (bf16[4,64,512]{2,1,0:T(8,128)(2,1)S(1)}, bf16[4,64,512]{2,1,0:T(8,128)(2,1)S(1)}, u32[]{:S(2)}, u32[]{:S(2)}) collective-permute-start(bf16[4,64,512]{2,1,0:T(8,128)(2,1)S(1)} %slice.82.own_ref), channel_id=1, source_target_pairs={{0,2},{1,3},{2,0},{3,1},{4,6},{5,7},{6,4},{7,5},{8,10},{9,11},{10,... | collective-permute-start | bytes 786440 | tf_op jit(solution)/shard_map/ppermute | solution.py:41
  145.0 6.2 %copy-start.5 = (bf16[4,64,512]{2,1,0:T(8,128)(2,1)}, bf16[4,64,512]{2,1,0:T(8,128)(2,1)S(1)}, u32[]{:S(2)}) copy-start(bf16[4,64,512]{2,1,0:T(8,128)(2,1)S(1)} %collective-permute-done.2.prev_ref) | copy-start | bytes 786436
  148.4 2.8 %copy-start.6 = (bf16[4,64,512]{2,1,0:T(8,128)(2,1)}, bf16[4,64,512]{2,1,0:T(8,128)(2,1)S(1)}, u32[]{:S(2)}) copy-start(bf16[4,64,512]{2,1,0:T(8,128)(2,1)S(1)} %collective-permute-done.3.next_ref) | copy-start | bytes 786436
  151.2 0.7 copy-start.7
  157.0 0.7 copy-start.3

commit v4 on v3

--- a/solution.py
+++ b/solution.py
@@ -36,20 +36,62 @@
 HALF_W = 3072
 
 
+def resident(x):
+    return pltpu.with_memory_space_constraint(x, pltpu.VMEM)
+
+
+def vmem_mib(count):
+    return pltpu.CompilerParams(vmem_limit_bytes=count << 20)
+
+
 def line_shift(x, step):
     pairs = [(line[i], line[(i + step) % 4]) for line in LINE_L for i in range(4)]
     return lax.ppermute(x, PLANE, pairs)
 
 
+def pack_kernel(gate_ref, up_ref, wa_ref, stage_ref, sems):
+    copies = [
+        pltpu.make_async_copy(gate_ref.at[0], stage_ref.at[pl.ds(0, 2048)], sems.at[0]),
+        pltpu.make_async_copy(
+            up_ref.at[0, pl.ds(0, 1024)], stage_ref.at[pl.ds(2048, 1024)], sems.at[1]
+        ),
+    ]
+    leave = [
+        pltpu.make_async_copy(
+            stage_ref.at[pl.ds(0, 2048)], wa_ref.at[pl.ds(0, 2048)], sems.at[2]
+        ),
+        pltpu.make_async_copy(
+            stage_ref.at[pl.ds(2048, 1024)], wa_ref.at[pl.ds(2048, 1024)], sems.at[3]
+        ),
+    ]
+    for copy in copies:
+        copy.start()
+    for come, go in zip(copies, leave):
+        come.wait()
+        go.start()
+    for go in leave:
+        go.wait()
+
+
+def pack(gate, up):
+    return pl.pallas_call(
+        pack_kernel,
+        out_shape=jax.ShapeDtypeStruct((HALF_W, 256), jnp.bfloat16),
+        in_specs=[ANY, ANY],
+        out_specs=ANY,
+        scratch_shapes=[
+            pltpu.VMEM((HALF_W, 256), jnp.bfloat16), pltpu.SemaphoreType.DMA((4,))
+        ],
+        compiler_params=vmem_mib(4),
+        name="pack",
+    )(gate, up)
+
+
 def prep_kernel(
-    x_ref, gain_ref, routes_ref, gate_ref, up_ref, down_ref,
-    out_ref, slot_ref, wa_ref, wb_ref, normed_ref, sa_ref, sb_ref, sems,
+    x_ref, gain_ref, routes_ref, up_ref, down_ref,
+    out_ref, slot_ref, wb_ref, normed_ref, sb_ref, sems,
 ):
-    copies = [
-        (gate_ref.at[0], sa_ref.at[pl.ds(0, 2048)]),
-        (up_ref.at[0, pl.ds(0, 1024)], sa_ref.at[pl.ds(2048, 1024)]),
-        (up_ref.at[0, pl.ds(1024, 1024)], sb_ref.at[pl.ds(0, 1024)]),
-    ] + [
+    copies = [(up_ref.at[0, pl.ds(1024, 1024)], sb_ref.at[pl.ds(0, 1024)])] + [
         (down_ref.at[0, :, pl.ds(c * 256, 256)], sb_ref.at[pl.ds(1024 + c * 256, 256)])
         for c in range(8)
     ]
@@ -67,12 +109,8 @@
     lax.fori_loop(0, ROWS_B // 32, norm_rows, 0)
     for copy in copies:
         copy.wait()
-    leave = [
-        pltpu.make_async_copy(sa_ref, wa_ref, sems.at[11]),
-        pltpu.make_async_copy(sb_ref, wb_ref, sems.at[12]),
-    ]
-    for copy in leave:
-        copy.start()
+    leave = pltpu.make_async_copy(sb_ref, wb_ref, sems.at[9])
+    leave.start()
 
     first = routes_ref[0:1, :]
     second = routes_ref[1:2, :]
@@ -112,30 +150,27 @@
     )
     even_row = ((lax.broadcasted_iota(jnp.int32, (ROWS_B, 512), 0) >> 3) & 1) == 0
     out_ref[...] = jnp.where(even_row, from_y, from_x).astype(jnp.bfloat16)
-    for copy in leave:
-        copy.wait()
-
-
-def prepare(expert_input, norm_gain, routes, gate, up, down):
-    half = jax.ShapeDtypeStruct((HALF_W, 256), jnp.bfloat16)
+    leave.wait()
+
+
+def prepare(expert_input, norm_gain, routes, up, down):
     return pl.pallas_call(
         prep_kernel,
         out_shape=(
             jax.ShapeDtypeStruct((ROWS_B, 512), jnp.bfloat16),
             jax.ShapeDtypeStruct((ROWS_B, 128), jnp.int32),
-            half,
-            half,
+            jax.ShapeDtypeStruct((HALF_W, 256), jnp.bfloat16),
         ),
-        in_specs=[VMEM, VMEM, VMEM, ANY, ANY, ANY],
-        out_specs=(VMEM, VMEM, ANY, ANY),
+        in_specs=[VMEM, VMEM, VMEM, ANY, ANY],
+        out_specs=(VMEM, VMEM, ANY),
         scratch_shapes=[
             pltpu.VMEM((ROWS_B, D), jnp.bfloat16),
             pltpu.VMEM((HALF_W, 256), jnp.bfloat16),
-            pltpu.VMEM((HALF_W, 256), jnp.bfloat16),
-            pltpu.SemaphoreType.DMA((13,)),
+            pltpu.SemaphoreType.DMA((10,)),
         ],
+        compiler_params=vmem_mib(16),
         name="prep",
-    )(expert_input, norm_gain.reshape(1, D), routes.T, gate, up, down)
+    )(expert_input, norm_gain.reshape(1, D), routes.T, up, down)
 
 
 def slice_hidden(x_ref, wa, wb):
@@ -190,8 +225,9 @@
             pltpu.VMEM((8, HALF_W, 256), jnp.bfloat16),
             pltpu.SemaphoreType.DMA((8,)),
         ],
+        compiler_params=vmem_mib(24),
         name="ffn",
-    )(x, *weights)
+    )(resident(x), *weights)
 
 
 def combine_kernel(ret_ref, slot_ref, weight_ref, out_ref):
@@ -211,8 +247,9 @@
         out_shape=jax.ShapeDtypeStruct((ROWS_B, 128), jnp.bfloat16),
         in_specs=[VMEM] * 3,
         out_specs=VMEM,
+        compiler_params=vmem_mib(12),
         name="combine",
-    )(returned, slots, route_weights)
+    )(resident(returned), slots, route_weights)
 
 
 def project_kernel(own_ref, prev_ref, next_ref, far_ref, weight_ref, out_ref, a_ref, w_ref):
@@ -243,8 +280,9 @@
         scratch_shapes=[
             pltpu.VMEM((256, 2048), jnp.bfloat16), pltpu.VMEM((2048, 256), jnp.bfloat16)
         ],
+        compiler_params=vmem_mib(12),
         name="project",
-    )(own, prev, nxt, far, out_weight)
+    )(*(resident(a) for a in (own, prev, nxt, far, out_weight)))
 
 
 def padded(block, axis, dim, width):
@@ -337,12 +375,13 @@
     up_weight,
     down_weight,
 ):
-    outgoing, slots, wa, wb = prepare(
-        expert_input, norm_gain, routes, gate_weight, up_weight, down_weight
-    )
+    wa = pack(gate_weight, up_weight)
     prev_a = line_shift(wa, 1)
+    next_a = line_shift(wa, -1)
+    outgoing, slots, wb = prepare(
+        expert_input, norm_gain, routes, up_weight, down_weight
+    )
     next_b = line_shift(wb, -1)
-    next_a = line_shift(wa, -1)
     prev_b = line_shift(wb, 1)
     arrived = lax.all_to_all(outgoing, EP, 0, 0, tiled=True)
     far_a = line_shift(prev_a, 1)

time: 161 us -> 159 us (0.988)
  Pallas kernels: 18.7 us -> 11.6 us
  waiting for transfers between devices: 37.7 us -> 41.3 us
  local copies, waits for them, and re-layouts: 5.44 us -> 7.52 us
    unnamed x24, local copies, waits for them, and re-layouts: 2.34 us -> 5.37 us
    all_to_all x1, waiting for transfers between devices: 2.62 us -> 5.53 us  [local(): returned = lax.all_to_all(result, EP, 0, 0, tiled=True)]
    pallas_call x1, Pallas kernels: 8.42 us -> 5.77 us  [ffn(): pl.pallas_call(ffn_kernel, out_shape=jax.ShapeDtypeStruct((16, ROWS_B, 12...]
    pallas_call x1, Pallas kernels: 5.62 us -> 3.22 us  [prepare(): pl.pallas_call(prep_kernel, out_shape=(jax.ShapeDtypeStruct((ROWS_B, 512)...]
  transfers between devices with their start and end apart: 14 -> 14, of which waited for: 7 -> 7; matrix products, arithmetic and copies ran while one was open for 4% -> 3% of each run, Pallas kernels for 2% -> 1%
where the time goes in v4:
time: 159 us; the launch traced here: 158 us
  starting transfers between devices  68.4 us (43%)
  waiting for transfers between devices  41.3 us (26%)
  blocking collectives  24.2 us (15%)
  Pallas kernels  11.6 us (7%)
  local copies, waits for them, and re-layouts  7.52 us (5%)
  other arithmetic  2.36 us (1%)
  between operations  1.66 us (1%)
    ppermute x9, starting transfers between devices, line_shift(): return lax.ppermute(x, PLANE, pairs)  26.8 us
    all_to_all x1, blocking collectives, local(): lax.all_to_all(partial, PLANE, 0, 0, tiled=True, axis_index_groups=WHOLE)  24.2 us
    all_to_all x1, starting transfers between devices, local(): arrived = lax.all_to_all(outgoing, EP, 0, 0, tiled=True)  15 us
    all_to_all x1, waiting for transfers between devices, local(): lax.all_to_all(jnp.broadcast_to(payload[None], (4, *payload.shape)), PLAN...  14.8 us
    all_to_all x1, starting transfers between devices, local(): returned = lax.all_to_all(result, EP, 0, 0, tiled=True)  13.3 us
    ppermute x9, waiting for transfers between devices, line_shift(): return lax.ppermute(x, PLANE, pairs)  11.7 us
    all_to_all x1, waiting for transfers between devices, local(): arrived = lax.all_to_all(outgoing, EP, 0, 0, tiled=True)  9.29 us
    pallas_call x1, Pallas kernels, ffn(): pl.pallas_call(ffn_kernel, out_shape=jax.ShapeDtypeStruct((16, ROWS_B, 12...  5.77 us
  transfers between devices with their start and end apart: 14, of which 7 were waited for; matrix products, arithmetic and copies ran while one was open for 3% of the time, Pallas kernels for 1%

profile of v4, /device:TPU:1, one launch (start us, length us, event | category | flops | bytes accessed | tf_op | source)
XLA Modules:
  0.0 158.4 jit_solution(228618650623445317)
XLA Ops:
  0.7 1.3 copy-done.1
  1.9 1.2 copy-done.3
  3.1 1.2 copy-done.4
  4.4 0.7 copy-done.6
  5.1 0.7 copy-done.7
  5.7 3.2 %prep.1 = (bf16[256,512]{1,0:T(8,128)(2,1)}, s32[256,128]{1,0:T(8,128)S(1)}, bf16[3072,256]{1,0:T(8,128)(2,1)}) custom-call(bf16[256,2048]{1,0:T(8,128)(2,1)S(1)} %copy-done.3, f32[1,2048]{1,0:T(1,128)S(1)} %bitcast.56, s32[2,256]{1,0:T(2,128)S(1)} %bitcast.57, bf16[1,2048,256]{2,1,0:T(8,128)(2,1)S(1)} %copy-done.1, bf16[1,256,2048]{2,1,0:T(8,128)(2,1)S(1)} %copy-done.4), custom_call_target="tpu_custom_call" | custom-call | tf_op jit(solution)/shard_map/prep/pallas_call | solution.py:157
  9.0 5.6 %collective-permute-start.8 = (bf16[3072,256]{1,0:T(8,128)(2,1)}, bf16[3072,256]{1,0:T(8,128)(2,1)}, u32[]{:S(2)}, u32[]{:S(2)}) collective-permute-start(bf16[3072,256]{1,0:T(8,128)(2,1)} %get-tuple-element.6.refs_1_), channel_id=1, source_target_pairs={{0,3},{1,0},{2,1},{3,2},{4,7},{5,4},{6,5},{7,6},{8,11},{9,8},{10,9... | collective-permute-start | bytes 4718600 | tf_op jit(solution)/shard_map/ppermute | solution.py:49
  14.6 1.9 %collective-permute-start.6 = (bf16[3072,256]{1,0:T(8,128)(2,1)}, bf16[3072,256]{1,0:T(8,128)(2,1)}, u32[]{:S(2)}, u32[]{:S(2)}) collective-permute-start(bf16[3072,256]{1,0:T(8,128)(2,1)} %get-tuple-element.6.refs_1_), channel_id=1, source_target_pairs={{0,1},{1,2},{2,3},{3,0},{4,5},{5,6},{6,7},{7,4},{8,9},{9,10},{10,1... | collective-permute-start | bytes 4718600 | tf_op jit(solution)/shard_map/ppermute | solution.py:49
  16.5 0.3 pack.1.refs_0_
  16.8 1.9 %collective-permute-start.5 = (bf16[3072,256]{1,0:T(8,128)(2,1)S(1)}, bf16[3072,256]{1,0:T(8,128)(2,1)}, u32[]{:S(2)}, u32[]{:S(2)}) collective-permute-start(bf16[3072,256]{1,0:T(8,128)(2,1)S(1)} %pack.1.refs_0_), channel_id=1, source_target_pairs={{0,1},{1,2},{2,3},{3,0},{4,5},{5,6},{6,7},{7,4},{8,9},{9,10},{10,1... | collective-permute-start | bytes 4718600 | tf_op jit(solution)/shard_map/ppermute | solution.py:49
  18.8 0.1 copy.20
  19.0 0.1 dynamic-slice_bitcast_fusion
  19.1 0.1 bitcast_convert_fusion
  19.2 1.3 fusion.26
  20.5 0.1 pad_maximum_fusion.5
  20.6 4.9 %collective-permute-start = (bf16[2,128,1,64]{3,1,2,0:T(8,128)(2,1)S(1)}, bf16[2,128,1,64]{3,1,2,0:T(8,128)(2,1)S(1)}, u32[]{:S(2)}, u32[]{:S(2)}) collective-permute-start(bf16[2,128,1,64]{3,1,2,0:T(8,128)(2,1)S(1)} %get-tuple-element.8), channel_id=1, source_target_pairs={{0,16},{16,32},{32,48},{48,64},{64,80},{80,96},{96,112},{112,128},... | collective-permute-start | bytes 98312 | tf_op jit(solution)/shard_map/ppermute | solution.py:292
  25.5 3.6 %collective-permute-start.1 = (bf16[2,128,1,64]{3,1,2,0:T(8,128)(2,1)S(1)}, bf16[2,128,1,64]{3,1,2,0:T(8,128)(2,1)S(1)}, u32[]{:S(2)}, u32[]{:S(2)}) collective-permute-start(bf16[2,128,1,64]{3,1,2,0:T(8,128)(2,1)S(1)} %get-tuple-element.9), channel_id=1, source_target_pairs={{16,0},{32,16},{48,32},{64,48},{80,64},{96,80},{112,96},{128,112},... | collective-permute-start | bytes 98312 | tf_op jit(solution)/shard_map/ppermute | solution.py:295
  29.1 15.0 %all-to-all-start = ((bf16[32,8,512]{2,1,0:T(8,128)(2,1)}), bf16[32,8,512]{2,1,0:T(8,128)(2,1)S(1)}, u32[]{:S(2)}, u32[]{:S(2)}) async-start(bf16[32,8,512]{2,1,0:T(8,128)(2,1)} %bitcast.2), calls=%async_computation | async-start | bytes 524288 | tf_op jit(solution)/shard_map/all_to_all | solution.py:386
  44.8 4.6 %collective-permute-start.7 = (bf16[3072,256]{1,0:T(8,128)(2,1)S(1)}, bf16[3072,256]{1,0:T(8,128)(2,1)}, u32[]{:S(2)}, u32[]{:S(2)}) collective-permute-start(bf16[3072,256]{1,0:T(8,128)(2,1)S(1)} %pack.1.refs_0_), channel_id=1, source_target_pairs={{0,3},{1,0},{2,1},{3,2},{4,7},{5,4},{6,5},{7,6},{8,11},{9,8},{10,9... | collective-permute-start | bytes 4718600 | tf_op jit(solution)/shard_map/ppermute | solution.py:49
  49.4 0.1 pad_maximum_fusion
  49.6 0.8 fusion.33
  50.4 0.3 fusion.2
  50.7 2.4 %collective-permute-start.10 = (bf16[3072,256]{1,0:T(8,128)(2,1)}, bf16[3072,256]{1,0:T(8,128)(2,1)}, u32[]{:S(2)}, u32[]{:S(2)}) collective-permute-start(bf16[3072,256]{1,0:T(8,128)(2,1)} %collective-permute-done.8.refs_5_), channel_id=1, source_target_pairs={{0,3},{1,0},{2,1},{3,2},{4,7},{5,4},{6,5},{7,6},{8,11},{9,8},{10,9... | collective-permute-start | bytes 4718600 | tf_op jit(solution)/shard_map/ppermute | solution.py:49
  53.1 1.4 collective-permute-done.5.refs_2_
  54.4 1.9 %collective-permute-start.9 = (bf16[3072,256]{1,0:T(8,128)(2,1)}, bf16[3072,256]{1,0:T(8,128)(2,1)}, u32[]{:S(2)}, u32[]{:S(2)}) collective-permute-start(bf16[3072,256]{1,0:T(8,128)(2,1)} %collective-permute-done.5.refs_2_), channel_id=1, source_target_pairs={{0,1},{1,2},{2,3},{3,0},{4,5},{5,6},{6,7},{7,4},{8,9},{9,10},{10,1... | collective-permute-start | bytes 4718600 | tf_op jit(solution)/shard_map/ppermute | solution.py:49
  56.4 0.4 fusion.3
  56.8 0.1 fusion.30
  56.9 0.1 fusion.21
  56.9 0.1 copy.21
  57.0 9.3 %all-to-all-done = bf16[32,8,512]{2,1,0:T(8,128)(2,1)S(1)} async-done(((bf16[32,8,512]{2,1,0:T(8,128)(2,1)}), bf16[32,8,512]{2,1,0:T(8,128)(2,1)S(1)}, u32[]{:S(2)}, u32[]{:S(2)}) %all-to-all-start) | async-done | bytes 262176 | tf_op jit(solution)/shard_map/all_to_all | solution.py:386
  66.4 1.2 broadcast_in_dim.6
  67.5 4.9 %all-to-all-start.1 = ((bf16[4,320,512]{2,1,0:T(8,128)(2,1)}), bf16[4,320,512]{2,1,0:T(8,128)(2,1)S(1)}, u32[]{:S(2)}, u32[]{:S(2)}) async-start(bf16[4,320,512]{2,1,0:T(8,128)(2,1)} %broadcast_in_dim.6), calls=%async_computation.1 | async-start | bytes 2621440 | tf_op jit(solution)/shard_map/all_to_all | solution.py:395
  72.5 14.8 %all-to-all-done.1.x_ref = bf16[4,320,512]{2,1,0:T(8,128)(2,1)S(1)} async-done(((bf16[4,320,512]{2,1,0:T(8,128)(2,1)}), bf16[4,320,512]{2,1,0:T(8,128)(2,1)S(1)}, u32[]{:S(2)}, u32[]{:S(2)}) %all-to-all-start.1) | async-done | bytes 1310752 | tf_op jit(solution)/shard_map/all_to_all | solution.py:395
  87.2 3.5 %collective-permute-done.10.refs_7_ = bf16[3072,256]{1,0:T(8,128)(2,1)} collective-permute-done((bf16[3072,256]{1,0:T(8,128)(2,1)}, bf16[3072,256]{1,0:T(8,128)(2,1)}, u32[]{:S(2)}, u32[]{:S(2)}) %collective-permute-start.10) | collective-permute-done | bytes 1572896 | tf_op jit(solution)/shard_map/ppermute | solution.py:49
  90.7 5.8 %ffn.1 = bf16[16,256,128]{2,1,0:T(8,128)(2,1)S(1)} custom-call(bf16[4,320,512]{2,1,0:T(8,128)(2,1)S(1)} %all-to-all-done.1.x_ref, bf16[3072,256]{1,0:T(8,128)(2,1)S(1)} %pack.1.refs_0_, bf16[3072,256]{1,0:T(8,128)(2,1)} %get-tuple-element.6.refs_1_, bf16[3072,256]{1,0:T(8,128)(2,1)} %collective-permute-done.5.refs_2_, ...), custom_call_target="tpu_custom_call" | custom-call | tf_op jit(solution)/shard_map/ffn/pallas_call | solution.py:218
  96.5 24.2 %all_to_all.27 = bf16[16,256,128]{2,1,0:T(8,128)(2,1)S(1)} all-to-all(bf16[16,256,128]{2,1,0:T(8,128)(2,1)S(1)} %ffn.1), channel_id=1, replica_groups={{0,1,2,3,4,5,6,7,8,9,10,11,12,13,14,15},{16,20,24,28,17,21,25,29,18,22,..., dimensions={0} | all-to-all | bytes 2097152 | tf_op jit(solution)/shard_map/all_to_all | solution.py:400
  120.8 0.2 reduce_sum.22
  121.0 0.7 copy_bitcast_fusion
  121.7 13.3 %all-to-all-start.3 = ((bf16[32,32,128]{2,1,0:T(8,128)(2,1)}), bf16[32,32,128]{2,1,0:T(8,128)(2,1)S(1)}, u32[]{:S(2)}, u32[]{:S(2)}) async-start(bf16[32,32,128]{2,1,0:T(8,128)(2,1)} %copy_bitcast_fusion), calls=%async_computation.3 | async-start | bytes 524288 | tf_op jit(solution)/shard_map/all_to_all | solution.py:405
  135.1 1.9 %collective-permute-start.2 = (bf16[4,64,512]{2,1,0:T(8,128)(2,1)S(1)}, bf16[4,64,512]{2,1,0:T(8,128)(2,1)S(1)}, u32[]{:S(2)}, u32[]{:S(2)}) collective-permute-start(bf16[4,64,512]{2,1,0:T(8,128)(2,1)S(1)} %slice.82.own_ref), channel_id=1, source_target_pairs={{0,1},{1,2},{2,3},{3,0},{4,5},{5,6},{6,7},{7,4},{8,9},{9,10},{10,1... | collective-permute-start | bytes 786440 | tf_op jit(solution)/shard_map/ppermute | solution.py:49
  137.0 4.6 %collective-permute-start.3 = (bf16[4,64,512]{2,1,0:T(8,128)(2,1)S(1)}, bf16[4,64,512]{2,1,0:T(8,128)(2,1)S(1)}, u32[]{:S(2)}, u32[]{:S(2)}) collective-permute-start(bf16[4,64,512]{2,1,0:T(8,128)(2,1)S(1)} %slice.82.own_ref), channel_id=1, source_target_pairs={{0,3},{1,0},{2,1},{3,2},{4,7},{5,4},{6,5},{7,6},{8,11},{9,8},{10,9... | collective-permute-start | bytes 786440 | tf_op jit(solution)/shard_map/ppermute | solution.py:49
  141.6 1.9 %collective-permute-start.4 = (bf16[4,64,512]{2,1,0:T(8,128)(2,1)S(1)}, bf16[4,64,512]{2,1,0:T(8,128)(2,1)S(1)}, u32[]{:S(2)}, u32[]{:S(2)}) collective-permute-start(bf16[4,64,512]{2,1,0:T(8,128)(2,1)S(1)} %slice.82.own_ref), channel_id=1, source_target_pairs={{0,2},{1,3},{2,0},{3,1},{4,6},{5,7},{6,4},{7,5},{8,10},{9,11},{10,... | collective-permute-start | bytes 786440 | tf_op jit(solution)/shard_map/ppermute | solution.py:49
  143.5 0.1 copy.23.weight_ref
  143.7 4.0 %collective-permute-done.3.next_ref = bf16[4,64,512]{2,1,0:T(8,128)(2,1)S(1)} collective-permute-done((bf16[4,64,512]{2,1,0:T(8,128)(2,1)S(1)}, bf16[4,64,512]{2,1,0:T(8,128)(2,1)S(1)}, u32[]{:S(2)}, u32[]{:S(2)}) %collective-permute-start.3) | collective-permute-done | bytes 262176 | tf_op jit(solution)/shard_map/ppermute | solution.py:49
  147.7 2.8 %collective-permute-done.4.far_ref = bf16[4,64,512]{2,1,0:T(8,128)(2,1)S(1)} collective-permute-done((bf16[4,64,512]{2,1,0:T(8,128)(2,1)S(1)}, bf16[4,64,512]{2,1,0:T(8,128)(2,1)S(1)}, u32[]{:S(2)}, u32[]{:S(2)}) %collective-permute-start.4) | collective-permute-done | bytes 262176 | tf_op jit(solution)/shard_map/ppermute | solution.py:49
  150.5 1.3 project.1
  151.7 5.5 %all-to-all-done.3 = bf16[32,32,128]{2,1,0:T(8,128)(2,1)S(1)} async-done(((bf16[32,32,128]{2,1,0:T(8,128)(2,1)}), bf16[32,32,128]{2,1,0:T(8,128)(2,1)S(1)}, u32[]{:S(2)}, u32[]{:S(2)}) %all-to-all-start.3) | async-done | bytes 262176 | tf_op jit(solution)/shard_map/all_to_all | solution.py:405
  157.3 1.1 combine.1
  (33 shorter events, 0.2 us)
Async XLA Ops:
  0.6 18.3 %copy-start = (bf16[512,256]{1,0:T(8,128)(2,1)S(1)}, bf16[512,256]{1,0:T(8,128)(2,1)}, u32[]{:S(2)}) copy-start(bf16[512,256]{1,0:T(8,128)(2,1)} %param.14) | copy-start | bytes 786436
  0.6 1.3 copy-start.1
  1.9 1.2 copy-start.3
  3.1 1.2 copy-start.4
  4.4 0.7 copy-start.6
  5.1 0.7 copy-start.7
  5.7 10.8 %copy-start.2 = (bf16[1,2048,256]{2,1,0:T(8,128)(2,1)S(1)}, bf16[1,2048,256]{2,1,0:T(8,128)(2,1)}, u32[]{:S(2)}) copy-start(bf16[1,2048,256]{2,1,0:T(8,128)(2,1)} %gate_ref.1) | copy-start | bytes 3145732
  9.0 9.8 %copy-start.8 = (bf16[512,64]{0,1:T(8,128)(2,1)S(1)}, bf16[512,64]{0,1:T(8,128)(2,1)}, u32[]{:S(2)}) copy-start(bf16[512,64]{0,1:T(8,128)(2,1)} %param.12) | copy-start | bytes 196612
  9.0 10.1 %copy-start.9 = (bf16[512,256]{1,0:T(8,128)(2,1)S(1)}, bf16[512,256]{1,0:T(8,128)(2,1)}, u32[]{:S(2)}) copy-start(bf16[512,256]{1,0:T(8,128)(2,1)} %param.13) | copy-start | bytes 786436
  9.0 41.7 %collective-permute-start.8 = (bf16[3072,256]{1,0:T(8,128)(2,1)}, bf16[3072,256]{1,0:T(8,128)(2,1)}, u32[]{:S(2)}, u32[]{:S(2)}) collective-permute-start(bf16[3072,256]{1,0:T(8,128)(2,1)} %get-tuple-element.6.refs_1_), channel_id=1, source_target_pairs={{0,3},{1,0},{2,1},{3,2},{4,7},{5,4},{6,5},{7,6},{8,11},{9,8},{10,9... | collective-permute-start | bytes 4718600 | tf_op jit(solution)/shard_map/ppermute | solution.py:49
  14.6 57.9 %collective-permute-start.6 = (bf16[3072,256]{1,0:T(8,128)(2,1)}, bf16[3072,256]{1,0:T(8,128)(2,1)}, u32[]{:S(2)}, u32[]{:S(2)}) collective-permute-start(bf16[3072,256]{1,0:T(8,128)(2,1)} %get-tuple-element.6.refs_1_), channel_id=1, source_target_pairs={{0,1},{1,2},{2,3},{3,0},{4,5},{5,6},{6,7},{7,4},{8,9},{9,10},{10,1... | collective-permute-start | bytes 4718600 | tf_op jit(solution)/shard_map/ppermute | solution.py:49
  16.8 37.6 %collective-permute-start.5 = (bf16[3072,256]{1,0:T(8,128)(2,1)S(1)}, bf16[3072,256]{1,0:T(8,128)(2,1)}, u32[]{:S(2)}, u32[]{:S(2)}) collective-permute-start(bf16[3072,256]{1,0:T(8,128)(2,1)S(1)} %pack.1.refs_0_), channel_id=1, source_target_pairs={{0,1},{1,2},{2,3},{3,0},{4,5},{5,6},{6,7},{7,4},{8,9},{9,10},{10,1... | collective-permute-start | bytes 4718600 | tf_op jit(solution)/shard_map/ppermute | solution.py:49
  20.6 24.2 %collective-permute-start = (bf16[2,128,1,64]{3,1,2,0:T(8,128)(2,1)S(1)}, bf16[2,128,1,64]{3,1,2,0:T(8,128)(2,1)S(1)}, u32[]{:S(2)}, u32[]{:S(2)}) collective-permute-start(bf16[2,128,1,64]{3,1,2,0:T(8,128)(2,1)S(1)} %get-tuple-element.8), channel_id=1, source_target_pairs={{0,16},{16,32},{32,48},{48,64},{64,80},{80,96},{96,112},{112,128},... | collective-permute-start | bytes 98312 | tf_op jit(solution)/shard_map/ppermute | solution.py:292
  25.5 24.0 %collective-permute-start.1 = (bf16[2,128,1,64]{3,1,2,0:T(8,128)(2,1)S(1)}, bf16[2,128,1,64]{3,1,2,0:T(8,128)(2,1)S(1)}, u32[]{:S(2)}, u32[]{:S(2)}) collective-permute-start(bf16[2,128,1,64]{3,1,2,0:T(8,128)(2,1)S(1)} %get-tuple-element.9), channel_id=1, source_target_pairs={{16,0},{32,16},{48,32},{64,48},{80,64},{96,80},{112,96},{128,112},... | collective-permute-start | bytes 98312 | tf_op jit(solution)/shard_map/ppermute | solution.py:295
  29.1 37.2 %all-to-all-start = ((bf16[32,8,512]{2,1,0:T(8,128)(2,1)}), bf16[32,8,512]{2,1,0:T(8,128)(2,1)S(1)}, u32[]{:S(2)}, u32[]{:S(2)}) async-start(bf16[32,8,512]{2,1,0:T(8,128)(2,1)} %bitcast.2), calls=%async_computation | async-start | bytes 524288 | tf_op jit(solution)/shard_map/all_to_all | solution.py:386
  44.8 27.7 %collective-permute-start.7 = (bf16[3072,256]{1,0:T(8,128)(2,1)S(1)}, bf16[3072,256]{1,0:T(8,128)(2,1)}, u32[]{:S(2)}, u32[]{:S(2)}) collective-permute-start(bf16[3072,256]{1,0:T(8,128)(2,1)S(1)} %pack.1.refs_0_), channel_id=1, source_target_pairs={{0,3},{1,0},{2,1},{3,2},{4,7},{5,4},{6,5},{7,6},{8,11},{9,8},{10,9... | collective-permute-start | bytes 4718600 | tf_op jit(solution)/shard_map/ppermute | solution.py:49
  50.7 40.0 %collective-permute-start.10 = (bf16[3072,256]{1,0:T(8,128)(2,1)}, bf16[3072,256]{1,0:T(8,128)(2,1)}, u32[]{:S(2)}, u32[]{:S(2)}) collective-permute-start(bf16[3072,256]{1,0:T(8,128)(2,1)} %collective-permute-done.8.refs_5_), channel_id=1, source_target_pairs={{0,3},{1,0},{2,1},{3,2},{4,7},{5,4},{6,5},{7,6},{8,11},{9,8},{10,9... | collective-permute-start | bytes 4718600 | tf_op jit(solution)/shard_map/ppermute | solution.py:49
  54.4 36.3 %collective-permute-start.9 = (bf16[3072,256]{1,0:T(8,128)(2,1)}, bf16[3072,256]{1,0:T(8,128)(2,1)}, u32[]{:S(2)}, u32[]{:S(2)}) collective-permute-start(bf16[3072,256]{1,0:T(8,128)(2,1)} %collective-permute-done.5.refs_2_), channel_id=1, source_target_pairs={{0,1},{1,2},{2,3},{3,0},{4,5},{5,6},{6,7},{7,4},{8,9},{9,10},{10,1... | collective-permute-start | bytes 4718600 | tf_op jit(solution)/shard_map/ppermute | solution.py:49
  67.5 19.7 %all-to-all-start.1 = ((bf16[4,320,512]{2,1,0:T(8,128)(2,1)}), bf16[4,320,512]{2,1,0:T(8,128)(2,1)S(1)}, u32[]{:S(2)}, u32[]{:S(2)}) async-start(bf16[4,320,512]{2,1,0:T(8,128)(2,1)} %broadcast_in_dim.6), calls=%async_computation.1 | async-start | bytes 2621440 | tf_op jit(solution)/shard_map/all_to_all | solution.py:395
  120.8 22.7 %copy-start.10 = (f32[256,2]{0,1:T(2,128)S(1)}, f32[256,2]{0,1:T(2,128)}, u32[]{:S(2)}) copy-start(f32[256,2]{0,1:T(2,128)} %param.20) | copy-start | bytes 6148
  120.8 29.7 %copy-start.5 = (bf16[1024,128]{1,0:T(8,128)(2,1)S(1)}, bf16[1024,128]{1,0:T(8,128)(2,1)}, u32[]{:S(2)}) copy-start(bf16[1024,128]{1,0:T(8,128)(2,1)} %weight_ref.2) | copy-start | bytes 786436
  121.7 35.5 %all-to-all-start.3 = ((bf16[32,32,128]{2,1,0:T(8,128)(2,1)}), bf16[32,32,128]{2,1,0:T(8,128)(2,1)S(1)}, u32[]{:S(2)}, u32[]{:S(2)}) async-start(bf16[32,32,128]{2,1,0:T(8,128)(2,1)} %copy_bitcast_fusion), calls=%async_computation.3 | async-start | bytes 524288 | tf_op jit(solution)/shard_map/all_to_all | solution.py:405
  135.1 8.6 %collective-permute-start.2 = (bf16[4,64,512]{2,1,0:T(8,128)(2,1)S(1)}, bf16[4,64,512]{2,1,0:T(8,128)(2,1)S(1)}, u32[]{:S(2)}, u32[]{:S(2)}) collective-permute-start(bf16[4,64,512]{2,1,0:T(8,128)(2,1)S(1)} %slice.82.own_ref), channel_id=1, source_target_pairs={{0,1},{1,2},{2,3},{3,0},{4,5},{5,6},{6,7},{7,4},{8,9},{9,10},{10,1... | collective-permute-start | bytes 786440 | tf_op jit(solution)/shard_map/ppermute | solution.py:49
  137.0 10.7 %collective-permute-start.3 = (bf16[4,64,512]{2,1,0:T(8,128)(2,1)S(1)}, bf16[4,64,512]{2,1,0:T(8,128)(2,1)S(1)}, u32[]{:S(2)}, u32[]{:S(2)}) collective-permute-start(bf16[4,64,512]{2,1,0:T(8,128)(2,1)S(1)} %slice.82.own_ref), channel_id=1, source_target_pairs={{0,3},{1,0},{2,1},{3,2},{4,7},{5,4},{6,5},{7,6},{8,11},{9,8},{10,9... | collective-permute-start | bytes 786440 | tf_op jit(solution)/shard_map/ppermute | solution.py:49
  141.6 8.9 %collective-permute-start.4 = (bf16[4,64,512]{2,1,0:T(8,128)(2,1)S(1)}, bf16[4,64,512]{2,1,0:T(8,128)(2,1)S(1)}, u32[]{:S(2)}, u32[]{:S(2)}) collective-permute-start(bf16[4,64,512]{2,1,0:T(8,128)(2,1)S(1)} %slice.82.own_ref), channel_id=1, source_target_pairs={{0,2},{1,3},{2,0},{3,1},{4,6},{5,7},{6,4},{7,5},{8,10},{9,11},{10,... | collective-permute-start | bytes 786440 | tf_op jit(solution)/shard_map/ppermute | solution.py:49

commit v5 on v4

v5 whole, which is shorter than its diff:
```python
import jax
import jax.numpy as jnp
from jax import lax
from jax.experimental import pallas as pl
from jax.experimental.pallas import tpu as pltpu
from jax.sharding import Mesh
from jax.sharding import PartitionSpec as P


D = 2048
HEAD_DIM = 64
HALF_WIN = 128
ROWS_B = 256
EXPERTS = 32
CAP = 32
EP = ("z", "co")
TP = ("y", "x")
PLANE = ("co", "y", "x")

NORM_EPS = 1e-06
ROPE_BASE = 10000.0
NEG_BIG = -1e30

LINE_L = [[y * 4 + x for x in range(4)] for y in range(4)] + [
    [16 + y * 4 + x for y in range(4)] for x in range(4)
]
LINE_M = [[y * 4 + x for y in range(4)] for x in range(4)] + [
    [16 + y * 4 + x for x in range(4)] for y in range(4)
]
WHOLE = [list(range(16)), [16 + (p % 4) * 4 + p // 4 for p in range(16)]]


ANY = pl.BlockSpec(memory_space=pl.ANY)
VMEM = pl.BlockSpec(memory_space=pltpu.VMEM)
HALF_W = 3072


def resident(x):
    return pltpu.with_memory_space_constraint(x, pltpu.VMEM)


def vmem_mib(count):
    return pltpu.CompilerParams(vmem_limit_bytes=count << 20)


def line_shift(x, step):
    pairs = [(line[i], line[(i + step) % 4]) for line in LINE_L for i in range(4)]
    return lax.ppermute(x, PLANE, pairs)


def pack_kernel(pieces, *refs):
    sources, out_ref, stage_ref, sems = refs[:-3], refs[-3], refs[-2], refs[-1]
    copies, leave = [], []
    for i, (which, rows, cols, at) in enumerate(pieces):
        source = sources[which].at[0, pl.ds(*rows), pl.ds(*cols)]
        part = pl.ds(at, rows[1])
        copies.append(pltpu.make_async_copy(source, stage_ref.at[part], sems.at[0, i]))
        leave.append(
            pltpu.make_async_copy(stage_ref.at[part], out_ref.at[part], sems.at[1, i])
        )
    for copy in copies:
        copy.start()
    for come, go in zip(copies, leave):
        come.wait()
        go.start()
    for go in leave:
        go.wait()


def pack(pieces, *sources):
    def body(*refs):
        pack_kernel(pieces, *refs)

    return pl.pallas_call(
        body,
        out_shape=jax.ShapeDtypeStruct((HALF_W, 256), jnp.bfloat16),
        in_specs=[ANY] * len(sources),
        out_specs=ANY,
        scratch_shapes=[
            pltpu.VMEM((HALF_W, 256), jnp.bfloat16),
            pltpu.SemaphoreType.DMA((2, len(pieces))),
        ],
        compiler_params=vmem_mib(4),
        name="pack",
    )(*sources)


PIECES_A = ((0, (0, 2048), (0, 256), 0), (1, (0, 1024), (0, 256), 2048))
PIECES_B = ((0, (1024, 1024), (0, 256), 0),) + tuple(
    (1, (0, 256), (c * 256, 256), 1024 + c * 256) for c in range(8)
)


def prep_kernel(x_ref, gain_ref, routes_ref, out_ref, slot_ref, normed_ref):
    def norm_rows(i, carry):
        rows = pl.ds(pl.multiple_of(i * 32, 32), 32)
        wide = x_ref[rows, :].astype(jnp.float32)
        scale = lax.rsqrt(jnp.mean(wide * wide, axis=1, keepdims=True) + NORM_EPS)
        normed_ref[rows, :] = (wide * scale * gain_ref[...]).astype(jnp.bfloat16)
        return carry

    lax.fori_loop(0, ROWS_B // 32, norm_rows, 0)

    first = routes_ref[0:1, :]
    second = routes_ref[1:2, :]
    expert = lax.broadcasted_iota(jnp.int32, (128, ROWS_B), 0)
    row = lax.broadcasted_iota(jnp.int32, (ROWS_B, ROWS_B), 0)
    col = lax.broadcasted_iota(jnp.int32, (ROWS_B, ROWS_B), 1)
    above = jnp.where(row < col, 1.0, 0.0).astype(jnp.bfloat16)
    named = jnp.where((first == expert) | (second == expert), 1.0, 0.0)
    rank = jnp.dot(named.astype(jnp.bfloat16), above, preferred_element_type=jnp.float32)
    rank_a = jnp.sum(jnp.where(first == expert, rank, 0.0), axis=0, keepdims=True)
    rank_b = jnp.sum(jnp.where(second == expert, rank, 0.0), axis=0, keepdims=True)
    slot_a = first * CAP + rank_a.astype(jnp.int32)
    slot_b = second * CAP + rank_b.astype(jnp.int32)
    both = jnp.where(expert == 0, slot_a, slot_b).astype(jnp.float32)
    slot_ref[...] = both.T.astype(jnp.int32)

    mark = jnp.where(named > 0.5, rank, -1.0).astype(jnp.bfloat16)
    spread = jnp.where(
        (lax.broadcasted_iota(jnp.int32, (ROWS_B, 128), 0) >> 3)
        == lax.broadcasted_iota(jnp.int32, (ROWS_B, 128), 1),
        1.0,
        0.0,
    ).astype(jnp.bfloat16)
    mark_rows = jnp.dot(spread, mark, preferred_element_type=jnp.float32)
    xi = lax.axis_index("x")
    yi = lax.axis_index("y")
    even = ((row >> 3) & 1) == 0
    wanted = jnp.where(even, xi, yi) * 8 + (row & 7)
    pick = jnp.where(mark_rows.astype(jnp.int32) == wanted, 1.0, 0.0).astype(jnp.bfloat16)
    from_y = jnp.dot(
        pick, normed_ref[:, pl.ds(pl.multiple_of(yi * 512, 512), 512)],
        preferred_element_type=jnp.float32,
    )
    from_x = jnp.dot(
        pick, normed_ref[:, pl.ds(pl.multiple_of(xi * 512, 512), 512)],
        preferred_element_type=jnp.float32,
    )
    even_row = ((lax.broadcasted_iota(jnp.int32, (ROWS_B, 512), 0) >> 3) & 1) == 0
    out_ref[...] = jnp.where(even_row, from_y, from_x).astype(jnp.bfloat16)


def prepare(expert_input, norm_gain, routes):
    return pl.pallas_call(
        prep_kernel,
        out_shape=(
            jax.ShapeDtypeStruct((ROWS_B, 512), jnp.bfloat16),
            jax.ShapeDtypeStruct((ROWS_B, 128), jnp.int32),
        ),
        in_specs=[VMEM] * 3,
        out_specs=(VMEM, VMEM),
        scratch_shapes=[pltpu.VMEM((ROWS_B, D), jnp.bfloat16)],
        compiler_params=vmem_mib(16),
        name="prep",
    )(expert_input, norm_gain.reshape(1, D), routes.T)


def slice_hidden(x_ref, wa, wb):
    def part(m, ref, start):
        return jnp.dot(
            x_ref[m, pl.ds(0, ROWS_B), :], ref[pl.ds(start, 512), :],
            preferred_element_type=jnp.float32,
        )

    gate = part(0, wa, 0) + part(1, wa, 512) + part(2, wa, 1024) + part(3, wa, 1536)
    up = part(0, wa, 2048) + part(1, wa, 2560) + part(2, wb, 0) + part(3, wb, 512)
    return (gate / (1.0 + jnp.exp(-gate)) * up).astype(jnp.bfloat16)


def ffn_kernel(x_ref, *refs):
    weights, out_ref, acc_ref, bufs, sems, piece_ref, out_sems = refs[:8], *refs[8:]
    leave = []
    copies = [
        pltpu.make_async_copy(w, bufs.at[i], sems.at[i]) for i, w in enumerate(weights)
    ]
    for copy in copies:
        copy.start()
    core = lax.axis_index("co")
    for s in range(4):
        copies[2 * s].wait()
        copies[2 * s + 1].wait()
        wa, wb = bufs.at[2 * s], bufs.at[2 * s + 1]
        hidden = slice_hidden(x_ref, wa, wb)
        for c in range(8):
            cols = pl.ds(c * 256, 256)
            term = jnp.dot(
                hidden, wb[pl.ds(1024 + c * 256, 256), :], preferred_element_type=jnp.float32
            )
            total = term if s == 0 else acc_ref[:, cols] + term
            if s < 3:
                acc_ref[:, cols] = total
                continue
            for k in range(2):
                t = 2 * c + k
                place = jnp.where(core == 0, t, (t % 4) * 4 + t // 4)
                piece = total[:, k * 128 : (k + 1) * 128].astype(jnp.bfloat16)
                piece_ref[t] = piece
                leave.append(
                    pltpu.make_async_copy(piece_ref.at[t], out_ref.at[place], out_sems.at[t])
                )
                leave[-1].start()
    for copy in leave:
        copy.wait()


def ffn(x, weights):
    return pl.pallas_call(
        ffn_kernel,
        out_shape=pltpu.HBM((16, ROWS_B, 128), jnp.bfloat16),
        in_specs=[VMEM] + [ANY] * 8,
        out_specs=pl.BlockSpec(memory_space=pltpu.HBM),
        scratch_shapes=[
            pltpu.VMEM((ROWS_B, D), jnp.float32),
            pltpu.VMEM((8, HALF_W, 256), jnp.bfloat16),
            pltpu.SemaphoreType.DMA((8,)),
            pltpu.VMEM((16, ROWS_B, 128), jnp.bfloat16),
            pltpu.SemaphoreType.DMA((16,)),
        ],
        compiler_params=vmem_mib(24),
        name="ffn",
    )(resident(x), *weights)


def combine_kernel(ret_ref, slot_ref, weight_ref, out_ref):
    place = lax.broadcasted_iota(jnp.int32, (ROWS_B, EXPERTS * CAP), 1)
    total = None
    for k in range(2):
        pick = jnp.where(place == slot_ref[:, k : k + 1], 1.0, 0.0).astype(jnp.bfloat16)
        rows = jnp.dot(pick, ret_ref[...], preferred_element_type=jnp.float32)
        term = rows * weight_ref[:, k : k + 1]
        total = term if total is None else total + term
    out_ref[...] = total.astype(jnp.bfloat16)


def combine(returned, slots, route_weights):
    return pl.pallas_call(
        combine_kernel,
        out_shape=jax.ShapeDtypeStruct((ROWS_B, 128), jnp.bfloat16),
        in_specs=[VMEM] * 3,
        out_specs=VMEM,
        compiler_params=vmem_mib(12),
        name="combine",
    )(resident(returned), slots, route_weights)


def project_kernel(own_ref, prev_ref, next_ref, far_ref, weight_ref, out_ref, a_ref):
    core = lax.axis_index("co")
    line = jnp.where(core == 0, lax.axis_index("x"), lax.axis_index("y"))
    for ref, step in ((own_ref, 0), (prev_ref, 3), (next_ref, 1), (far_ref, 2)):
        source = lax.rem(line + step, 4)
        for m in range(4):
            head = jnp.where(core == 0, m * 4 + source, source * 4 + m)
            a_ref[pl.ds(pl.multiple_of(head * HEAD_DIM, HEAD_DIM), HEAD_DIM), :] = ref[m]
    turned = weight_ref[...].astype(jnp.float32).T.astype(jnp.bfloat16)
    out = jnp.dot(turned, a_ref[...], preferred_element_type=jnp.float32)
    out_ref[...] = out.T.astype(jnp.bfloat16)


def project(own, prev, nxt, far, out_weight):
    return pl.pallas_call(
        project_kernel,
        out_shape=jax.ShapeDtypeStruct((512, 128), jnp.bfloat16),
        in_specs=[VMEM] * 5,
        out_specs=VMEM,
        scratch_shapes=[pltpu.VMEM((1024, 512), jnp.bfloat16)],
        compiler_params=vmem_mib(12),
        name="project",
    )(*(resident(a) for a in (own, prev, nxt, far, out_weight)))


def attend_kernel(q_ref, kv_ref, low_ref, high_ref, cos_ref, sin_ref, sink_ref, out_ref,
                  k_scr, vt_scr):
    half = HEAD_DIM // 2

    def turn(x, rows):
        wide = x.astype(jnp.float32)
        swapped = jnp.concatenate([wide[:, half:], wide[:, :half]], axis=1)
        return (wide * cos_ref[rows, :] + swapped * sin_ref[rows, :]).astype(jnp.bfloat16)

    spans = ((low_ref, 0, HALF_WIN), (kv_ref, HALF_WIN, 512), (high_ref, 512 + HALF_WIN, HALF_WIN))
    for ref, at, count in spans:
        rows = pl.ds(at, count)
        k_scr[rows, :] = turn(ref[0], rows)
        value = ref[1].astype(jnp.float32)
        vt_scr[:, rows] = jnp.concatenate([value, value], axis=1).T.astype(jnp.bfloat16)
    start = (lax.axis_index("z") * 2 + lax.axis_index("co")) * 512
    key_at = lax.broadcasted_iota(jnp.int32, (384, 128), 0) - HALF_WIN
    gap = key_at - lax.broadcasted_iota(jnp.int32, (384, 128), 1)
    sink = sink_ref[0]
    for j in range(4):
        query = turn(q_ref[pl.ds(j * 128, 128), :], pl.ds(HALF_WIN + j * 128, 128))
        scores = lax.dot_general(
            k_scr[pl.ds(j * 128, 384), :], query, (((1,), (1,)), ((), ())),
            preferred_element_type=jnp.float32,
        ) * HEAD_DIM ** (-0.5)
        key = key_at + (start + j * 128)
        allowed = (jnp.abs(gap) <= HALF_WIN) & (key >= 0) & (key < 16384)
        scores = jnp.where(allowed, scores, NEG_BIG)
        peak = jnp.maximum(jnp.max(scores, axis=0, keepdims=True), sink)
        lifted = jnp.exp(scores - peak)
        total = jnp.sum(lifted, axis=0, keepdims=True) + jnp.exp(sink - peak)
        probs = (lifted / total).astype(jnp.bfloat16)
        mixed = jnp.dot(
            vt_scr[pl.ds(0, HEAD_DIM), pl.ds(j * 128, 384)], probs,
            preferred_element_type=jnp.float32,
        )
        out_ref[:, pl.ds(j * 128, 128)] = mixed.astype(jnp.bfloat16)


def attend(query_proj, key_proj, value_proj, sink_logit):
    kv_at = lax.axis_index("y") * HEAD_DIM
    own = jnp.stack(
        [lax.dynamic_slice_in_dim(a, kv_at, HEAD_DIM, 1) for a in (key_proj, value_proj)]
    )
    count = lax.axis_size(EP)
    forward = [(i, i + 1) for i in range(count - 1)]
    backward = [(target, source) for source, target in forward]
    low = lax.ppermute(own[:, 512 - HALF_WIN :], EP, forward)
    high = lax.ppermute(own[:, :HALF_WIN], EP, backward)
    offset = lax.axis_index(EP) * 512 - HALF_WIN
    half = HEAD_DIM // 2
    channel = jnp.arange(HEAD_DIM, dtype=jnp.int32)
    inverse_freq = 1.0 / ROPE_BASE ** ((channel % half).astype(jnp.float32) * 2.0 / HEAD_DIM)
    position = (jnp.arange(512 + 2 * HALF_WIN, dtype=jnp.int32) + offset).astype(jnp.float32)
    angles = position[:, None] * inverse_freq[None, :]
    cosine = jnp.cos(angles)
    sine = jnp.where(channel < half, -1.0, 1.0)[None, :] * jnp.sin(angles)
    return pl.pallas_call(
        attend_kernel,
        out_shape=jax.ShapeDtypeStruct((HEAD_DIM, 512), jnp.bfloat16),
        in_specs=[VMEM] * 6 + [pl.BlockSpec(memory_space=pltpu.SMEM)],
        out_specs=VMEM,
        scratch_shapes=[
            pltpu.VMEM((768, HEAD_DIM), jnp.bfloat16), pltpu.VMEM((128, 768), jnp.bfloat16)
        ],
        compiler_params=vmem_mib(12),
        name="attend",
    )(*(resident(a) for a in (query_proj, own, low, high, cosine, sine)), sink_logit)


def local(
    query_proj,
    key_proj,
    value_proj,
    sink_logit,
    out_weight,
    expert_input,
    norm_gain,
    routes,
    route_weights,
    gate_weight,
    up_weight,
    down_weight,
):
    wa = pack(PIECES_A, gate_weight, up_weight)
    prev_a = line_shift(wa, 1)
    wb = pack(PIECES_B, up_weight, down_weight)
    next_b = line_shift(wb, -1)
    outgoing, slots = prepare(expert_input, norm_gain, routes)
    next_a = line_shift(wa, -1)
    prev_b = line_shift(wb, 1)
    arrived = lax.all_to_all(outgoing, EP, 0, 0, tiled=True)
    far_a = line_shift(prev_a, 1)
    far_b = line_shift(next_b, -1)

    attended = attend(query_proj, key_proj, value_proj, sink_logit)

    payload = jnp.concatenate([arrived, attended], axis=0)
    rows = lax.all_to_all(
        jnp.broadcast_to(payload[None], (4, *payload.shape)),
        PLANE, 0, 0, tiled=True, axis_index_groups=LINE_M,
    )
    partial = ffn(rows, (wa, wb, prev_a, prev_b, next_a, next_b, far_a, far_b))
    parts = lax.all_to_all(partial, PLANE, 0, 0, tiled=True, axis_index_groups=WHOLE)
    parts = parts.reshape(4, 4, 256, 128)
    result = jnp.sum(parts.astype(jnp.float32), axis=0).astype(jnp.bfloat16)
    result = jnp.moveaxis(result.reshape(4, EXPERTS, 8, 128), 0, 1)
    result = result.reshape(EXPERTS, CAP, 128)
    returned = lax.all_to_all(result, EP, 0, 0, tiled=True)
    expert_out = combine(returned.reshape(EXPERTS * CAP, 128), slots, route_weights)

    heads = rows[:, 256:]
    around = [line_shift(heads, step) for step in (1, -1, 2)]
    mixer_out = project(heads, *around, out_weight)
    return (mixer_out, expert_out)


def solution(mesh):
    finer = Mesh(mesh.devices.reshape(16, 2, 4, 4), ("z", "co", "y", "x"))
    in_specs = (
        P(EP, TP),
        P(EP, None),
        P(EP, None),
        P(TP),
        P(None, TP),
        P(EP, None),
        P(),
        P(EP, None),
        P(EP, None),
        P(EP, None, TP),
        P(EP, None, TP),
        P(EP, TP, None),
    )
    out_specs = (P(EP, TP), P(EP, TP))
    return jax.shard_map(local, mesh=finer, in_specs=in_specs, out_specs=out_specs, check_vma=False)
```

time: 159 us -> 150 us (0.943)
  waiting for transfers between devices: 41.3 us -> 33.6 us
  Pallas kernels: 11.6 us -> 15.6 us
  local copies, waits for them, and re-layouts: 7.52 us -> 4.83 us
  blocking collectives: 24.2 us -> 22.1 us
    all_to_all x1, waiting for transfers between devices: 9.29 us -> 0.01 us  [local(): arrived = lax.all_to_all(outgoing, EP, 0, 0, tiled=True)]
    pallas_call x2 -> x4, Pallas kernels: 6.03 us -> 11 us  [the longest x1 6.57 us: ffn(): pl.pallas_call(ffn_kernel, out_shape=pltpu.HBM((16, ROWS_B, 128), jnp.bfl...]
    ppermute x9, waiting for transfers between devices: 11.7 us -> 7.32 us  [line_shift(): return lax.ppermute(x, PLANE, pairs)]
    ppermute x2, waiting for transfers between devices: 0.01 us -> 3.2 us  [the longest x1 3.2 us: attend(): high = lax.ppermute(own[:, :HALF_WIN], EP, backward)]
    all_to_all x1, waiting for transfers between devices: 14.8 us -> 17.4 us  [local(): lax.all_to_all(jnp.broadcast_to(payload[None], (4, *payload.shape)), PLAN...]
    unnamed x24 -> x26, local copies, waits for them, and re-layouts: 5.37 us -> 2.74 us
    ppermute x2, starting transfers between devices: 8.5 us -> 5.94 us  [the longest x1 4.02 us: attend(): low = lax.ppermute(own[:, 512 - HALF_WIN:], EP, forward)]
    ppermute x9, starting transfers between devices: 26.8 us -> 29.2 us  [line_shift(): return lax.ppermute(x, PLANE, pairs)]
  transfers between devices with their start and end apart: 14 -> 14, of which waited for: 7 -> 6; matrix products, arithmetic and copies ran while one was open for 3% -> 2% of each run, Pallas kernels for 1% -> 4%
where the time goes in v5:
time: 150 us; the launch traced here: 149 us
  starting transfers between devices  69.2 us (46%)
  waiting for transfers between devices  33.6 us (22%)
  blocking collectives  22.1 us (15%)
  Pallas kernels  15.6 us (10%)
  local copies, waits for them, and re-layouts  4.83 us (3%)
  other arithmetic  1.79 us (1%)
  between operations  1.69 us (1%)
    ppermute x9, starting transfers between devices, line_shift(): return lax.ppermute(x, PLANE, pairs)  29.2 us
    all_to_all x1, blocking collectives, local(): lax.all_to_all(partial, PLANE, 0, 0, tiled=True, axis_index_groups=WHOLE)  22.1 us
    all_to_all x1, waiting for transfers between devices, local(): lax.all_to_all(jnp.broadcast_to(payload[None], (4, *payload.shape)), PLAN...  17.4 us
    all_to_all x1, starting transfers between devices, local(): arrived = lax.all_to_all(outgoing, EP, 0, 0, tiled=True)  16.1 us
    all_to_all x1, starting transfers between devices, local(): returned = lax.all_to_all(result, EP, 0, 0, tiled=True)  14.5 us
    ppermute x9, waiting for transfers between devices, line_shift(): return lax.ppermute(x, PLANE, pairs)  7.32 us
    pallas_call x1, Pallas kernels, ffn(): pl.pallas_call(ffn_kernel, out_shape=pltpu.HBM((16, ROWS_B, 128), jnp.bfl...  6.57 us
    all_to_all x1, waiting for transfers between devices, local(): returned = lax.all_to_all(result, EP, 0, 0, tiled=True)  5.67 us
  transfers between devices with their start and end apart: 14, of which 6 were waited for; matrix products, arithmetic and copies ran while one was open for 2% of the time, Pallas kernels for 4%

profile of v5, /device:TPU:1, one launch (start us, length us, event | category | flops | bytes accessed | tf_op | source)
XLA Modules:
  0.0 148.8 jit_solution(5703897897843673276)
XLA Ops:
  0.6 1.2 copy-done
  1.9 1.2 copy-done.2
  3.1 1.8 %pack.3.refs_1_ = bf16[3072,256]{1,0:T(8,128)(2,1)S(1)} custom-call(bf16[1,2048,256]{2,1,0:T(8,128)(2,1)S(1)} %copy-done, bf16[1,256,2048]{2,1,0:T(8,128)(2,1)S(1)} %copy-done.2), custom_call_target="tpu_custom_call" | custom-call | tf_op jit(solution)/shard_map/pack/pallas_call | solution.py:74
  4.8 0.0 copy-start.4
  4.9 0.0 copy-start.6
  4.9 0.0 copy-start.7
  4.9 5.6 %collective-permute-start.8 = (bf16[3072,256]{1,0:T(8,128)(2,1)S(1)}, bf16[3072,256]{1,0:T(8,128)(2,1)}, u32[]{:S(2)}, u32[]{:S(2)}) collective-permute-start(bf16[3072,256]{1,0:T(8,128)(2,1)S(1)} %pack.3.refs_1_), channel_id=1, source_target_pairs={{0,3},{1,0},{2,1},{3,2},{4,7},{5,4},{6,5},{7,6},{8,11},{9,8},{10,9... | collective-permute-start | bytes 4718600 | tf_op jit(solution)/shard_map/ppermute | solution.py:48
  10.5 1.3 pack.2.refs_0_
  11.9 0.0 copy-start.8
  11.9 0.0 copy-start.9
  11.9 2.1 %collective-permute-start.5 = (bf16[3072,256]{1,0:T(8,128)(2,1)}, bf16[3072,256]{1,0:T(8,128)(2,1)}, u32[]{:S(2)}, u32[]{:S(2)}) collective-permute-start(bf16[3072,256]{1,0:T(8,128)(2,1)} %pack.2.refs_0_), channel_id=1, source_target_pairs={{0,1},{1,2},{2,3},{3,0},{4,5},{5,6},{6,7},{7,4},{8,9},{9,10},{10,1... | collective-permute-start | bytes 4718600 | tf_op jit(solution)/shard_map/ppermute | solution.py:48
  14.0 2.4 %prep.1 = (bf16[256,512]{1,0:T(8,128)(2,1)}, s32[256,128]{1,0:T(8,128)S(1)}) custom-call(bf16[256,2048]{1,0:T(8,128)(2,1)S(1)} %copy-done.4, f32[1,2048]{1,0:T(1,128)S(1)} %bitcast.18, s32[2,256]{1,0:T(2,128)S(1)} %bitcast.19), custom_call_target="tpu_custom_call" | custom-call | tf_op jit(solution)/shard_map/prep/pallas_call | solution.py:145
  16.3 16.1 %all-to-all-start = ((bf16[32,8,512]{2,1,0:T(8,128)(2,1)}), bf16[32,8,512]{2,1,0:T(8,128)(2,1)S(1)}, u32[]{:S(2)}, u32[]{:S(2)}) async-start(bf16[32,8,512]{2,1,0:T(8,128)(2,1)} %bitcast.2), calls=%async_computation | async-start | bytes 524288 | tf_op jit(solution)/shard_map/all_to_all | solution.py:363
  32.4 3.2 %collective-permute-start.6 = (bf16[3072,256]{1,0:T(8,128)(2,1)S(1)}, bf16[3072,256]{1,0:T(8,128)(2,1)}, u32[]{:S(2)}, u32[]{:S(2)}) collective-permute-start(bf16[3072,256]{1,0:T(8,128)(2,1)S(1)} %pack.3.refs_1_), channel_id=1, source_target_pairs={{0,1},{1,2},{2,3},{3,0},{4,5},{5,6},{6,7},{7,4},{8,9},{9,10},{10,1... | collective-permute-start | bytes 4718600 | tf_op jit(solution)/shard_map/ppermute | solution.py:48
  35.6 3.4 %collective-permute-start.7 = (bf16[3072,256]{1,0:T(8,128)(2,1)}, bf16[3072,256]{1,0:T(8,128)(2,1)}, u32[]{:S(2)}, u32[]{:S(2)}) collective-permute-start(bf16[3072,256]{1,0:T(8,128)(2,1)} %pack.2.refs_0_), channel_id=1, source_target_pairs={{0,3},{1,0},{2,1},{3,2},{4,7},{5,4},{6,5},{7,6},{8,11},{9,8},{10,9... | collective-permute-start | bytes 4718600 | tf_op jit(solution)/shard_map/ppermute | solution.py:48
  39.0 0.1 dynamic-slice_bitcast_fusion
  39.2 4.0 %collective-permute-start = (bf16[2,128,64]{2,1,0:T(8,128)(2,1)S(1)}, bf16[2,128,64]{2,1,0:T(8,128)(2,1)S(1)}, u32[]{:S(2)}, u32[]{:S(2)}) collective-permute-start(bf16[2,128,64]{2,1,0:T(8,128)(2,1)S(1)} %get-tuple-element.7), channel_id=1, source_target_pairs={{0,16},{16,32},{32,48},{48,64},{64,80},{80,96},{96,112},{112,128},... | collective-permute-start | bytes 98312 | tf_op jit(solution)/shard_map/ppermute | solution.py:319
  43.3 0.0 collective-permute-done.8.refs_5_
  43.3 4.7 %collective-permute-start.10 = (bf16[3072,256]{1,0:T(8,128)(2,1)}, bf16[3072,256]{1,0:T(8,128)(2,1)}, u32[]{:S(2)}, u32[]{:S(2)}) collective-permute-start(bf16[3072,256]{1,0:T(8,128)(2,1)} %collective-permute-done.8.refs_5_), channel_id=1, source_target_pairs={{0,3},{1,0},{2,1},{3,2},{4,7},{5,4},{6,5},{7,6},{8,11},{9,8},{10,9... | collective-permute-start | bytes 4718600 | tf_op jit(solution)/shard_map/ppermute | solution.py:48
  47.9 0.0 collective-permute-done.5.refs_2_
  48.0 1.9 %collective-permute-start.9 = (bf16[3072,256]{1,0:T(8,128)(2,1)}, bf16[3072,256]{1,0:T(8,128)(2,1)}, u32[]{:S(2)}, u32[]{:S(2)}) collective-permute-start(bf16[3072,256]{1,0:T(8,128)(2,1)} %collective-permute-done.5.refs_2_), channel_id=1, source_target_pairs={{0,1},{1,2},{2,3},{3,0},{4,5},{5,6},{6,7},{7,4},{8,9},{9,10},{10,1... | collective-permute-start | bytes 4718600 | tf_op jit(solution)/shard_map/ppermute | solution.py:48
  49.9 1.4 fusion
  51.4 1.9 %collective-permute-start.1 = (bf16[2,128,64]{2,1,0:T(8,128)(2,1)S(1)}, bf16[2,128,64]{2,1,0:T(8,128)(2,1)S(1)}, u32[]{:S(2)}, u32[]{:S(2)}) collective-permute-start(bf16[2,128,64]{2,1,0:T(8,128)(2,1)S(1)} %get-tuple-element.6), channel_id=1, source_target_pairs={{16,0},{32,16},{48,32},{64,48},{80,64},{96,80},{112,96},{128,112},... | collective-permute-start | bytes 98312 | tf_op jit(solution)/shard_map/ppermute | solution.py:320
  53.3 0.1 pad_maximum_fusion.kv_ref
  53.4 0.1 copy.22.q_ref
  54.1 3.2 %collective-permute-done.1.high_ref = bf16[2,128,64]{2,1,0:T(8,128)(2,1)S(1)} collective-permute-done((bf16[2,128,64]{2,1,0:T(8,128)(2,1)S(1)}, bf16[2,128,64]{2,1,0:T(8,128)(2,1)S(1)}, u32[]{:S(2)}, u32[]{:S(2)}) %collective-permute-start.1) | collective-permute-done | bytes 32800 | tf_op jit(solution)/shard_map/ppermute | solution.py:320
  57.3 1.3 attend.1
  58.6 0.0 all-to-all-done
  58.7 1.2 broadcast_in_dim.9
  59.9 3.5 %all-to-all-start.1 = ((bf16[4,320,512]{2,1,0:T(8,128)(2,1)}), bf16[4,320,512]{2,1,0:T(8,128)(2,1)S(1)}, u32[]{:S(2)}, u32[]{:S(2)}) async-start(bf16[4,320,512]{2,1,0:T(8,128)(2,1)} %broadcast_in_dim.9), calls=%async_computation.1 | async-start | bytes 2621440 | tf_op jit(solution)/shard_map/all_to_all | solution.py:370
  63.4 0.0 collective-permute-done.6.refs_3_
  63.4 17.4 %all-to-all-done.1.x_ref = bf16[4,320,512]{2,1,0:T(8,128)(2,1)S(1)} async-done(((bf16[4,320,512]{2,1,0:T(8,128)(2,1)}), bf16[4,320,512]{2,1,0:T(8,128)(2,1)S(1)}, u32[]{:S(2)}, u32[]{:S(2)}) %all-to-all-start.1) | async-done | bytes 1310752 | tf_op jit(solution)/shard_map/all_to_all | solution.py:370
  80.8 0.5 collective-permute-done.10.refs_7_
  81.3 6.6 %ffn.1 = bf16[16,256,128]{2,1,0:T(8,128)(2,1)} custom-call(bf16[4,320,512]{2,1,0:T(8,128)(2,1)S(1)} %all-to-all-done.1.x_ref, bf16[3072,256]{1,0:T(8,128)(2,1)} %pack.2.refs_0_, bf16[3072,256]{1,0:T(8,128)(2,1)S(1)} %pack.3.refs_1_, bf16[3072,256]{1,0:T(8,128)(2,1)} %collective-permute-done.5.refs_2_, bf16[3072,256]{1,0:T(8,128)(2,1)} %collective-permute-done.6.refs_3_, ...), custom_call_target="tpu_custom_call" | custom-call | tf_op jit(solution)/shard_map/ffn/pallas_call | solution.py:208
  87.9 22.1 %all_to_all.27 = bf16[16,256,128]{2,1,0:T(8,128)(2,1)S(1)} all-to-all(bf16[16,256,128]{2,1,0:T(8,128)(2,1)} %ffn.1), channel_id=1, replica_groups={{0,1,2,3,4,5,6,7,8,9,10,11,12,13,14,15},{16,20,24,28,17,21,25,29,18,22,..., dimensions={0} | all-to-all | bytes 2097152 | tf_op jit(solution)/shard_map/all_to_all | solution.py:375
  110.0 0.2 reduce_sum.12
  110.2 0.7 copy_bitcast_fusion
  110.9 14.5 %all-to-all-start.3 = ((bf16[32,32,128]{2,1,0:T(8,128)(2,1)}), bf16[32,32,128]{2,1,0:T(8,128)(2,1)S(1)}, u32[]{:S(2)}, u32[]{:S(2)}) async-start(bf16[32,32,128]{2,1,0:T(8,128)(2,1)} %copy_bitcast_fusion), calls=%async_computation.3 | async-start | bytes 524288 | tf_op jit(solution)/shard_map/all_to_all | solution.py:380
  125.4 1.9 %collective-permute-start.2 = (bf16[4,64,512]{2,1,0:T(8,128)(2,1)S(1)}, bf16[4,64,512]{2,1,0:T(8,128)(2,1)S(1)}, u32[]{:S(2)}, u32[]{:S(2)}) collective-permute-start(bf16[4,64,512]{2,1,0:T(8,128)(2,1)S(1)} %slice.16.own_ref), channel_id=1, source_target_pairs={{0,1},{1,2},{2,3},{3,0},{4,5},{5,6},{6,7},{7,4},{8,9},{9,10},{10,1... | collective-permute-start | bytes 786440 | tf_op jit(solution)/shard_map/ppermute | solution.py:48
  127.4 4.6 %collective-permute-start.3 = (bf16[4,64,512]{2,1,0:T(8,128)(2,1)S(1)}, bf16[4,64,512]{2,1,0:T(8,128)(2,1)S(1)}, u32[]{:S(2)}, u32[]{:S(2)}) collective-permute-start(bf16[4,64,512]{2,1,0:T(8,128)(2,1)S(1)} %slice.16.own_ref), channel_id=1, source_target_pairs={{0,3},{1,0},{2,1},{3,2},{4,7},{5,4},{6,5},{7,6},{8,11},{9,8},{10,9... | collective-permute-start | bytes 786440 | tf_op jit(solution)/shard_map/ppermute | solution.py:48
  131.9 1.9 %collective-permute-start.4 = (bf16[4,64,512]{2,1,0:T(8,128)(2,1)S(1)}, bf16[4,64,512]{2,1,0:T(8,128)(2,1)S(1)}, u32[]{:S(2)}, u32[]{:S(2)}) collective-permute-start(bf16[4,64,512]{2,1,0:T(8,128)(2,1)S(1)} %slice.16.own_ref), channel_id=1, source_target_pairs={{0,2},{1,3},{2,0},{3,1},{4,6},{5,7},{6,4},{7,5},{8,10},{9,11},{10,... | collective-permute-start | bytes 786440 | tf_op jit(solution)/shard_map/ppermute | solution.py:48
  133.9 0.1 copy.24.weight_ref
  134.0 0.0 collective-permute-done.2.prev_ref
  134.1 4.0 %collective-permute-done.3.next_ref = bf16[4,64,512]{2,1,0:T(8,128)(2,1)S(1)} collective-permute-done((bf16[4,64,512]{2,1,0:T(8,128)(2,1)S(1)}, bf16[4,64,512]{2,1,0:T(8,128)(2,1)S(1)}, u32[]{:S(2)}, u32[]{:S(2)}) %collective-permute-start.3) | collective-permute-done | bytes 262176 | tf_op jit(solution)/shard_map/ppermute | solution.py:48
  138.1 2.8 %collective-permute-done.4.far_ref = bf16[4,64,512]{2,1,0:T(8,128)(2,1)S(1)} collective-permute-done((bf16[4,64,512]{2,1,0:T(8,128)(2,1)S(1)}, bf16[4,64,512]{2,1,0:T(8,128)(2,1)S(1)}, u32[]{:S(2)}, u32[]{:S(2)}) %collective-permute-start.4) | collective-permute-done | bytes 262176 | tf_op jit(solution)/shard_map/ppermute | solution.py:48
  140.9 1.1 project.1
  142.0 5.7 %all-to-all-done.3 = bf16[32,32,128]{2,1,0:T(8,128)(2,1)S(1)} async-done(((bf16[32,32,128]{2,1,0:T(8,128)(2,1)}), bf16[32,32,128]{2,1,0:T(8,128)(2,1)S(1)}, u32[]{:S(2)}, u32[]{:S(2)}) %all-to-all-start.3) | async-done | bytes 262176 | tf_op jit(solution)/shard_map/all_to_all | solution.py:380
  147.7 1.1 combine.1
  (25 shorter events, 0.1 us)
Async XLA Ops:
  0.6 1.2 copy-start
  1.9 1.2 copy-start.2
  3.1 7.4 %copy-start.1 = (bf16[1,2048,256]{2,1,0:T(8,128)(2,1)S(1)}, bf16[1,2048,256]{2,1,0:T(8,128)(2,1)}, u32[]{:S(2)}) copy-start(bf16[1,2048,256]{2,1,0:T(8,128)(2,1)} %refs_0_.3) | copy-start | bytes 3145732
  3.1 7.4 %copy-start.3 = (bf16[1,2048,256]{2,1,0:T(8,128)(2,1)S(1)}, bf16[1,2048,256]{2,1,0:T(8,128)(2,1)}, u32[]{:S(2)}) copy-start(bf16[1,2048,256]{2,1,0:T(8,128)(2,1)} %refs_0_.2) | copy-start | bytes 3145732
  4.8 9.1 %copy-start.4 = (bf16[256,2048]{1,0:T(8,128)(2,1)S(1)}, bf16[256,2048]{1,0:T(8,128)(2,1)}, u32[]{:S(2)}) copy-start(bf16[256,2048]{1,0:T(8,128)(2,1)} %x_ref.1) | copy-start | bytes 3145732
  4.9 9.1 %copy-start.6 = (f32[2048]{0:T(1024)S(1)}, f32[2048]{0:T(1024)}, u32[]{:S(2)}) copy-start(f32[2048]{0:T(1024)} %param.18) | copy-start | bytes 24580
  4.9 9.1 %copy-start.7 = (s32[256,2]{0,1:T(2,128)S(1)}, s32[256,2]{0,1:T(2,128)}, u32[]{:S(2)}) copy-start(s32[256,2]{0,1:T(2,128)} %param.19) | copy-start | bytes 6148
  4.9 38.4 %collective-permute-start.8 = (bf16[3072,256]{1,0:T(8,128)(2,1)S(1)}, bf16[3072,256]{1,0:T(8,128)(2,1)}, u32[]{:S(2)}, u32[]{:S(2)}) collective-permute-start(bf16[3072,256]{1,0:T(8,128)(2,1)S(1)} %pack.3.refs_1_), channel_id=1, source_target_pairs={{0,3},{1,0},{2,1},{3,2},{4,7},{5,4},{6,5},{7,6},{8,11},{9,8},{10,9... | collective-permute-start | bytes 4718600 | tf_op jit(solution)/shard_map/ppermute | solution.py:48
  11.9 27.2 %copy-start.8 = (bf16[512,256]{1,0:T(8,128)(2,1)S(1)}, bf16[512,256]{1,0:T(8,128)(2,1)}, u32[]{:S(2)}) copy-start(bf16[512,256]{1,0:T(8,128)(2,1)} %param.14) | copy-start | bytes 786436
  11.9 27.2 %copy-start.9 = (bf16[512,256]{1,0:T(8,128)(2,1)S(1)}, bf16[512,256]{1,0:T(8,128)(2,1)}, u32[]{:S(2)}) copy-start(bf16[512,256]{1,0:T(8,128)(2,1)} %param.13) | copy-start | bytes 786436
  11.9 36.1 %collective-permute-start.5 = (bf16[3072,256]{1,0:T(8,128)(2,1)}, bf16[3072,256]{1,0:T(8,128)(2,1)}, u32[]{:S(2)}, u32[]{:S(2)}) collective-permute-start(bf16[3072,256]{1,0:T(8,128)(2,1)} %pack.2.refs_0_), channel_id=1, source_target_pairs={{0,1},{1,2},{2,3},{3,0},{4,5},{5,6},{6,7},{7,4},{8,9},{9,10},{10,1... | collective-permute-start | bytes 4718600 | tf_op jit(solution)/shard_map/ppermute | solution.py:48
  16.3 37.0 %copy-start.10 = (bf16[512,64]{0,1:T(8,128)(2,1)S(1)}, bf16[512,64]{0,1:T(8,128)(2,1)}, u32[]{:S(2)}) copy-start(bf16[512,64]{0,1:T(8,128)(2,1)} %param.12) | copy-start | bytes 196612
  16.3 42.3 %all-to-all-start = ((bf16[32,8,512]{2,1,0:T(8,128)(2,1)}), bf16[32,8,512]{2,1,0:T(8,128)(2,1)S(1)}, u32[]{:S(2)}, u32[]{:S(2)}) async-start(bf16[32,8,512]{2,1,0:T(8,128)(2,1)} %bitcast.2), calls=%async_computation | async-start | bytes 524288 | tf_op jit(solution)/shard_map/all_to_all | solution.py:363
  32.4 31.0 %collective-permute-start.6 = (bf16[3072,256]{1,0:T(8,128)(2,1)S(1)}, bf16[3072,256]{1,0:T(8,128)(2,1)}, u32[]{:S(2)}, u32[]{:S(2)}) collective-permute-start(bf16[3072,256]{1,0:T(8,128)(2,1)S(1)} %pack.3.refs_1_), channel_id=1, source_target_pairs={{0,1},{1,2},{2,3},{3,0},{4,5},{5,6},{6,7},{7,4},{8,9},{9,10},{10,1... | collective-permute-start | bytes 4718600 | tf_op jit(solution)/shard_map/ppermute | solution.py:48
  35.6 27.8 %collective-permute-start.7 = (bf16[3072,256]{1,0:T(8,128)(2,1)}, bf16[3072,256]{1,0:T(8,128)(2,1)}, u32[]{:S(2)}, u32[]{:S(2)}) collective-permute-start(bf16[3072,256]{1,0:T(8,128)(2,1)} %pack.2.refs_0_), channel_id=1, source_target_pairs={{0,3},{1,0},{2,1},{3,2},{4,7},{5,4},{6,5},{7,6},{8,11},{9,8},{10,9... | collective-permute-start | bytes 4718600 | tf_op jit(solution)/shard_map/ppermute | solution.py:48
  39.2 12.1 %collective-permute-start = (bf16[2,128,64]{2,1,0:T(8,128)(2,1)S(1)}, bf16[2,128,64]{2,1,0:T(8,128)(2,1)S(1)}, u32[]{:S(2)}, u32[]{:S(2)}) collective-permute-start(bf16[2,128,64]{2,1,0:T(8,128)(2,1)S(1)} %get-tuple-element.7), channel_id=1, source_target_pairs={{0,16},{16,32},{32,48},{48,64},{64,80},{80,96},{96,112},{112,128},... | collective-permute-start | bytes 98312 | tf_op jit(solution)/shard_map/ppermute | solution.py:319
  43.3 38.0 %collective-permute-start.10 = (bf16[3072,256]{1,0:T(8,128)(2,1)}, bf16[3072,256]{1,0:T(8,128)(2,1)}, u32[]{:S(2)}, u32[]{:S(2)}) collective-permute-start(bf16[3072,256]{1,0:T(8,128)(2,1)} %collective-permute-done.8.refs_5_), channel_id=1, source_target_pairs={{0,3},{1,0},{2,1},{3,2},{4,7},{5,4},{6,5},{7,6},{8,11},{9,8},{10,9... | collective-permute-start | bytes 4718600 | tf_op jit(solution)/shard_map/ppermute | solution.py:48
  48.0 33.3 %collective-permute-start.9 = (bf16[3072,256]{1,0:T(8,128)(2,1)}, bf16[3072,256]{1,0:T(8,128)(2,1)}, u32[]{:S(2)}, u32[]{:S(2)}) collective-permute-start(bf16[3072,256]{1,0:T(8,128)(2,1)} %collective-permute-done.5.refs_2_), channel_id=1, source_target_pairs={{0,1},{1,2},{2,3},{3,0},{4,5},{5,6},{6,7},{7,4},{8,9},{9,10},{10,1... | collective-permute-start | bytes 4718600 | tf_op jit(solution)/shard_map/ppermute | solution.py:48
  51.4 6.0 %collective-permute-start.1 = (bf16[2,128,64]{2,1,0:T(8,128)(2,1)S(1)}, bf16[2,128,64]{2,1,0:T(8,128)(2,1)S(1)}, u32[]{:S(2)}, u32[]{:S(2)}) collective-permute-start(bf16[2,128,64]{2,1,0:T(8,128)(2,1)S(1)} %get-tuple-element.6), channel_id=1, source_target_pairs={{16,0},{32,16},{48,32},{64,48},{80,64},{96,80},{112,96},{128,112},... | collective-permute-start | bytes 98312 | tf_op jit(solution)/shard_map/ppermute | solution.py:320
  59.9 21.0 %all-to-all-start.1 = ((bf16[4,320,512]{2,1,0:T(8,128)(2,1)}), bf16[4,320,512]{2,1,0:T(8,128)(2,1)S(1)}, u32[]{:S(2)}, u32[]{:S(2)}) async-start(bf16[4,320,512]{2,1,0:T(8,128)(2,1)} %broadcast_in_dim.9), calls=%async_computation.1 | async-start | bytes 2621440 | tf_op jit(solution)/shard_map/all_to_all | solution.py:370
  109.9 23.9 %copy-start.11 = (f32[256,2]{0,1:T(2,128)S(1)}, f32[256,2]{0,1:T(2,128)}, u32[]{:S(2)}) copy-start(f32[256,2]{0,1:T(2,128)} %param.20) | copy-start | bytes 6148
  110.0 30.9 %copy-start.5 = (bf16[1024,128]{1,0:T(8,128)(2,1)S(1)}, bf16[1024,128]{1,0:T(8,128)(2,1)}, u32[]{:S(2)}) copy-start(bf16[1024,128]{1,0:T(8,128)(2,1)} %weight_ref.2) | copy-start | bytes 786436
  110.9 36.7 %all-to-all-start.3 = ((bf16[32,32,128]{2,1,0:T(8,128)(2,1)}), bf16[32,32,128]{2,1,0:T(8,128)(2,1)S(1)}, u32[]{:S(2)}, u32[]{:S(2)}) async-start(bf16[32,32,128]{2,1,0:T(8,128)(2,1)} %copy_bitcast_fusion), calls=%async_computation.3 | async-start | bytes 524288 | tf_op jit(solution)/shard_map/all_to_all | solution.py:380
  125.4 8.6 %collective-permute-start.2 = (bf16[4,64,512]{2,1,0:T(8,128)(2,1)S(1)}, bf16[4,64,512]{2,1,0:T(8,128)(2,1)S(1)}, u32[]{:S(2)}, u32[]{:S(2)}) collective-permute-start(bf16[4,64,512]{2,1,0:T(8,128)(2,1)S(1)} %slice.16.own_ref), channel_id=1, source_target_pairs={{0,1},{1,2},{2,3},{3,0},{4,5},{5,6},{6,7},{7,4},{8,9},{9,10},{10,1... | collective-permute-start | bytes 786440 | tf_op jit(solution)/shard_map/ppermute | solution.py:48
  127.4 10.7 %collective-permute-start.3 = (bf16[4,64,512]{2,1,0:T(8,128)(2,1)S(1)}, bf16[4,64,512]{2,1,0:T(8,128)(2,1)S(1)}, u32[]{:S(2)}, u32[]{:S(2)}) collective-permute-start(bf16[4,64,512]{2,1,0:T(8,128)(2,1)S(1)} %slice.16.own_ref), channel_id=1, source_target_pairs={{0,3},{1,0},{2,1},{3,2},{4,7},{5,4},{6,5},{7,6},{8,11},{9,8},{10,9... | collective-permute-start | bytes 786440 | tf_op jit(solution)/shard_map/ppermute | solution.py:48
  131.9 8.9 %collective-permute-start.4 = (bf16[4,64,512]{2,1,0:T(8,128)(2,1)S(1)}, bf16[4,64,512]{2,1,0:T(8,128)(2,1)S(1)}, u32[]{:S(2)}, u32[]{:S(2)}) collective-permute-start(bf16[4,64,512]{2,1,0:T(8,128)(2,1)S(1)} %slice.16.own_ref), channel_id=1, source_target_pairs={{0,2},{1,3},{2,0},{3,1},{4,6},{5,7},{6,4},{7,5},{8,10},{9,11},{10,... | collective-permute-start | bytes 786440 | tf_op jit(solution)/shard_map/ppermute | solution.py:48

commit v6 on v5

--- a/solution.py
+++ b/solution.py
@@ -32,11 +32,16 @@
 
 ANY = pl.BlockSpec(memory_space=pl.ANY)
 VMEM = pl.BlockSpec(memory_space=pltpu.VMEM)
+IN_HBM = pl.BlockSpec(memory_space=pltpu.HBM)
 HALF_W = 3072
 
 
 def resident(x):
     return pltpu.with_memory_space_constraint(x, pltpu.VMEM)
+
+
+def in_hbm(x):
+    return pltpu.with_memory_space_constraint(x, pltpu.HBM)
 
 
 def vmem_mib(count):
@@ -48,41 +53,31 @@
     return lax.ppermute(x, PLANE, pairs)
 
 
-def pack_kernel(pieces, *refs):
-    sources, out_ref, stage_ref, sems = refs[:-3], refs[-3], refs[-2], refs[-1]
-    copies, leave = [], []
-    for i, (which, rows, cols, at) in enumerate(pieces):
-        source = sources[which].at[0, pl.ds(*rows), pl.ds(*cols)]
-        part = pl.ds(at, rows[1])
-        copies.append(pltpu.make_async_copy(source, stage_ref.at[part], sems.at[0, i]))
-        leave.append(
-            pltpu.make_async_copy(stage_ref.at[part], out_ref.at[part], sems.at[1, i])
-        )
-    for copy in copies:
-        copy.start()
-    for come, go in zip(copies, leave):
-        come.wait()
-        go.start()
-    for go in leave:
-        go.wait()
-
-
 def pack(pieces, *sources):
     def body(*refs):
-        pack_kernel(pieces, *refs)
+        inputs, out_ref, sems = refs[:-2], refs[-2], refs[-1]
+        copies = [
+            pltpu.make_async_copy(
+                inputs[which].at[0, pl.ds(*rows), pl.ds(*cols)],
+                out_ref.at[pl.ds(at, rows[1])],
+                sems.at[i],
+            )
+            for i, (which, rows, cols, at) in enumerate(pieces)
+        ]
+        for copy in copies:
+            copy.start()
+        for copy in copies:
+            copy.wait()
 
     return pl.pallas_call(
         body,
-        out_shape=jax.ShapeDtypeStruct((HALF_W, 256), jnp.bfloat16),
-        in_specs=[ANY] * len(sources),
-        out_specs=ANY,
-        scratch_shapes=[
-            pltpu.VMEM((HALF_W, 256), jnp.bfloat16),
-            pltpu.SemaphoreType.DMA((2, len(pieces))),
-        ],
+        out_shape=pltpu.VMEM((HALF_W, 256), jnp.bfloat16),
+        in_specs=[IN_HBM] * len(sources),
+        out_specs=VMEM,
+        scratch_shapes=[pltpu.SemaphoreType.DMA((len(pieces),))],
         compiler_params=vmem_mib(4),
         name="pack",
-    )(*sources)
+    )(*(in_hbm(a) for a in sources))
 
 
 PIECES_A = ((0, (0, 2048), (0, 256), 0), (1, (0, 1024), (0, 256), 2048))
@@ -170,13 +165,11 @@
 
 def ffn_kernel(x_ref, *refs):
     weights, out_ref, acc_ref, bufs, sems, piece_ref, out_sems = refs[:8], *refs[8:]
-    leave = []
-    copies = [
-        pltpu.make_async_copy(w, bufs.at[i], sems.at[i]) for i, w in enumerate(weights)
-    ]
+    copies = [pltpu.make_async_copy(w, bufs.at[i], sems.at[i]) for i, w in enumerate(weights)]
     for copy in copies:
         copy.start()
     core = lax.axis_index("co")
+    leave = []
     for s in range(4):
         copies[2 * s].wait()
         copies[2 * s + 1].wait()
@@ -194,8 +187,7 @@
             for k in range(2):
                 t = 2 * c + k
                 place = jnp.where(core == 0, t, (t % 4) * 4 + t // 4)
-                piece = total[:, k * 128 : (k + 1) * 128].astype(jnp.bfloat16)
-                piece_ref[t] = piece
+                piece_ref[t] = total[:, k * 128 : (k + 1) * 128].astype(jnp.bfloat16)
                 leave.append(
                     pltpu.make_async_copy(piece_ref.at[t], out_ref.at[place], out_sems.at[t])
                 )
@@ -209,7 +201,7 @@
         ffn_kernel,
         out_shape=pltpu.HBM((16, ROWS_B, 128), jnp.bfloat16),
         in_specs=[VMEM] + [ANY] * 8,
-        out_specs=pl.BlockSpec(memory_space=pltpu.HBM),
+        out_specs=IN_HBM,
         scratch_shapes=[
             pltpu.VMEM((ROWS_B, D), jnp.float32),
             pltpu.VMEM((8, HALF_W, 256), jnp.bfloat16),
@@ -220,6 +212,23 @@
         compiler_params=vmem_mib(24),
         name="ffn",
     )(resident(x), *weights)
+
+
+def total_kernel(parts_ref, out_ref):
+    for l in range(4):
+        rows = sum(parts_ref[4 * m + l].astype(jnp.float32) for m in range(4))
+        out_ref[:, l] = rows.astype(jnp.bfloat16).reshape(EXPERTS, 8, 128)
+
+
+def total(parts):
+    return pl.pallas_call(
+        total_kernel,
+        out_shape=jax.ShapeDtypeStruct((EXPERTS, 4, 8, 128), jnp.bfloat16),
+        in_specs=[VMEM],
+        out_specs=VMEM,
+        compiler_params=vmem_mib(8),
+        name="total",
+    )(resident(parts))
 
 
 def combine_kernel(ret_ref, slot_ref, weight_ref, out_ref):
@@ -355,11 +364,11 @@
 ):
     wa = pack(PIECES_A, gate_weight, up_weight)
     prev_a = line_shift(wa, 1)
+    next_a = line_shift(wa, -1)
     wb = pack(PIECES_B, up_weight, down_weight)
     next_b = line_shift(wb, -1)
+    prev_b = line_shift(wb, 1)
     outgoing, slots = prepare(expert_input, norm_gain, routes)
-    next_a = line_shift(wa, -1)
-    prev_b = line_shift(wb, 1)
     arrived = lax.all_to_all(outgoing, EP, 0, 0, tiled=True)
     far_a = line_shift(prev_a, 1)
     far_b = line_shift(next_b, -1)
@@ -373,10 +382,7 @@
     )
     partial = ffn(rows, (wa, wb, prev_a, prev_b, next_a, next_b, far_a, far_b))
     parts = lax.all_to_all(partial, PLANE, 0, 0, tiled=True, axis_index_groups=WHOLE)
-    parts = parts.reshape(4, 4, 256, 128)
-    result = jnp.sum(parts.astype(jnp.float32), axis=0).astype(jnp.bfloat16)
-    result = jnp.moveaxis(result.reshape(4, EXPERTS, 8, 128), 0, 1)
-    result = result.reshape(EXPERTS, CAP, 128)
+    result = total(parts).reshape(EXPERTS, CAP, 128)
     returned = lax.all_to_all(result, EP, 0, 0, tiled=True)
     expert_out = combine(returned.reshape(EXPERTS * CAP, 128), slots, route_weights)
 

time: 150 us -> 148 us (0.987)
  local copies, waits for them, and re-layouts: 4.83 us -> 1.64 us
  Pallas kernels: 15.6 us -> 17.3 us
    unnamed x26 -> x18, local copies, waits for them, and re-layouts: 2.74 us -> 0.29 us
    pallas_call x2 -> x3, Pallas kernels: 3.09 us -> 4.83 us  [the longest x2 4 us: pack(): pl.pallas_call(body, out_shape=pltpu.VMEM((HALF_W, 256), jnp.bfloat16), i...]
  transfers between devices with their start and end apart: 14 -> 14, of which waited for: 6 -> 6; matrix products, arithmetic and copies ran while one was open for 2% -> 2% of each run, Pallas kernels for 4% -> 5%
where the time goes in v6:
time: 148 us; the launch traced here: 147 us
  starting transfers between devices  69.2 us (47%)
  waiting for transfers between devices  33.6 us (23%)
  blocking collectives  22.1 us (15%)
  Pallas kernels  17.3 us (12%)
  between operations  1.66 us (1%)
  local copies, waits for them, and re-layouts  1.64 us (1%)
  other arithmetic  1.57 us (1%)
    ppermute x9, starting transfers between devices, line_shift(): return lax.ppermute(x, PLANE, pairs)  29.2 us
    all_to_all x1, blocking collectives, local(): lax.all_to_all(partial, PLANE, 0, 0, tiled=True, axis_index_groups=WHOLE)  22.1 us
    all_to_all x1, waiting for transfers between devices, local(): lax.all_to_all(jnp.broadcast_to(payload[None], (4, *payload.shape)), PLAN...  17.4 us
    all_to_all x1, starting transfers between devices, local(): arrived = lax.all_to_all(outgoing, EP, 0, 0, tiled=True)  16.1 us
    all_to_all x1, starting transfers between devices, local(): returned = lax.all_to_all(result, EP, 0, 0, tiled=True)  14.4 us
    ppermute x9, waiting for transfers between devices, line_shift(): return lax.ppermute(x, PLANE, pairs)  7.31 us
    pallas_call x1, Pallas kernels, ffn(): pl.pallas_call(ffn_kernel, out_shape=pltpu.HBM((16, ROWS_B, 128), jnp.bfl...  6.61 us
    all_to_all x1, waiting for transfers between devices, local(): returned = lax.all_to_all(result, EP, 0, 0, tiled=True)  5.67 us
  transfers between devices with their start and end apart: 14, of which 6 were waited for; matrix products, arithmetic and copies ran while one was open for 2% of the time, Pallas kernels for 5%

profile of v6, /device:TPU:1, one launch (start us, length us, event | category | flops | bytes accessed | tf_op | source)
XLA Modules:
  0.0 147.1 jit_solution(13665278383607412340)
XLA Ops:
  0.6 1.4 pack.3.refs_1_
  2.1 0.0 copy-start
  2.1 0.0 copy-start.2
  2.1 0.0 copy-start.3
  2.1 5.6 %collective-permute-start.8 = (bf16[3072,256]{1,0:T(8,128)(2,1)S(1)}, bf16[3072,256]{1,0:T(8,128)(2,1)}, u32[]{:S(2)}, u32[]{:S(2)}) collective-permute-start(bf16[3072,256]{1,0:T(8,128)(2,1)S(1)} %pack.3.refs_1_), channel_id=1, source_target_pairs={{0,3},{1,0},{2,1},{3,2},{4,7},{5,4},{6,5},{7,6},{8,11},{9,8},{10,9... | collective-permute-start | bytes 4718600 | tf_op jit(solution)/shard_map/ppermute | solution.py:53
  7.7 2.6 %pack.2.refs_0_ = bf16[3072,256]{1,0:T(8,128)(2,1)} custom-call(bf16[1,2048,256]{2,1,0:T(8,128)(2,1)} %refs_0_.2, bf16[1,2048,256]{2,1,0:T(8,128)(2,1)} %refs_0_.3), custom_call_target="tpu_custom_call" | custom-call | tf_op jit(solution)/shard_map/pack/pallas_call | solution.py:72
  10.3 0.0 copy-start.4
  10.3 0.0 copy-start.5
  10.3 2.1 %collective-permute-start.5 = (bf16[3072,256]{1,0:T(8,128)(2,1)}, bf16[3072,256]{1,0:T(8,128)(2,1)}, u32[]{:S(2)}, u32[]{:S(2)}) collective-permute-start(bf16[3072,256]{1,0:T(8,128)(2,1)} %pack.2.refs_0_), channel_id=1, source_target_pairs={{0,1},{1,2},{2,3},{3,0},{4,5},{5,6},{6,7},{7,4},{8,9},{9,10},{10,1... | collective-permute-start | bytes 4718600 | tf_op jit(solution)/shard_map/ppermute | solution.py:53
  12.4 2.4 %prep.1 = (bf16[256,512]{1,0:T(8,128)(2,1)}, s32[256,128]{1,0:T(8,128)S(1)}) custom-call(bf16[256,2048]{1,0:T(8,128)(2,1)S(1)} %copy-done, f32[1,2048]{1,0:T(1,128)S(1)} %bitcast.11, s32[2,256]{1,0:T(2,128)S(1)} %bitcast.12), custom_call_target="tpu_custom_call" | custom-call | tf_op jit(solution)/shard_map/prep/pallas_call | solution.py:140
  14.8 16.1 %all-to-all-start = ((bf16[32,8,512]{2,1,0:T(8,128)(2,1)}), bf16[32,8,512]{2,1,0:T(8,128)(2,1)S(1)}, u32[]{:S(2)}, u32[]{:S(2)}) async-start(bf16[32,8,512]{2,1,0:T(8,128)(2,1)} %bitcast.2), calls=%async_computation | async-start | bytes 524288 | tf_op jit(solution)/shard_map/all_to_all | solution.py:372
  30.8 3.2 %collective-permute-start.6 = (bf16[3072,256]{1,0:T(8,128)(2,1)S(1)}, bf16[3072,256]{1,0:T(8,128)(2,1)}, u32[]{:S(2)}, u32[]{:S(2)}) collective-permute-start(bf16[3072,256]{1,0:T(8,128)(2,1)S(1)} %pack.3.refs_1_), channel_id=1, source_target_pairs={{0,1},{1,2},{2,3},{3,0},{4,5},{5,6},{6,7},{7,4},{8,9},{9,10},{10,1... | collective-permute-start | bytes 4718600 | tf_op jit(solution)/shard_map/ppermute | solution.py:53
  34.1 3.4 %collective-permute-start.7 = (bf16[3072,256]{1,0:T(8,128)(2,1)}, bf16[3072,256]{1,0:T(8,128)(2,1)}, u32[]{:S(2)}, u32[]{:S(2)}) collective-permute-start(bf16[3072,256]{1,0:T(8,128)(2,1)} %pack.2.refs_0_), channel_id=1, source_target_pairs={{0,3},{1,0},{2,1},{3,2},{4,7},{5,4},{6,5},{7,6},{8,11},{9,8},{10,9... | collective-permute-start | bytes 4718600 | tf_op jit(solution)/shard_map/ppermute | solution.py:53
  37.5 0.1 dynamic-slice_bitcast_fusion
  37.6 4.0 %collective-permute-start = (bf16[2,128,64]{2,1,0:T(8,128)(2,1)S(1)}, bf16[2,128,64]{2,1,0:T(8,128)(2,1)S(1)}, u32[]{:S(2)}, u32[]{:S(2)}) collective-permute-start(bf16[2,128,64]{2,1,0:T(8,128)(2,1)S(1)} %get-tuple-element.7), channel_id=1, source_target_pairs={{0,16},{16,32},{32,48},{48,64},{64,80},{80,96},{96,112},{112,128},... | collective-permute-start | bytes 98312 | tf_op jit(solution)/shard_map/ppermute | solution.py:328
  41.7 0.0 collective-permute-done.8.refs_5_
  41.7 4.6 %collective-permute-start.10 = (bf16[3072,256]{1,0:T(8,128)(2,1)}, bf16[3072,256]{1,0:T(8,128)(2,1)}, u32[]{:S(2)}, u32[]{:S(2)}) collective-permute-start(bf16[3072,256]{1,0:T(8,128)(2,1)} %collective-permute-done.8.refs_5_), channel_id=1, source_target_pairs={{0,3},{1,0},{2,1},{3,2},{4,7},{5,4},{6,5},{7,6},{8,11},{9,8},{10,9... | collective-permute-start | bytes 4718600 | tf_op jit(solution)/shard_map/ppermute | solution.py:53
  46.4 0.0 collective-permute-done.5.refs_2_
  46.4 1.9 %collective-permute-start.9 = (bf16[3072,256]{1,0:T(8,128)(2,1)}, bf16[3072,256]{1,0:T(8,128)(2,1)}, u32[]{:S(2)}, u32[]{:S(2)}) collective-permute-start(bf16[3072,256]{1,0:T(8,128)(2,1)} %collective-permute-done.5.refs_2_), channel_id=1, source_target_pairs={{0,1},{1,2},{2,3},{3,0},{4,5},{5,6},{6,7},{7,4},{8,9},{9,10},{10,1... | collective-permute-start | bytes 4718600 | tf_op jit(solution)/shard_map/ppermute | solution.py:53
  48.3 1.4 fusion
  49.8 0.0 collective-permute-done.low_ref
  49.8 1.9 %collective-permute-start.1 = (bf16[2,128,64]{2,1,0:T(8,128)(2,1)S(1)}, bf16[2,128,64]{2,1,0:T(8,128)(2,1)S(1)}, u32[]{:S(2)}, u32[]{:S(2)}) collective-permute-start(bf16[2,128,64]{2,1,0:T(8,128)(2,1)S(1)} %get-tuple-element.6), channel_id=1, source_target_pairs={{16,0},{32,16},{48,32},{64,48},{80,64},{96,80},{112,96},{128,112},... | collective-permute-start | bytes 98312 | tf_op jit(solution)/shard_map/ppermute | solution.py:329
  51.7 0.1 pad_maximum_fusion.kv_ref
  51.8 0.1 copy.17.q_ref
  52.6 3.2 %collective-permute-done.1.high_ref = bf16[2,128,64]{2,1,0:T(8,128)(2,1)S(1)} collective-permute-done((bf16[2,128,64]{2,1,0:T(8,128)(2,1)S(1)}, bf16[2,128,64]{2,1,0:T(8,128)(2,1)S(1)}, u32[]{:S(2)}, u32[]{:S(2)}) %collective-permute-start.1) | collective-permute-done | bytes 32800 | tf_op jit(solution)/shard_map/ppermute | solution.py:329
  55.8 1.3 attend.1
  57.1 0.0 all-to-all-done
  57.1 1.2 broadcast_in_dim.9
  58.3 3.5 %all-to-all-start.1 = ((bf16[4,320,512]{2,1,0:T(8,128)(2,1)}), bf16[4,320,512]{2,1,0:T(8,128)(2,1)S(1)}, u32[]{:S(2)}, u32[]{:S(2)}) async-start(bf16[4,320,512]{2,1,0:T(8,128)(2,1)} %broadcast_in_dim.9), calls=%async_computation.1 | async-start | bytes 2621440 | tf_op jit(solution)/shard_map/all_to_all | solution.py:379
  61.8 0.0 collective-permute-done.6.refs_3_
  61.8 0.0 collective-permute-done.7.refs_4_
  61.8 17.4 %all-to-all-done.1.x_ref = bf16[4,320,512]{2,1,0:T(8,128)(2,1)S(1)} async-done(((bf16[4,320,512]{2,1,0:T(8,128)(2,1)}), bf16[4,320,512]{2,1,0:T(8,128)(2,1)S(1)}, u32[]{:S(2)}, u32[]{:S(2)}) %all-to-all-start.1) | async-done | bytes 1310752 | tf_op jit(solution)/shard_map/all_to_all | solution.py:379
  79.2 0.5 collective-permute-done.10.refs_7_
  79.7 0.0 collective-permute-done.9.refs_6_
  79.7 6.6 %ffn.1 = bf16[16,256,128]{2,1,0:T(8,128)(2,1)} custom-call(bf16[4,320,512]{2,1,0:T(8,128)(2,1)S(1)} %all-to-all-done.1.x_ref, bf16[3072,256]{1,0:T(8,128)(2,1)} %pack.2.refs_0_, bf16[3072,256]{1,0:T(8,128)(2,1)S(1)} %pack.3.refs_1_, bf16[3072,256]{1,0:T(8,128)(2,1)} %collective-permute-done.5.refs_2_, bf16[3072,256]{1,0:T(8,128)(2,1)} %collective-permute-done.6.refs_3_, ...), custom_call_target="tpu_custom_call" | custom-call | tf_op jit(solution)/shard_map/ffn/pallas_call | solution.py:200
  86.3 22.1 %all_to_all.27.parts_ref = bf16[16,256,128]{2,1,0:T(8,128)(2,1)S(1)} all-to-all(bf16[16,256,128]{2,1,0:T(8,128)(2,1)} %ffn.1), channel_id=1, replica_groups={{0,1,2,3,4,5,6,7,8,9,10,11,12,13,14,15},{16,20,24,28,17,21,25,29,18,22,..., dimensions={0} | all-to-all | bytes 2097152 | tf_op jit(solution)/shard_map/all_to_all | solution.py:384
  108.4 0.8 total.1
  109.3 14.4 %all-to-all-start.3 = ((bf16[32,32,128]{2,1,0:T(8,128)(2,1)}), bf16[32,32,128]{2,1,0:T(8,128)(2,1)S(1)}, u32[]{:S(2)}, u32[]{:S(2)}) async-start(bf16[32,32,128]{2,1,0:T(8,128)(2,1)} %bitcast.6), calls=%async_computation.3 | async-start | bytes 524288 | tf_op jit(solution)/shard_map/all_to_all | solution.py:386
  123.8 1.9 %collective-permute-start.2 = (bf16[4,64,512]{2,1,0:T(8,128)(2,1)S(1)}, bf16[4,64,512]{2,1,0:T(8,128)(2,1)S(1)}, u32[]{:S(2)}, u32[]{:S(2)}) collective-permute-start(bf16[4,64,512]{2,1,0:T(8,128)(2,1)S(1)} %slice.16.own_ref), channel_id=1, source_target_pairs={{0,1},{1,2},{2,3},{3,0},{4,5},{5,6},{6,7},{7,4},{8,9},{9,10},{10,1... | collective-permute-start | bytes 786440 | tf_op jit(solution)/shard_map/ppermute | solution.py:53
  125.7 4.6 %collective-permute-start.3 = (bf16[4,64,512]{2,1,0:T(8,128)(2,1)S(1)}, bf16[4,64,512]{2,1,0:T(8,128)(2,1)S(1)}, u32[]{:S(2)}, u32[]{:S(2)}) collective-permute-start(bf16[4,64,512]{2,1,0:T(8,128)(2,1)S(1)} %slice.16.own_ref), channel_id=1, source_target_pairs={{0,3},{1,0},{2,1},{3,2},{4,7},{5,4},{6,5},{7,6},{8,11},{9,8},{10,9... | collective-permute-start | bytes 786440 | tf_op jit(solution)/shard_map/ppermute | solution.py:53
  130.3 1.9 %collective-permute-start.4 = (bf16[4,64,512]{2,1,0:T(8,128)(2,1)S(1)}, bf16[4,64,512]{2,1,0:T(8,128)(2,1)S(1)}, u32[]{:S(2)}, u32[]{:S(2)}) collective-permute-start(bf16[4,64,512]{2,1,0:T(8,128)(2,1)S(1)} %slice.16.own_ref), channel_id=1, source_target_pairs={{0,2},{1,3},{2,0},{3,1},{4,6},{5,7},{6,4},{7,5},{8,10},{9,11},{10,... | collective-permute-start | bytes 786440 | tf_op jit(solution)/shard_map/ppermute | solution.py:53
  132.2 0.1 copy.18.weight_ref
  132.3 0.0 collective-permute-done.2.prev_ref
  132.4 4.0 %collective-permute-done.3.next_ref = bf16[4,64,512]{2,1,0:T(8,128)(2,1)S(1)} collective-permute-done((bf16[4,64,512]{2,1,0:T(8,128)(2,1)S(1)}, bf16[4,64,512]{2,1,0:T(8,128)(2,1)S(1)}, u32[]{:S(2)}, u32[]{:S(2)}) %collective-permute-start.3) | collective-permute-done | bytes 262176 | tf_op jit(solution)/shard_map/ppermute | solution.py:53
  136.4 2.8 %collective-permute-done.4.far_ref = bf16[4,64,512]{2,1,0:T(8,128)(2,1)S(1)} collective-permute-done((bf16[4,64,512]{2,1,0:T(8,128)(2,1)S(1)}, bf16[4,64,512]{2,1,0:T(8,128)(2,1)S(1)}, u32[]{:S(2)}, u32[]{:S(2)}) %collective-permute-start.4) | collective-permute-done | bytes 262176 | tf_op jit(solution)/shard_map/ppermute | solution.py:53
  139.2 1.1 project.1
  140.3 5.7 %all-to-all-done.3 = bf16[32,32,128]{2,1,0:T(8,128)(2,1)S(1)} async-done(((bf16[32,32,128]{2,1,0:T(8,128)(2,1)}), bf16[32,32,128]{2,1,0:T(8,128)(2,1)S(1)}, u32[]{:S(2)}, u32[]{:S(2)}) %all-to-all-start.3) | async-done | bytes 262176 | tf_op jit(solution)/shard_map/all_to_all | solution.py:386
  146.0 1.1 combine.1
  (16 shorter events, 0.1 us)
Async XLA Ops:
  2.1 10.3 %copy-start = (bf16[256,2048]{1,0:T(8,128)(2,1)S(1)}, bf16[256,2048]{1,0:T(8,128)(2,1)}, u32[]{:S(2)}) copy-start(bf16[256,2048]{1,0:T(8,128)(2,1)} %x_ref.1) | copy-start | bytes 3145732
  2.1 10.3 %copy-start.2 = (f32[2048]{0:T(1024)S(1)}, f32[2048]{0:T(1024)}, u32[]{:S(2)}) copy-start(f32[2048]{0:T(1024)} %param.18) | copy-start | bytes 24580
  2.1 10.3 %copy-start.3 = (s32[256,2]{0,1:T(2,128)S(1)}, s32[256,2]{0,1:T(2,128)}, u32[]{:S(2)}) copy-start(s32[256,2]{0,1:T(2,128)} %param.19) | copy-start | bytes 6148
  2.1 39.6 %collective-permute-start.8 = (bf16[3072,256]{1,0:T(8,128)(2,1)S(1)}, bf16[3072,256]{1,0:T(8,128)(2,1)}, u32[]{:S(2)}, u32[]{:S(2)}) collective-permute-start(bf16[3072,256]{1,0:T(8,128)(2,1)S(1)} %pack.3.refs_1_), channel_id=1, source_target_pairs={{0,3},{1,0},{2,1},{3,2},{4,7},{5,4},{6,5},{7,6},{8,11},{9,8},{10,9... | collective-permute-start | bytes 4718600 | tf_op jit(solution)/shard_map/ppermute | solution.py:53
  10.3 27.2 %copy-start.4 = (bf16[512,256]{1,0:T(8,128)(2,1)S(1)}, bf16[512,256]{1,0:T(8,128)(2,1)}, u32[]{:S(2)}) copy-start(bf16[512,256]{1,0:T(8,128)(2,1)} %param.14) | copy-start | bytes 786436
  10.3 27.2 %copy-start.5 = (bf16[512,256]{1,0:T(8,128)(2,1)S(1)}, bf16[512,256]{1,0:T(8,128)(2,1)}, u32[]{:S(2)}) copy-start(bf16[512,256]{1,0:T(8,128)(2,1)} %param.13) | copy-start | bytes 786436
  10.3 36.1 %collective-permute-start.5 = (bf16[3072,256]{1,0:T(8,128)(2,1)}, bf16[3072,256]{1,0:T(8,128)(2,1)}, u32[]{:S(2)}, u32[]{:S(2)}) collective-permute-start(bf16[3072,256]{1,0:T(8,128)(2,1)} %pack.2.refs_0_), channel_id=1, source_target_pairs={{0,1},{1,2},{2,3},{3,0},{4,5},{5,6},{6,7},{7,4},{8,9},{9,10},{10,1... | collective-permute-start | bytes 4718600 | tf_op jit(solution)/shard_map/ppermute | solution.py:53
  14.8 37.0 %copy-start.6 = (bf16[512,64]{0,1:T(8,128)(2,1)S(1)}, bf16[512,64]{0,1:T(8,128)(2,1)}, u32[]{:S(2)}) copy-start(bf16[512,64]{0,1:T(8,128)(2,1)} %param.12) | copy-start | bytes 196612
  14.8 42.3 %all-to-all-start = ((bf16[32,8,512]{2,1,0:T(8,128)(2,1)}), bf16[32,8,512]{2,1,0:T(8,128)(2,1)S(1)}, u32[]{:S(2)}, u32[]{:S(2)}) async-start(bf16[32,8,512]{2,1,0:T(8,128)(2,1)} %bitcast.2), calls=%async_computation | async-start | bytes 524288 | tf_op jit(solution)/shard_map/all_to_all | solution.py:372
  30.8 31.0 %collective-permute-start.6 = (bf16[3072,256]{1,0:T(8,128)(2,1)S(1)}, bf16[3072,256]{1,0:T(8,128)(2,1)}, u32[]{:S(2)}, u32[]{:S(2)}) collective-permute-start(bf16[3072,256]{1,0:T(8,128)(2,1)S(1)} %pack.3.refs_1_), channel_id=1, source_target_pairs={{0,1},{1,2},{2,3},{3,0},{4,5},{5,6},{6,7},{7,4},{8,9},{9,10},{10,1... | collective-permute-start | bytes 4718600 | tf_op jit(solution)/shard_map/ppermute | solution.py:53
  34.1 27.8 %collective-permute-start.7 = (bf16[3072,256]{1,0:T(8,128)(2,1)}, bf16[3072,256]{1,0:T(8,128)(2,1)}, u32[]{:S(2)}, u32[]{:S(2)}) collective-permute-start(bf16[3072,256]{1,0:T(8,128)(2,1)} %pack.2.refs_0_), channel_id=1, source_target_pairs={{0,3},{1,0},{2,1},{3,2},{4,7},{5,4},{6,5},{7,6},{8,11},{9,8},{10,9... | collective-permute-start | bytes 4718600 | tf_op jit(solution)/shard_map/ppermute | solution.py:53
  37.6 12.1 %collective-permute-start = (bf16[2,128,64]{2,1,0:T(8,128)(2,1)S(1)}, bf16[2,128,64]{2,1,0:T(8,128)(2,1)S(1)}, u32[]{:S(2)}, u32[]{:S(2)}) collective-permute-start(bf16[2,128,64]{2,1,0:T(8,128)(2,1)S(1)} %get-tuple-element.7), channel_id=1, source_target_pairs={{0,16},{16,32},{32,48},{48,64},{64,80},{80,96},{96,112},{112,128},... | collective-permute-start | bytes 98312 | tf_op jit(solution)/shard_map/ppermute | solution.py:328
  41.7 38.0 %collective-permute-start.10 = (bf16[3072,256]{1,0:T(8,128)(2,1)}, bf16[3072,256]{1,0:T(8,128)(2,1)}, u32[]{:S(2)}, u32[]{:S(2)}) collective-permute-start(bf16[3072,256]{1,0:T(8,128)(2,1)} %collective-permute-done.8.refs_5_), channel_id=1, source_target_pairs={{0,3},{1,0},{2,1},{3,2},{4,7},{5,4},{6,5},{7,6},{8,11},{9,8},{10,9... | collective-permute-start | bytes 4718600 | tf_op jit(solution)/shard_map/ppermute | solution.py:53
  46.4 33.3 %collective-permute-start.9 = (bf16[3072,256]{1,0:T(8,128)(2,1)}, bf16[3072,256]{1,0:T(8,128)(2,1)}, u32[]{:S(2)}, u32[]{:S(2)}) collective-permute-start(bf16[3072,256]{1,0:T(8,128)(2,1)} %collective-permute-done.5.refs_2_), channel_id=1, source_target_pairs={{0,1},{1,2},{2,3},{3,0},{4,5},{5,6},{6,7},{7,4},{8,9},{9,10},{10,1... | collective-permute-start | bytes 4718600 | tf_op jit(solution)/shard_map/ppermute | solution.py:53
  49.8 6.0 %collective-permute-start.1 = (bf16[2,128,64]{2,1,0:T(8,128)(2,1)S(1)}, bf16[2,128,64]{2,1,0:T(8,128)(2,1)S(1)}, u32[]{:S(2)}, u32[]{:S(2)}) collective-permute-start(bf16[2,128,64]{2,1,0:T(8,128)(2,1)S(1)} %get-tuple-element.6), channel_id=1, source_target_pairs={{16,0},{32,16},{48,32},{64,48},{80,64},{96,80},{112,96},{128,112},... | collective-permute-start | bytes 98312 | tf_op jit(solution)/shard_map/ppermute | solution.py:329
  58.3 21.0 %all-to-all-start.1 = ((bf16[4,320,512]{2,1,0:T(8,128)(2,1)}), bf16[4,320,512]{2,1,0:T(8,128)(2,1)S(1)}, u32[]{:S(2)}, u32[]{:S(2)}) async-start(bf16[4,320,512]{2,1,0:T(8,128)(2,1)} %broadcast_in_dim.9), calls=%async_computation.1 | async-start | bytes 2621440 | tf_op jit(solution)/shard_map/all_to_all | solution.py:379
  108.4 23.8 %copy-start.7 = (f32[256,2]{0,1:T(2,128)S(1)}, f32[256,2]{0,1:T(2,128)}, u32[]{:S(2)}) copy-start(f32[256,2]{0,1:T(2,128)} %param.20) | copy-start | bytes 6148
  108.4 30.7 %copy-start.1 = (bf16[1024,128]{1,0:T(8,128)(2,1)S(1)}, bf16[1024,128]{1,0:T(8,128)(2,1)}, u32[]{:S(2)}) copy-start(bf16[1024,128]{1,0:T(8,128)(2,1)} %weight_ref.2) | copy-start | bytes 786436
  109.3 36.7 %all-to-all-start.3 = ((bf16[32,32,128]{2,1,0:T(8,128)(2,1)}), bf16[32,32,128]{2,1,0:T(8,128)(2,1)S(1)}, u32[]{:S(2)}, u32[]{:S(2)}) async-start(bf16[32,32,128]{2,1,0:T(8,128)(2,1)} %bitcast.6), calls=%async_computation.3 | async-start | bytes 524288 | tf_op jit(solution)/shard_map/all_to_all | solution.py:386
  123.8 8.6 %collective-permute-start.2 = (bf16[4,64,512]{2,1,0:T(8,128)(2,1)S(1)}, bf16[4,64,512]{2,1,0:T(8,128)(2,1)S(1)}, u32[]{:S(2)}, u32[]{:S(2)}) collective-permute-start(bf16[4,64,512]{2,1,0:T(8,128)(2,1)S(1)} %slice.16.own_ref), channel_id=1, source_target_pairs={{0,1},{1,2},{2,3},{3,0},{4,5},{5,6},{6,7},{7,4},{8,9},{9,10},{10,1... | collective-permute-start | bytes 786440 | tf_op jit(solution)/shard_map/ppermute | solution.py:53
  125.7 10.7 %collective-permute-start.3 = (bf16[4,64,512]{2,1,0:T(8,128)(2,1)S(1)}, bf16[4,64,512]{2,1,0:T(8,128)(2,1)S(1)}, u32[]{:S(2)}, u32[]{:S(2)}) collective-permute-start(bf16[4,64,512]{2,1,0:T(8,128)(2,1)S(1)} %slice.16.own_ref), channel_id=1, source_target_pairs={{0,3},{1,0},{2,1},{3,2},{4,7},{5,4},{6,5},{7,6},{8,11},{9,8},{10,9... | collective-permute-start | bytes 786440 | tf_op jit(solution)/shard_map/ppermute | solution.py:53
  130.3 8.9 %collective-permute-start.4 = (bf16[4,64,512]{2,1,0:T(8,128)(2,1)S(1)}, bf16[4,64,512]{2,1,0:T(8,128)(2,1)S(1)}, u32[]{:S(2)}, u32[]{:S(2)}) collective-permute-start(bf16[4,64,512]{2,1,0:T(8,128)(2,1)S(1)} %slice.16.own_ref), channel_id=1, source_target_pairs={{0,2},{1,3},{2,0},{3,1},{4,6},{5,7},{6,4},{7,5},{8,10},{9,11},{10,... | collective-permute-start | bytes 786440 | tf_op jit(solution)/shard_map/ppermute | solution.py:53

commit v7 on v6

--- a/solution.py
+++ b/solution.py
@@ -53,37 +53,33 @@
     return lax.ppermute(x, PLANE, pairs)
 
 
-def pack(pieces, *sources):
-    def body(*refs):
-        inputs, out_ref, sems = refs[:-2], refs[-2], refs[-1]
-        copies = [
-            pltpu.make_async_copy(
-                inputs[which].at[0, pl.ds(*rows), pl.ds(*cols)],
-                out_ref.at[pl.ds(at, rows[1])],
-                sems.at[i],
-            )
-            for i, (which, rows, cols, at) in enumerate(pieces)
-        ]
-        for copy in copies:
-            copy.start()
-        for copy in copies:
-            copy.wait()
-
-    return pl.pallas_call(
-        body,
-        out_shape=pltpu.VMEM((HALF_W, 256), jnp.bfloat16),
-        in_specs=[IN_HBM] * len(sources),
-        out_specs=VMEM,
-        scratch_shapes=[pltpu.SemaphoreType.DMA((len(pieces),))],
-        compiler_params=vmem_mib(4),
+def pack_kernel(gate_ref, up_ref, down_ref, wa_ref, wb_ref, sems):
+    copies = [
+        (gate_ref.at[0], wa_ref.at[pl.ds(0, 2048)]),
+        (up_ref.at[0, pl.ds(0, 1024)], wa_ref.at[pl.ds(2048, 1024)]),
+        (up_ref.at[0, pl.ds(1024, 1024)], wb_ref.at[pl.ds(0, 1024)]),
+    ] + [
+        (down_ref.at[0, :, pl.ds(c * 256, 256)], wb_ref.at[pl.ds(1024 + c * 256, 256)])
+        for c in range(8)
+    ]
+    copies = [pltpu.make_async_copy(s, d, sems.at[i]) for i, (s, d) in enumerate(copies)]
+    for copy in copies:
+        copy.start()
+    for copy in copies:
+        copy.wait()
+
+
+def pack(gate, up, down):
+    half = pltpu.VMEM((HALF_W, 256), jnp.bfloat16)
+    return pl.pallas_call(
+        pack_kernel,
+        out_shape=(half, half),
+        in_specs=[IN_HBM] * 3,
+        out_specs=(VMEM, VMEM),
+        scratch_shapes=[pltpu.SemaphoreType.DMA((11,))],
+        compiler_params=vmem_mib(8),
         name="pack",
-    )(*(in_hbm(a) for a in sources))
-
-
-PIECES_A = ((0, (0, 2048), (0, 256), 0), (1, (0, 1024), (0, 256), 2048))
-PIECES_B = ((0, (1024, 1024), (0, 256), 0),) + tuple(
-    (1, (0, 256), (c * 256, 256), 1024 + c * 256) for c in range(8)
-)
+    )(*(in_hbm(a) for a in (gate, up, down)))
 
 
 def prep_kernel(x_ref, gain_ref, routes_ref, out_ref, slot_ref, normed_ref):
@@ -223,7 +219,7 @@
 def total(parts):
     return pl.pallas_call(
         total_kernel,
-        out_shape=jax.ShapeDtypeStruct((EXPERTS, 4, 8, 128), jnp.bfloat16),
+        out_shape=pltpu.VMEM((EXPERTS, 4, 8, 128), jnp.bfloat16),
         in_specs=[VMEM],
         out_specs=VMEM,
         compiler_params=vmem_mib(8),
@@ -362,11 +358,10 @@
     up_weight,
     down_weight,
 ):
-    wa = pack(PIECES_A, gate_weight, up_weight)
+    wa, wb = pack(gate_weight, up_weight, down_weight)
     prev_a = line_shift(wa, 1)
+    next_b = line_shift(wb, -1)
     next_a = line_shift(wa, -1)
-    wb = pack(PIECES_B, up_weight, down_weight)
-    next_b = line_shift(wb, -1)
     prev_b = line_shift(wb, 1)
     outgoing, slots = prepare(expert_input, norm_gain, routes)
     arrived = lax.all_to_all(outgoing, EP, 0, 0, tiled=True)
@@ -387,8 +382,9 @@
     expert_out = combine(returned.reshape(EXPERTS * CAP, 128), slots, route_weights)
 
     heads = rows[:, 256:]
-    around = [line_shift(heads, step) for step in (1, -1, 2)]
-    mixer_out = project(heads, *around, out_weight)
+    near = [line_shift(heads, step) for step in (1, -1)]
+    far = line_shift(heads, 2)
+    mixer_out = project(heads, *near, far, out_weight)
     return (mixer_out, expert_out)
 
 

time: 148 us -> 147 us (level)
    pallas_call x3 -> x2, Pallas kernels: 4.83 us -> 4.05 us  [the longest x1 3.21 us: pack(): pl.pallas_call(pack_kernel, out_shape=(half, half), in_specs=[IN_HBM] * 3...]
  transfers between devices with their start and end apart: 14 -> 14, of which waited for: 6 -> 6; matrix products, arithmetic and copies ran while one was open for 2% -> 2% of each run, Pallas kernels for 5% -> 3%
where the time goes in v7:
time: 147 us; the launch traced here: 146 us
  starting transfers between devices  69 us (47%)
  waiting for transfers between devices  33.4 us (23%)
  blocking collectives  22.1 us (15%)
  Pallas kernels  16.7 us (11%)
  between operations  1.65 us (1%)
  local copies, waits for them, and re-layouts  1.63 us (1%)
  other arithmetic  1.57 us (1%)
    ppermute x9, starting transfers between devices, line_shift(): return lax.ppermute(x, PLANE, pairs)  29 us
    all_to_all x1, blocking collectives, local(): lax.all_to_all(partial, PLANE, 0, 0, tiled=True, axis_index_groups=WHOLE)  22.1 us
    all_to_all x1, waiting for transfers between devices, local(): lax.all_to_all(jnp.broadcast_to(payload[None], (4, *payload.shape)), PLAN...  17.6 us
    all_to_all x1, starting transfers between devices, local(): arrived = lax.all_to_all(outgoing, EP, 0, 0, tiled=True)  16.1 us
    all_to_all x1, starting transfers between devices, local(): returned = lax.all_to_all(result, EP, 0, 0, tiled=True)  14.4 us
    ppermute x9, waiting for transfers between devices, line_shift(): return lax.ppermute(x, PLANE, pairs)  6.9 us
    pallas_call x1, Pallas kernels, ffn(): pl.pallas_call(ffn_kernel, out_shape=pltpu.HBM((16, ROWS_B, 128), jnp.bfl...  6.7 us
    all_to_all x1, waiting for transfers between devices, local(): returned = lax.all_to_all(result, EP, 0, 0, tiled=True)  5.67 us
  transfers between devices with their start and end apart: 14, of which 6 were waited for; matrix products, arithmetic and copies ran while one was open for 2% of the time, Pallas kernels for 3%

profile of v7, /device:TPU:1, one launch (start us, length us, event | category | flops | bytes accessed | tf_op | source)
XLA Modules:
  0.0 146.1 jit_solution(5825696568016985554)
XLA Ops:
  0.6 0.0 copy-start.2
  0.7 3.2 %pack.1 = (bf16[3072,256]{1,0:T(8,128)(2,1)S(1)}, bf16[3072,256]{1,0:T(8,128)(2,1)}) custom-call(bf16[1,2048,256]{2,1,0:T(8,128)(2,1)} %gate_ref.1, bf16[1,2048,256]{2,1,0:T(8,128)(2,1)} %up_ref.1, bf16[1,256,2048]{2,1,0:T(8,128)(2,1)} %down_ref.1), custom_call_target="tpu_custom_call" | custom-call | tf_op jit(solution)/shard_map/pack/pallas_call | solution.py:74
  3.9 0.0 copy-start.4
  3.9 0.0 copy-start.5
  3.9 5.6 %collective-permute-start.8 = (bf16[3072,256]{1,0:T(8,128)(2,1)}, bf16[3072,256]{1,0:T(8,128)(2,1)}, u32[]{:S(2)}, u32[]{:S(2)}) collective-permute-start(bf16[3072,256]{1,0:T(8,128)(2,1)} %get-tuple-element.8.refs_1_), channel_id=1, source_target_pairs={{0,3},{1,0},{2,1},{3,2},{4,7},{5,4},{6,5},{7,6},{8,11},{9,8},{10,9... | collective-permute-start | bytes 4718600 | tf_op jit(solution)/shard_map/ppermute | solution.py:53
  9.5 1.9 %collective-permute-start.5 = (bf16[3072,256]{1,0:T(8,128)(2,1)S(1)}, bf16[3072,256]{1,0:T(8,128)(2,1)}, u32[]{:S(2)}, u32[]{:S(2)}) collective-permute-start(bf16[3072,256]{1,0:T(8,128)(2,1)S(1)} %get-tuple-element.7.refs_0_), channel_id=1, source_target_pairs={{0,1},{1,2},{2,3},{3,0},{4,5},{5,6},{6,7},{7,4},{8,9},{9,10},{10,1... | collective-permute-start | bytes 4718600 | tf_op jit(solution)/shard_map/ppermute | solution.py:53
  11.4 0.0 copy-done.2
  11.4 0.0 copy-done.3
  11.5 0.0 copy-done
  11.5 2.4 %prep.1 = (bf16[256,512]{1,0:T(8,128)(2,1)}, s32[256,128]{1,0:T(8,128)S(1)}) custom-call(bf16[256,2048]{1,0:T(8,128)(2,1)S(1)} %copy-done, f32[1,2048]{1,0:T(1,128)S(1)} %bitcast.11, s32[2,256]{1,0:T(2,128)S(1)} %bitcast.12), custom_call_target="tpu_custom_call" | custom-call | tf_op jit(solution)/shard_map/prep/pallas_call | solution.py:136
  13.8 16.1 %all-to-all-start = ((bf16[32,8,512]{2,1,0:T(8,128)(2,1)}), bf16[32,8,512]{2,1,0:T(8,128)(2,1)S(1)}, u32[]{:S(2)}, u32[]{:S(2)}) async-start(bf16[32,8,512]{2,1,0:T(8,128)(2,1)} %bitcast.2), calls=%async_computation | async-start | bytes 524288 | tf_op jit(solution)/shard_map/all_to_all | solution.py:367
  29.9 3.2 %collective-permute-start.6 = (bf16[3072,256]{1,0:T(8,128)(2,1)}, bf16[3072,256]{1,0:T(8,128)(2,1)}, u32[]{:S(2)}, u32[]{:S(2)}) collective-permute-start(bf16[3072,256]{1,0:T(8,128)(2,1)} %get-tuple-element.8.refs_1_), channel_id=1, source_target_pairs={{0,1},{1,2},{2,3},{3,0},{4,5},{5,6},{6,7},{7,4},{8,9},{9,10},{10,1... | collective-permute-start | bytes 4718600 | tf_op jit(solution)/shard_map/ppermute | solution.py:53
  33.1 3.4 %collective-permute-start.7 = (bf16[3072,256]{1,0:T(8,128)(2,1)S(1)}, bf16[3072,256]{1,0:T(8,128)(2,1)}, u32[]{:S(2)}, u32[]{:S(2)}) collective-permute-start(bf16[3072,256]{1,0:T(8,128)(2,1)S(1)} %get-tuple-element.7.refs_0_), channel_id=1, source_target_pairs={{0,3},{1,0},{2,1},{3,2},{4,7},{5,4},{6,5},{7,6},{8,11},{9,8},{10,9... | collective-permute-start | bytes 4718600 | tf_op jit(solution)/shard_map/ppermute | solution.py:53
  36.5 0.1 dynamic-slice_bitcast_fusion
  36.7 4.0 %collective-permute-start = (bf16[2,128,64]{2,1,0:T(8,128)(2,1)S(1)}, bf16[2,128,64]{2,1,0:T(8,128)(2,1)S(1)}, u32[]{:S(2)}, u32[]{:S(2)}) collective-permute-start(bf16[2,128,64]{2,1,0:T(8,128)(2,1)S(1)} %get-tuple-element.11), channel_id=1, source_target_pairs={{0,16},{16,32},{32,48},{48,64},{64,80},{80,96},{96,112},{112,128},... | collective-permute-start | bytes 98312 | tf_op jit(solution)/shard_map/ppermute | solution.py:324
  40.8 0.0 collective-permute-done.8.refs_5_
  40.8 4.6 %collective-permute-start.10 = (bf16[3072,256]{1,0:T(8,128)(2,1)}, bf16[3072,256]{1,0:T(8,128)(2,1)}, u32[]{:S(2)}, u32[]{:S(2)}) collective-permute-start(bf16[3072,256]{1,0:T(8,128)(2,1)} %collective-permute-done.8.refs_5_), channel_id=1, source_target_pairs={{0,3},{1,0},{2,1},{3,2},{4,7},{5,4},{6,5},{7,6},{8,11},{9,8},{10,9... | collective-permute-start | bytes 4718600 | tf_op jit(solution)/shard_map/ppermute | solution.py:53
  45.4 0.0 collective-permute-done.5.refs_2_
  45.4 1.9 %collective-permute-start.9 = (bf16[3072,256]{1,0:T(8,128)(2,1)}, bf16[3072,256]{1,0:T(8,128)(2,1)}, u32[]{:S(2)}, u32[]{:S(2)}) collective-permute-start(bf16[3072,256]{1,0:T(8,128)(2,1)} %collective-permute-done.5.refs_2_), channel_id=1, source_target_pairs={{0,1},{1,2},{2,3},{3,0},{4,5},{5,6},{6,7},{7,4},{8,9},{9,10},{10,1... | collective-permute-start | bytes 4718600 | tf_op jit(solution)/shard_map/ppermute | solution.py:53
  47.4 1.4 fusion
  48.8 0.0 collective-permute-done.low_ref
  48.8 1.9 %collective-permute-start.1 = (bf16[2,128,64]{2,1,0:T(8,128)(2,1)S(1)}, bf16[2,128,64]{2,1,0:T(8,128)(2,1)S(1)}, u32[]{:S(2)}, u32[]{:S(2)}) collective-permute-start(bf16[2,128,64]{2,1,0:T(8,128)(2,1)S(1)} %get-tuple-element.10), channel_id=1, source_target_pairs={{16,0},{32,16},{48,32},{64,48},{80,64},{96,80},{112,96},{128,112},... | collective-permute-start | bytes 98312 | tf_op jit(solution)/shard_map/ppermute | solution.py:325
  50.8 0.1 pad_maximum_fusion.kv_ref
  50.8 0.1 copy.17.q_ref
  51.6 3.2 %collective-permute-done.1.high_ref = bf16[2,128,64]{2,1,0:T(8,128)(2,1)S(1)} collective-permute-done((bf16[2,128,64]{2,1,0:T(8,128)(2,1)S(1)}, bf16[2,128,64]{2,1,0:T(8,128)(2,1)S(1)}, u32[]{:S(2)}, u32[]{:S(2)}) %collective-permute-start.1) | collective-permute-done | bytes 32800 | tf_op jit(solution)/shard_map/ppermute | solution.py:325
  54.8 1.3 attend.1
  56.1 0.0 all-to-all-done
  56.2 1.2 broadcast_in_dim.9
  57.4 3.5 %all-to-all-start.1 = ((bf16[4,320,512]{2,1,0:T(8,128)(2,1)}), bf16[4,320,512]{2,1,0:T(8,128)(2,1)S(1)}, u32[]{:S(2)}, u32[]{:S(2)}) async-start(bf16[4,320,512]{2,1,0:T(8,128)(2,1)} %broadcast_in_dim.9), calls=%async_computation.1 | async-start | bytes 2621440 | tf_op jit(solution)/shard_map/all_to_all | solution.py:374
  60.9 0.0 collective-permute-done.6.refs_3_
  60.9 0.0 collective-permute-done.7.refs_4_
  60.9 17.6 %all-to-all-done.1.x_ref = bf16[4,320,512]{2,1,0:T(8,128)(2,1)S(1)} async-done(((bf16[4,320,512]{2,1,0:T(8,128)(2,1)}), bf16[4,320,512]{2,1,0:T(8,128)(2,1)S(1)}, u32[]{:S(2)}, u32[]{:S(2)}) %all-to-all-start.1) | async-done | bytes 1310752 | tf_op jit(solution)/shard_map/all_to_all | solution.py:374
  78.5 0.1 collective-permute-done.10.refs_7_
  78.6 0.0 collective-permute-done.9.refs_6_
  78.6 6.7 %ffn.1 = bf16[16,256,128]{2,1,0:T(8,128)(2,1)} custom-call(bf16[4,320,512]{2,1,0:T(8,128)(2,1)S(1)} %all-to-all-done.1.x_ref, bf16[3072,256]{1,0:T(8,128)(2,1)S(1)} %get-tuple-element.7.refs_0_, bf16[3072,256]{1,0:T(8,128)(2,1)} %get-tuple-element.8.refs_1_, bf16[3072,256]{1,0:T(8,128)(2,1)} %collective-permute-done.5.refs_2_, ...), custom_call_target="tpu_custom_call" | custom-call | tf_op jit(solution)/shard_map/ffn/pallas_call | solution.py:196
  85.3 22.1 %all_to_all.27.parts_ref = bf16[16,256,128]{2,1,0:T(8,128)(2,1)S(1)} all-to-all(bf16[16,256,128]{2,1,0:T(8,128)(2,1)} %ffn.1), channel_id=1, replica_groups={{0,1,2,3,4,5,6,7,8,9,10,11,12,13,14,15},{16,20,24,28,17,21,25,29,18,22,..., dimensions={0} | all-to-all | bytes 2097152 | tf_op jit(solution)/shard_map/all_to_all | solution.py:379
  107.4 0.8 total.1
  108.3 14.4 %all-to-all-start.3 = ((bf16[32,32,128]{2,1,0:T(8,128)(2,1)}), bf16[32,32,128]{2,1,0:T(8,128)(2,1)S(1)}, u32[]{:S(2)}, u32[]{:S(2)}) async-start(bf16[32,32,128]{2,1,0:T(8,128)(2,1)} %bitcast.6), calls=%async_computation.3 | async-start | bytes 524288 | tf_op jit(solution)/shard_map/all_to_all | solution.py:381
  122.7 1.9 %collective-permute-start.2 = (bf16[4,64,512]{2,1,0:T(8,128)(2,1)S(1)}, bf16[4,64,512]{2,1,0:T(8,128)(2,1)S(1)}, u32[]{:S(2)}, u32[]{:S(2)}) collective-permute-start(bf16[4,64,512]{2,1,0:T(8,128)(2,1)S(1)} %slice.16.own_ref), channel_id=1, source_target_pairs={{0,1},{1,2},{2,3},{3,0},{4,5},{5,6},{6,7},{7,4},{8,9},{9,10},{10,1... | collective-permute-start | bytes 786440 | tf_op jit(solution)/shard_map/ppermute | solution.py:53
  124.6 4.6 %collective-permute-start.3 = (bf16[4,64,512]{2,1,0:T(8,128)(2,1)S(1)}, bf16[4,64,512]{2,1,0:T(8,128)(2,1)S(1)}, u32[]{:S(2)}, u32[]{:S(2)}) collective-permute-start(bf16[4,64,512]{2,1,0:T(8,128)(2,1)S(1)} %slice.16.own_ref), channel_id=1, source_target_pairs={{0,3},{1,0},{2,1},{3,2},{4,7},{5,4},{6,5},{7,6},{8,11},{9,8},{10,9... | collective-permute-start | bytes 786440 | tf_op jit(solution)/shard_map/ppermute | solution.py:53
  129.2 1.9 %collective-permute-start.4 = (bf16[4,64,512]{2,1,0:T(8,128)(2,1)S(1)}, bf16[4,64,512]{2,1,0:T(8,128)(2,1)S(1)}, u32[]{:S(2)}, u32[]{:S(2)}) collective-permute-start(bf16[4,64,512]{2,1,0:T(8,128)(2,1)S(1)} %slice.16.own_ref), channel_id=1, source_target_pairs={{0,2},{1,3},{2,0},{3,1},{4,6},{5,7},{6,4},{7,5},{8,10},{9,11},{10,... | collective-permute-start | bytes 786440 | tf_op jit(solution)/shard_map/ppermute | solution.py:53
  131.2 0.1 copy.18.weight_ref
  131.3 0.0 collective-permute-done.2.prev_ref
  131.3 4.0 %collective-permute-done.3.next_ref = bf16[4,64,512]{2,1,0:T(8,128)(2,1)S(1)} collective-permute-done((bf16[4,64,512]{2,1,0:T(8,128)(2,1)S(1)}, bf16[4,64,512]{2,1,0:T(8,128)(2,1)S(1)}, u32[]{:S(2)}, u32[]{:S(2)}) %collective-permute-start.3) | collective-permute-done | bytes 262176 | tf_op jit(solution)/shard_map/ppermute | solution.py:53
  135.3 2.8 %collective-permute-done.4.far_ref = bf16[4,64,512]{2,1,0:T(8,128)(2,1)S(1)} collective-permute-done((bf16[4,64,512]{2,1,0:T(8,128)(2,1)S(1)}, bf16[4,64,512]{2,1,0:T(8,128)(2,1)S(1)}, u32[]{:S(2)}, u32[]{:S(2)}) %collective-permute-start.4) | collective-permute-done | bytes 262176 | tf_op jit(solution)/shard_map/ppermute | solution.py:53
  138.1 1.1 project.1
  139.3 5.7 %all-to-all-done.3 = bf16[32,32,128]{2,1,0:T(8,128)(2,1)S(1)} async-done(((bf16[32,32,128]{2,1,0:T(8,128)(2,1)}), bf16[32,32,128]{2,1,0:T(8,128)(2,1)S(1)}, u32[]{:S(2)}, u32[]{:S(2)}) %all-to-all-start.3) | async-done | bytes 262176 | tf_op jit(solution)/shard_map/all_to_all | solution.py:381
  144.9 1.1 combine.1
  (15 shorter events, 0.1 us)
Async XLA Ops:
  0.6 10.8 %copy-start.2 = (f32[2048]{0:T(1024)S(1)}, f32[2048]{0:T(1024)}, u32[]{:S(2)}) copy-start(f32[2048]{0:T(1024)} %param.18) | copy-start | bytes 24580
  0.6 10.8 %copy-start.3 = (s32[256,2]{0,1:T(2,128)S(1)}, s32[256,2]{0,1:T(2,128)}, u32[]{:S(2)}) copy-start(s32[256,2]{0,1:T(2,128)} %param.19) | copy-start | bytes 6148
  0.7 10.8 %copy-start = (bf16[256,2048]{1,0:T(8,128)(2,1)S(1)}, bf16[256,2048]{1,0:T(8,128)(2,1)}, u32[]{:S(2)}) copy-start(bf16[256,2048]{1,0:T(8,128)(2,1)} %x_ref.1) | copy-start | bytes 3145732
  3.9 32.6 %copy-start.4 = (bf16[512,256]{1,0:T(8,128)(2,1)S(1)}, bf16[512,256]{1,0:T(8,128)(2,1)}, u32[]{:S(2)}) copy-start(bf16[512,256]{1,0:T(8,128)(2,1)} %param.14) | copy-start | bytes 786436
  3.9 32.6 %copy-start.5 = (bf16[512,256]{1,0:T(8,128)(2,1)S(1)}, bf16[512,256]{1,0:T(8,128)(2,1)}, u32[]{:S(2)}) copy-start(bf16[512,256]{1,0:T(8,128)(2,1)} %param.13) | copy-start | bytes 786436
  3.9 36.9 %collective-permute-start.8 = (bf16[3072,256]{1,0:T(8,128)(2,1)}, bf16[3072,256]{1,0:T(8,128)(2,1)}, u32[]{:S(2)}, u32[]{:S(2)}) collective-permute-start(bf16[3072,256]{1,0:T(8,128)(2,1)} %get-tuple-element.8.refs_1_), channel_id=1, source_target_pairs={{0,3},{1,0},{2,1},{3,2},{4,7},{5,4},{6,5},{7,6},{8,11},{9,8},{10,9... | collective-permute-start | bytes 4718600 | tf_op jit(solution)/shard_map/ppermute | solution.py:53
  9.5 35.9 %collective-permute-start.5 = (bf16[3072,256]{1,0:T(8,128)(2,1)S(1)}, bf16[3072,256]{1,0:T(8,128)(2,1)}, u32[]{:S(2)}, u32[]{:S(2)}) collective-permute-start(bf16[3072,256]{1,0:T(8,128)(2,1)S(1)} %get-tuple-element.7.refs_0_), channel_id=1, source_target_pairs={{0,1},{1,2},{2,3},{3,0},{4,5},{5,6},{6,7},{7,4},{8,9},{9,10},{10,1... | collective-permute-start | bytes 4718600 | tf_op jit(solution)/shard_map/ppermute | solution.py:53
  13.8 37.0 %copy-start.6 = (bf16[512,64]{0,1:T(8,128)(2,1)S(1)}, bf16[512,64]{0,1:T(8,128)(2,1)}, u32[]{:S(2)}) copy-start(bf16[512,64]{0,1:T(8,128)(2,1)} %param.12) | copy-start | bytes 196612
  13.8 42.3 %all-to-all-start = ((bf16[32,8,512]{2,1,0:T(8,128)(2,1)}), bf16[32,8,512]{2,1,0:T(8,128)(2,1)S(1)}, u32[]{:S(2)}, u32[]{:S(2)}) async-start(bf16[32,8,512]{2,1,0:T(8,128)(2,1)} %bitcast.2), calls=%async_computation | async-start | bytes 524288 | tf_op jit(solution)/shard_map/all_to_all | solution.py:367
  29.9 31.0 %collective-permute-start.6 = (bf16[3072,256]{1,0:T(8,128)(2,1)}, bf16[3072,256]{1,0:T(8,128)(2,1)}, u32[]{:S(2)}, u32[]{:S(2)}) collective-permute-start(bf16[3072,256]{1,0:T(8,128)(2,1)} %get-tuple-element.8.refs_1_), channel_id=1, source_target_pairs={{0,1},{1,2},{2,3},{3,0},{4,5},{5,6},{6,7},{7,4},{8,9},{9,10},{10,1... | collective-permute-start | bytes 4718600 | tf_op jit(solution)/shard_map/ppermute | solution.py:53
  33.1 27.8 %collective-permute-start.7 = (bf16[3072,256]{1,0:T(8,128)(2,1)S(1)}, bf16[3072,256]{1,0:T(8,128)(2,1)}, u32[]{:S(2)}, u32[]{:S(2)}) collective-permute-start(bf16[3072,256]{1,0:T(8,128)(2,1)S(1)} %get-tuple-element.7.refs_0_), channel_id=1, source_target_pairs={{0,3},{1,0},{2,1},{3,2},{4,7},{5,4},{6,5},{7,6},{8,11},{9,8},{10,9... | collective-permute-start | bytes 4718600 | tf_op jit(solution)/shard_map/ppermute | solution.py:53
  36.7 12.1 %collective-permute-start = (bf16[2,128,64]{2,1,0:T(8,128)(2,1)S(1)}, bf16[2,128,64]{2,1,0:T(8,128)(2,1)S(1)}, u32[]{:S(2)}, u32[]{:S(2)}) collective-permute-start(bf16[2,128,64]{2,1,0:T(8,128)(2,1)S(1)} %get-tuple-element.11), channel_id=1, source_target_pairs={{0,16},{16,32},{32,48},{48,64},{64,80},{80,96},{96,112},{112,128},... | collective-permute-start | bytes 98312 | tf_op jit(solution)/shard_map/ppermute | solution.py:324
  40.8 37.8 %collective-permute-start.10 = (bf16[3072,256]{1,0:T(8,128)(2,1)}, bf16[3072,256]{1,0:T(8,128)(2,1)}, u32[]{:S(2)}, u32[]{:S(2)}) collective-permute-start(bf16[3072,256]{1,0:T(8,128)(2,1)} %collective-permute-done.8.refs_5_), channel_id=1, source_target_pairs={{0,3},{1,0},{2,1},{3,2},{4,7},{5,4},{6,5},{7,6},{8,11},{9,8},{10,9... | collective-permute-start | bytes 4718600 | tf_op jit(solution)/shard_map/ppermute | solution.py:53
  45.4 33.1 %collective-permute-start.9 = (bf16[3072,256]{1,0:T(8,128)(2,1)}, bf16[3072,256]{1,0:T(8,128)(2,1)}, u32[]{:S(2)}, u32[]{:S(2)}) collective-permute-start(bf16[3072,256]{1,0:T(8,128)(2,1)} %collective-permute-done.5.refs_2_), channel_id=1, source_target_pairs={{0,1},{1,2},{2,3},{3,0},{4,5},{5,6},{6,7},{7,4},{8,9},{9,10},{10,1... | collective-permute-start | bytes 4718600 | tf_op jit(solution)/shard_map/ppermute | solution.py:53
  48.8 6.0 %collective-permute-start.1 = (bf16[2,128,64]{2,1,0:T(8,128)(2,1)S(1)}, bf16[2,128,64]{2,1,0:T(8,128)(2,1)S(1)}, u32[]{:S(2)}, u32[]{:S(2)}) collective-permute-start(bf16[2,128,64]{2,1,0:T(8,128)(2,1)S(1)} %get-tuple-element.10), channel_id=1, source_target_pairs={{16,0},{32,16},{48,32},{64,48},{80,64},{96,80},{112,96},{128,112},... | collective-permute-start | bytes 98312 | tf_op jit(solution)/shard_map/ppermute | solution.py:325
  57.4 21.2 %all-to-all-start.1 = ((bf16[4,320,512]{2,1,0:T(8,128)(2,1)}), bf16[4,320,512]{2,1,0:T(8,128)(2,1)S(1)}, u32[]{:S(2)}, u32[]{:S(2)}) async-start(bf16[4,320,512]{2,1,0:T(8,128)(2,1)} %broadcast_in_dim.9), calls=%async_computation.1 | async-start | bytes 2621440 | tf_op jit(solution)/shard_map/all_to_all | solution.py:374
  107.4 23.7 %copy-start.7 = (f32[256,2]{0,1:T(2,128)S(1)}, f32[256,2]{0,1:T(2,128)}, u32[]{:S(2)}) copy-start(f32[256,2]{0,1:T(2,128)} %param.20) | copy-start | bytes 6148
  107.4 30.7 %copy-start.1 = (bf16[1024,128]{1,0:T(8,128)(2,1)S(1)}, bf16[1024,128]{1,0:T(8,128)(2,1)}, u32[]{:S(2)}) copy-start(bf16[1024,128]{1,0:T(8,128)(2,1)} %weight_ref.2) | copy-start | bytes 786436
  108.3 36.7 %all-to-all-start.3 = ((bf16[32,32,128]{2,1,0:T(8,128)(2,1)}), bf16[32,32,128]{2,1,0:T(8,128)(2,1)S(1)}, u32[]{:S(2)}, u32[]{:S(2)}) async-start(bf16[32,32,128]{2,1,0:T(8,128)(2,1)} %bitcast.6), calls=%async_computation.3 | async-start | bytes 524288 | tf_op jit(solution)/shard_map/all_to_all | solution.py:381
  122.7 8.6 %collective-permute-start.2 = (bf16[4,64,512]{2,1,0:T(8,128)(2,1)S(1)}, bf16[4,64,512]{2,1,0:T(8,128)(2,1)S(1)}, u32[]{:S(2)}, u32[]{:S(2)}) collective-permute-start(bf16[4,64,512]{2,1,0:T(8,128)(2,1)S(1)} %slice.16.own_ref), channel_id=1, source_target_pairs={{0,1},{1,2},{2,3},{3,0},{4,5},{5,6},{6,7},{7,4},{8,9},{9,10},{10,1... | collective-permute-start | bytes 786440 | tf_op jit(solution)/shard_map/ppermute | solution.py:53
  124.6 10.7 %collective-permute-start.3 = (bf16[4,64,512]{2,1,0:T(8,128)(2,1)S(1)}, bf16[4,64,512]{2,1,0:T(8,128)(2,1)S(1)}, u32[]{:S(2)}, u32[]{:S(2)}) collective-permute-start(bf16[4,64,512]{2,1,0:T(8,128)(2,1)S(1)} %slice.16.own_ref), channel_id=1, source_target_pairs={{0,3},{1,0},{2,1},{3,2},{4,7},{5,4},{6,5},{7,6},{8,11},{9,8},{10,9... | collective-permute-start | bytes 786440 | tf_op jit(solution)/shard_map/ppermute | solution.py:53
  129.2 8.9 %collective-permute-start.4 = (bf16[4,64,512]{2,1,0:T(8,128)(2,1)S(1)}, bf16[4,64,512]{2,1,0:T(8,128)(2,1)S(1)}, u32[]{:S(2)}, u32[]{:S(2)}) collective-permute-start(bf16[4,64,512]{2,1,0:T(8,128)(2,1)S(1)} %slice.16.own_ref), channel_id=1, source_target_pairs={{0,2},{1,3},{2,0},{3,1},{4,6},{5,7},{6,4},{7,5},{8,10},{9,11},{10,... | collective-permute-start | bytes 786440 | tf_op jit(solution)/shard_map/ppermute | solution.py:53

commit v8 on v7

--- a/solution.py
+++ b/solution.py
@@ -48,8 +48,13 @@
     return pltpu.CompilerParams(vmem_limit_bytes=count << 20)
 
 
-def line_shift(x, step):
-    pairs = [(line[i], line[(i + step) % 4]) for line in LINE_L for i in range(4)]
+NEAR_A = (1, 0, 3, 2)
+NEAR_B = (3, 2, 1, 0)
+ACROSS = (2, 3, 0, 1)
+
+
+def swap(x, partner):
+    pairs = [(line[i], line[partner[i]]) for line in LINE_L for i in range(4)]
     return lax.ppermute(x, PLANE, pairs)
 
 
@@ -249,11 +254,16 @@
     )(resident(returned), slots, route_weights)
 
 
-def project_kernel(own_ref, prev_ref, next_ref, far_ref, weight_ref, out_ref, a_ref):
+def project_kernel(own_ref, one_ref, two_ref, far_ref, weight_ref, out_ref, a_ref):
     core = lax.axis_index("co")
     line = jnp.where(core == 0, lax.axis_index("x"), lax.axis_index("y"))
-    for ref, step in ((own_ref, 0), (prev_ref, 3), (next_ref, 1), (far_ref, 2)):
-        source = lax.rem(line + step, 4)
+    odd = lax.rem(line, 2)
+    for ref, source in (
+        (own_ref, line),
+        (one_ref, line + 1 - 2 * odd),
+        (two_ref, 3 - line),
+        (far_ref, lax.rem(line + 2, 4)),
+    ):
         for m in range(4):
             head = jnp.where(core == 0, m * 4 + source, source * 4 + m)
             a_ref[pl.ds(pl.multiple_of(head * HEAD_DIM, HEAD_DIM), HEAD_DIM), :] = ref[m]
@@ -262,7 +272,7 @@
     out_ref[...] = out.T.astype(jnp.bfloat16)
 
 
-def project(own, prev, nxt, far, out_weight):
+def project(own, one, two, far, out_weight):
     return pl.pallas_call(
         project_kernel,
         out_shape=jax.ShapeDtypeStruct((512, 128), jnp.bfloat16),
@@ -271,7 +281,7 @@
         scratch_shapes=[pltpu.VMEM((1024, 512), jnp.bfloat16)],
         compiler_params=vmem_mib(12),
         name="project",
-    )(*(resident(a) for a in (own, prev, nxt, far, out_weight)))
+    )(*(resident(a) for a in (own, one, two, far, out_weight)))
 
 
 def attend_kernel(q_ref, kv_ref, low_ref, high_ref, cos_ref, sin_ref, sink_ref, out_ref,
@@ -359,14 +369,14 @@
     down_weight,
 ):
     wa, wb = pack(gate_weight, up_weight, down_weight)
-    prev_a = line_shift(wa, 1)
-    next_b = line_shift(wb, -1)
-    next_a = line_shift(wa, -1)
-    prev_b = line_shift(wb, 1)
+    one_a = swap(wa, NEAR_A)
+    two_b = swap(wb, NEAR_B)
+    one_b = swap(wb, NEAR_A)
+    two_a = swap(wa, NEAR_B)
     outgoing, slots = prepare(expert_input, norm_gain, routes)
     arrived = lax.all_to_all(outgoing, EP, 0, 0, tiled=True)
-    far_a = line_shift(prev_a, 1)
-    far_b = line_shift(next_b, -1)
+    far_a = swap(one_a, NEAR_B)
+    far_b = swap(two_b, NEAR_A)
 
     attended = attend(query_proj, key_proj, value_proj, sink_logit)
 
@@ -375,15 +385,15 @@
         jnp.broadcast_to(payload[None], (4, *payload.shape)),
         PLANE, 0, 0, tiled=True, axis_index_groups=LINE_M,
     )
-    partial = ffn(rows, (wa, wb, prev_a, prev_b, next_a, next_b, far_a, far_b))
+    partial = ffn(rows, (wa, wb, one_a, one_b, two_a, two_b, far_a, far_b))
     parts = lax.all_to_all(partial, PLANE, 0, 0, tiled=True, axis_index_groups=WHOLE)
     result = total(parts).reshape(EXPERTS, CAP, 128)
     returned = lax.all_to_all(result, EP, 0, 0, tiled=True)
     expert_out = combine(returned.reshape(EXPERTS * CAP, 128), slots, route_weights)
 
     heads = rows[:, 256:]
-    near = [line_shift(heads, step) for step in (1, -1)]
-    far = line_shift(heads, 2)
+    near = [swap(heads, partner) for partner in (NEAR_A, NEAR_B)]
+    far = swap(heads, ACROSS)
     mixer_out = project(heads, *near, far, out_weight)
     return (mixer_out, expert_out)
 

time: 147 us -> 146 us (level)
  blocking collectives: 22.1 us -> 19.4 us
    all_to_all x1, blocking collectives: 22.1 us -> 19.4 us  [local(): lax.all_to_all(partial, PLANE, 0, 0, tiled=True, axis_index_groups=WHOLE)]
    all_to_all x1, waiting for transfers between devices: 5.67 us -> 7.44 us  [local(): returned = lax.all_to_all(result, EP, 0, 0, tiled=True)]
where the time goes in v8:
time: 146 us; the launch traced here: 145 us
  starting transfers between devices  69.8 us (48%)
  waiting for transfers between devices  34.3 us (23%)
  blocking collectives  19.4 us (13%)
  Pallas kernels  16.7 us (11%)
  between operations  1.64 us (1%)
  local copies, waits for them, and re-layouts  1.63 us (1%)
  other arithmetic  1.57 us (1%)
    ppermute x9, starting transfers between devices, swap(): return lax.ppermute(x, PLANE, pairs)  30 us
    all_to_all x1, blocking collectives, local(): lax.all_to_all(partial, PLANE, 0, 0, tiled=True, axis_index_groups=WHOLE)  19.4 us
    all_to_all x1, waiting for transfers between devices, local(): lax.all_to_all(jnp.broadcast_to(payload[None], (4, *payload.shape)), PLAN...  17.1 us
    all_to_all x1, starting transfers between devices, local(): arrived = lax.all_to_all(outgoing, EP, 0, 0, tiled=True)  16.3 us
    all_to_all x1, starting transfers between devices, local(): returned = lax.all_to_all(result, EP, 0, 0, tiled=True)  14.7 us
    all_to_all x1, waiting for transfers between devices, local(): returned = lax.all_to_all(result, EP, 0, 0, tiled=True)  7.44 us
    pallas_call x1, Pallas kernels, ffn(): pl.pallas_call(ffn_kernel, out_shape=pltpu.HBM((16, ROWS_B, 128), jnp.bfl...  6.7 us
    ppermute x9, waiting for transfers between devices, swap(): return lax.ppermute(x, PLANE, pairs)  6.59 us
  transfers between devices with their start and end apart: 14, of which 6 were waited for; matrix products, arithmetic and copies ran while one was open for 2% of the time, Pallas kernels for 3%

profile of v8, /device:TPU:1, one launch (start us, length us, event | category | flops | bytes accessed | tf_op | source)
XLA Modules:
  0.0 145.0 jit_solution(10603891536566057536)
XLA Ops:
  0.7 3.2 %pack.1 = (bf16[3072,256]{1,0:T(8,128)(2,1)S(1)}, bf16[3072,256]{1,0:T(8,128)(2,1)}) custom-call(bf16[1,2048,256]{2,1,0:T(8,128)(2,1)} %gate_ref.1, bf16[1,2048,256]{2,1,0:T(8,128)(2,1)} %up_ref.1, bf16[1,256,2048]{2,1,0:T(8,128)(2,1)} %down_ref.1), custom_call_target="tpu_custom_call" | custom-call | tf_op jit(solution)/shard_map/pack/pallas_call | solution.py:79
  3.9 0.0 copy-start.4
  3.9 0.0 copy-start.5
  3.9 5.6 %collective-permute-start.8 = (bf16[3072,256]{1,0:T(8,128)(2,1)}, bf16[3072,256]{1,0:T(8,128)(2,1)}, u32[]{:S(2)}, u32[]{:S(2)}) collective-permute-start(bf16[3072,256]{1,0:T(8,128)(2,1)} %get-tuple-element.8.refs_1_), channel_id=1, source_target_pairs={{0,3},{1,2},{2,1},{3,0},{4,7},{5,6},{6,5},{7,4},{8,11},{9,10},{10,... | collective-permute-start | bytes 4718600 | tf_op jit(solution)/shard_map/ppermute | solution.py:58
  9.5 1.9 %collective-permute-start.5 = (bf16[3072,256]{1,0:T(8,128)(2,1)S(1)}, bf16[3072,256]{1,0:T(8,128)(2,1)}, u32[]{:S(2)}, u32[]{:S(2)}) collective-permute-start(bf16[3072,256]{1,0:T(8,128)(2,1)S(1)} %get-tuple-element.7.refs_0_), channel_id=1, source_target_pairs={{0,1},{1,0},{2,3},{3,2},{4,5},{5,4},{6,7},{7,6},{8,9},{9,8},{10,11... | collective-permute-start | bytes 4718600 | tf_op jit(solution)/shard_map/ppermute | solution.py:58
  11.4 0.0 copy-done.2
  11.4 0.0 copy-done.3
  11.5 0.0 copy-done
  11.5 2.4 %prep.1 = (bf16[256,512]{1,0:T(8,128)(2,1)}, s32[256,128]{1,0:T(8,128)S(1)}) custom-call(bf16[256,2048]{1,0:T(8,128)(2,1)S(1)} %copy-done, f32[1,2048]{1,0:T(1,128)S(1)} %bitcast.11, s32[2,256]{1,0:T(2,128)S(1)} %bitcast.12), custom_call_target="tpu_custom_call" | custom-call | tf_op jit(solution)/shard_map/prep/pallas_call | solution.py:141
  13.8 16.3 %all-to-all-start = ((bf16[32,8,512]{2,1,0:T(8,128)(2,1)}), bf16[32,8,512]{2,1,0:T(8,128)(2,1)S(1)}, u32[]{:S(2)}, u32[]{:S(2)}) async-start(bf16[32,8,512]{2,1,0:T(8,128)(2,1)} %bitcast.2), calls=%async_computation | async-start | bytes 524288 | tf_op jit(solution)/shard_map/all_to_all | solution.py:377
  30.1 3.2 %collective-permute-start.6 = (bf16[3072,256]{1,0:T(8,128)(2,1)}, bf16[3072,256]{1,0:T(8,128)(2,1)}, u32[]{:S(2)}, u32[]{:S(2)}) collective-permute-start(bf16[3072,256]{1,0:T(8,128)(2,1)} %get-tuple-element.8.refs_1_), channel_id=1, source_target_pairs={{0,1},{1,0},{2,3},{3,2},{4,5},{5,4},{6,7},{7,6},{8,9},{9,8},{10,11... | collective-permute-start | bytes 4718600 | tf_op jit(solution)/shard_map/ppermute | solution.py:58
  33.4 3.8 %collective-permute-start.7 = (bf16[3072,256]{1,0:T(8,128)(2,1)S(1)}, bf16[3072,256]{1,0:T(8,128)(2,1)}, u32[]{:S(2)}, u32[]{:S(2)}) collective-permute-start(bf16[3072,256]{1,0:T(8,128)(2,1)S(1)} %get-tuple-element.7.refs_0_), channel_id=1, source_target_pairs={{0,3},{1,2},{2,1},{3,0},{4,7},{5,6},{6,5},{7,4},{8,11},{9,10},{10,... | collective-permute-start | bytes 4718600 | tf_op jit(solution)/shard_map/ppermute | solution.py:58
  37.2 0.1 dynamic-slice_bitcast_fusion
  37.4 3.1 %collective-permute-start = (bf16[2,128,64]{2,1,0:T(8,128)(2,1)S(1)}, bf16[2,128,64]{2,1,0:T(8,128)(2,1)S(1)}, u32[]{:S(2)}, u32[]{:S(2)}) collective-permute-start(bf16[2,128,64]{2,1,0:T(8,128)(2,1)S(1)} %get-tuple-element.11), channel_id=1, source_target_pairs={{0,16},{16,32},{32,48},{48,64},{64,80},{80,96},{96,112},{112,128},... | collective-permute-start | bytes 98312 | tf_op jit(solution)/shard_map/ppermute | solution.py:334
  40.5 0.0 collective-permute-done.8.refs_5_
  40.5 3.4 %collective-permute-start.10 = (bf16[3072,256]{1,0:T(8,128)(2,1)}, bf16[3072,256]{1,0:T(8,128)(2,1)}, u32[]{:S(2)}, u32[]{:S(2)}) collective-permute-start(bf16[3072,256]{1,0:T(8,128)(2,1)} %collective-permute-done.8.refs_5_), channel_id=1, source_target_pairs={{0,1},{1,0},{2,3},{3,2},{4,5},{5,4},{6,7},{7,6},{8,9},{9,8},{10,11... | collective-permute-start | bytes 4718600 | tf_op jit(solution)/shard_map/ppermute | solution.py:58
  43.9 0.0 collective-permute-done.5.refs_2_
  43.9 3.1 %collective-permute-start.9 = (bf16[3072,256]{1,0:T(8,128)(2,1)}, bf16[3072,256]{1,0:T(8,128)(2,1)}, u32[]{:S(2)}, u32[]{:S(2)}) collective-permute-start(bf16[3072,256]{1,0:T(8,128)(2,1)} %collective-permute-done.5.refs_2_), channel_id=1, source_target_pairs={{0,3},{1,2},{2,1},{3,0},{4,7},{5,6},{6,5},{7,4},{8,11},{9,10},{10,... | collective-permute-start | bytes 4718600 | tf_op jit(solution)/shard_map/ppermute | solution.py:58
  47.1 1.4 fusion
  48.5 0.0 collective-permute-done.low_ref
  48.6 1.9 %collective-permute-start.1 = (bf16[2,128,64]{2,1,0:T(8,128)(2,1)S(1)}, bf16[2,128,64]{2,1,0:T(8,128)(2,1)S(1)}, u32[]{:S(2)}, u32[]{:S(2)}) collective-permute-start(bf16[2,128,64]{2,1,0:T(8,128)(2,1)S(1)} %get-tuple-element.10), channel_id=1, source_target_pairs={{16,0},{32,16},{48,32},{64,48},{80,64},{96,80},{112,96},{128,112},... | collective-permute-start | bytes 98312 | tf_op jit(solution)/shard_map/ppermute | solution.py:335
  50.5 0.1 pad_maximum_fusion.kv_ref
  50.5 0.0 copy-done.6
  50.6 0.1 copy.17.q_ref
  51.3 3.2 %collective-permute-done.1.high_ref = bf16[2,128,64]{2,1,0:T(8,128)(2,1)S(1)} collective-permute-done((bf16[2,128,64]{2,1,0:T(8,128)(2,1)S(1)}, bf16[2,128,64]{2,1,0:T(8,128)(2,1)S(1)}, u32[]{:S(2)}, u32[]{:S(2)}) %collective-permute-start.1) | collective-permute-done | bytes 32800 | tf_op jit(solution)/shard_map/ppermute | solution.py:335
  54.5 1.3 attend.1
  55.8 0.0 all-to-all-done
  55.9 1.2 broadcast_in_dim.9
  57.1 3.7 %all-to-all-start.1 = ((bf16[4,320,512]{2,1,0:T(8,128)(2,1)}), bf16[4,320,512]{2,1,0:T(8,128)(2,1)S(1)}, u32[]{:S(2)}, u32[]{:S(2)}) async-start(bf16[4,320,512]{2,1,0:T(8,128)(2,1)} %broadcast_in_dim.9), calls=%async_computation.1 | async-start | bytes 2621440 | tf_op jit(solution)/shard_map/all_to_all | solution.py:384
  60.8 0.0 collective-permute-done.6.refs_3_
  60.8 0.0 collective-permute-done.7.refs_4_
  60.8 17.1 %all-to-all-done.1.x_ref = bf16[4,320,512]{2,1,0:T(8,128)(2,1)S(1)} async-done(((bf16[4,320,512]{2,1,0:T(8,128)(2,1)}), bf16[4,320,512]{2,1,0:T(8,128)(2,1)S(1)}, u32[]{:S(2)}, u32[]{:S(2)}) %all-to-all-start.1) | async-done | bytes 1310752 | tf_op jit(solution)/shard_map/all_to_all | solution.py:384
  77.9 0.0 collective-permute-done.10.refs_7_
  77.9 2.1 %collective-permute-done.9.refs_6_ = bf16[3072,256]{1,0:T(8,128)(2,1)} collective-permute-done((bf16[3072,256]{1,0:T(8,128)(2,1)}, bf16[3072,256]{1,0:T(8,128)(2,1)}, u32[]{:S(2)}, u32[]{:S(2)}) %collective-permute-start.9) | collective-permute-done | bytes 1572896 | tf_op jit(solution)/shard_map/ppermute | solution.py:58
  80.0 6.7 %ffn.1 = bf16[16,256,128]{2,1,0:T(8,128)(2,1)} custom-call(bf16[4,320,512]{2,1,0:T(8,128)(2,1)S(1)} %all-to-all-done.1.x_ref, bf16[3072,256]{1,0:T(8,128)(2,1)S(1)} %get-tuple-element.7.refs_0_, bf16[3072,256]{1,0:T(8,128)(2,1)} %get-tuple-element.8.refs_1_, bf16[3072,256]{1,0:T(8,128)(2,1)} %collective-permute-done.5.refs_2_, ...), custom_call_target="tpu_custom_call" | custom-call | tf_op jit(solution)/shard_map/ffn/pallas_call | solution.py:201
  86.7 19.4 %all_to_all.27.parts_ref = bf16[16,256,128]{2,1,0:T(8,128)(2,1)S(1)} all-to-all(bf16[16,256,128]{2,1,0:T(8,128)(2,1)} %ffn.1), channel_id=1, replica_groups={{0,1,2,3,4,5,6,7,8,9,10,11,12,13,14,15},{16,20,24,28,17,21,25,29,18,22,..., dimensions={0} | all-to-all | bytes 2097152 | tf_op jit(solution)/shard_map/all_to_all | solution.py:389
  106.1 0.8 total.1
  107.0 14.7 %all-to-all-start.3 = ((bf16[32,32,128]{2,1,0:T(8,128)(2,1)}), bf16[32,32,128]{2,1,0:T(8,128)(2,1)S(1)}, u32[]{:S(2)}, u32[]{:S(2)}) async-start(bf16[32,32,128]{2,1,0:T(8,128)(2,1)} %bitcast.6), calls=%async_computation.3 | async-start | bytes 524288 | tf_op jit(solution)/shard_map/all_to_all | solution.py:391
  121.7 1.9 %collective-permute-start.2 = (bf16[4,64,512]{2,1,0:T(8,128)(2,1)S(1)}, bf16[4,64,512]{2,1,0:T(8,128)(2,1)S(1)}, u32[]{:S(2)}, u32[]{:S(2)}) collective-permute-start(bf16[4,64,512]{2,1,0:T(8,128)(2,1)S(1)} %slice.16.own_ref), channel_id=1, source_target_pairs={{0,1},{1,0},{2,3},{3,2},{4,5},{5,4},{6,7},{7,6},{8,9},{9,8},{10,11... | collective-permute-start | bytes 786440 | tf_op jit(solution)/shard_map/ppermute | solution.py:58
  123.6 2.8 %collective-permute-start.3 = (bf16[4,64,512]{2,1,0:T(8,128)(2,1)S(1)}, bf16[4,64,512]{2,1,0:T(8,128)(2,1)S(1)}, u32[]{:S(2)}, u32[]{:S(2)}) collective-permute-start(bf16[4,64,512]{2,1,0:T(8,128)(2,1)S(1)} %slice.16.own_ref), channel_id=1, source_target_pairs={{0,3},{1,2},{2,1},{3,0},{4,7},{5,6},{6,5},{7,4},{8,11},{9,10},{10,... | collective-permute-start | bytes 786440 | tf_op jit(solution)/shard_map/ppermute | solution.py:58
  126.4 4.3 %collective-permute-start.4 = (bf16[4,64,512]{2,1,0:T(8,128)(2,1)S(1)}, bf16[4,64,512]{2,1,0:T(8,128)(2,1)S(1)}, u32[]{:S(2)}, u32[]{:S(2)}) collective-permute-start(bf16[4,64,512]{2,1,0:T(8,128)(2,1)S(1)} %slice.16.own_ref), channel_id=1, source_target_pairs={{0,2},{1,3},{2,0},{3,1},{4,6},{5,7},{6,4},{7,5},{8,10},{9,11},{10,... | collective-permute-start | bytes 786440 | tf_op jit(solution)/shard_map/ppermute | solution.py:58
  130.7 0.1 copy.18.weight_ref
  130.8 0.0 collective-permute-done.2.one_ref
  130.8 1.4 collective-permute-done.3.two_ref
  132.2 3.1 %collective-permute-done.4.far_ref = bf16[4,64,512]{2,1,0:T(8,128)(2,1)S(1)} collective-permute-done((bf16[4,64,512]{2,1,0:T(8,128)(2,1)S(1)}, bf16[4,64,512]{2,1,0:T(8,128)(2,1)S(1)}, u32[]{:S(2)}, u32[]{:S(2)}) %collective-permute-start.4) | collective-permute-done | bytes 262176 | tf_op jit(solution)/shard_map/ppermute | solution.py:58
  135.3 1.1 project.1
  136.4 7.4 %all-to-all-done.3 = bf16[32,32,128]{2,1,0:T(8,128)(2,1)S(1)} async-done(((bf16[32,32,128]{2,1,0:T(8,128)(2,1)}), bf16[32,32,128]{2,1,0:T(8,128)(2,1)S(1)}, u32[]{:S(2)}, u32[]{:S(2)}) %all-to-all-start.3) | async-done | bytes 262176 | tf_op jit(solution)/shard_map/all_to_all | solution.py:391
  143.9 1.1 combine.1
  (15 shorter events, 0.1 us)
Async XLA Ops:
  0.6 10.8 %copy-start.2 = (f32[2048]{0:T(1024)S(1)}, f32[2048]{0:T(1024)}, u32[]{:S(2)}) copy-start(f32[2048]{0:T(1024)} %param.18) | copy-start | bytes 24580
  0.6 10.8 %copy-start.3 = (s32[256,2]{0,1:T(2,128)S(1)}, s32[256,2]{0,1:T(2,128)}, u32[]{:S(2)}) copy-start(s32[256,2]{0,1:T(2,128)} %param.19) | copy-start | bytes 6148
  0.7 10.8 %copy-start = (bf16[256,2048]{1,0:T(8,128)(2,1)S(1)}, bf16[256,2048]{1,0:T(8,128)(2,1)}, u32[]{:S(2)}) copy-start(bf16[256,2048]{1,0:T(8,128)(2,1)} %x_ref.1) | copy-start | bytes 3145732
  3.9 33.3 %copy-start.4 = (bf16[512,256]{1,0:T(8,128)(2,1)S(1)}, bf16[512,256]{1,0:T(8,128)(2,1)}, u32[]{:S(2)}) copy-start(bf16[512,256]{1,0:T(8,128)(2,1)} %param.14) | copy-start | bytes 786436
  3.9 33.3 %copy-start.5 = (bf16[512,256]{1,0:T(8,128)(2,1)S(1)}, bf16[512,256]{1,0:T(8,128)(2,1)}, u32[]{:S(2)}) copy-start(bf16[512,256]{1,0:T(8,128)(2,1)} %param.13) | copy-start | bytes 786436
  3.9 36.6 %collective-permute-start.8 = (bf16[3072,256]{1,0:T(8,128)(2,1)}, bf16[3072,256]{1,0:T(8,128)(2,1)}, u32[]{:S(2)}, u32[]{:S(2)}) collective-permute-start(bf16[3072,256]{1,0:T(8,128)(2,1)} %get-tuple-element.8.refs_1_), channel_id=1, source_target_pairs={{0,3},{1,2},{2,1},{3,0},{4,7},{5,6},{6,5},{7,4},{8,11},{9,10},{10,... | collective-permute-start | bytes 4718600 | tf_op jit(solution)/shard_map/ppermute | solution.py:58
  9.5 34.4 %collective-permute-start.5 = (bf16[3072,256]{1,0:T(8,128)(2,1)S(1)}, bf16[3072,256]{1,0:T(8,128)(2,1)}, u32[]{:S(2)}, u32[]{:S(2)}) collective-permute-start(bf16[3072,256]{1,0:T(8,128)(2,1)S(1)} %get-tuple-element.7.refs_0_), channel_id=1, source_target_pairs={{0,1},{1,0},{2,3},{3,2},{4,5},{5,4},{6,7},{7,6},{8,9},{9,8},{10,11... | collective-permute-start | bytes 4718600 | tf_op jit(solution)/shard_map/ppermute | solution.py:58
  13.8 36.7 %copy-start.6 = (bf16[512,64]{0,1:T(8,128)(2,1)S(1)}, bf16[512,64]{0,1:T(8,128)(2,1)}, u32[]{:S(2)}) copy-start(bf16[512,64]{0,1:T(8,128)(2,1)} %param.12) | copy-start | bytes 196612
  13.8 42.0 %all-to-all-start = ((bf16[32,8,512]{2,1,0:T(8,128)(2,1)}), bf16[32,8,512]{2,1,0:T(8,128)(2,1)S(1)}, u32[]{:S(2)}, u32[]{:S(2)}) async-start(bf16[32,8,512]{2,1,0:T(8,128)(2,1)} %bitcast.2), calls=%async_computation | async-start | bytes 524288 | tf_op jit(solution)/shard_map/all_to_all | solution.py:377
  30.1 30.7 %collective-permute-start.6 = (bf16[3072,256]{1,0:T(8,128)(2,1)}, bf16[3072,256]{1,0:T(8,128)(2,1)}, u32[]{:S(2)}, u32[]{:S(2)}) collective-permute-start(bf16[3072,256]{1,0:T(8,128)(2,1)} %get-tuple-element.8.refs_1_), channel_id=1, source_target_pairs={{0,1},{1,0},{2,3},{3,2},{4,5},{5,4},{6,7},{7,6},{8,9},{9,8},{10,11... | collective-permute-start | bytes 4718600 | tf_op jit(solution)/shard_map/ppermute | solution.py:58
  33.4 27.5 %collective-permute-start.7 = (bf16[3072,256]{1,0:T(8,128)(2,1)S(1)}, bf16[3072,256]{1,0:T(8,128)(2,1)}, u32[]{:S(2)}, u32[]{:S(2)}) collective-permute-start(bf16[3072,256]{1,0:T(8,128)(2,1)S(1)} %get-tuple-element.7.refs_0_), channel_id=1, source_target_pairs={{0,3},{1,2},{2,1},{3,0},{4,7},{5,6},{6,5},{7,4},{8,11},{9,10},{10,... | collective-permute-start | bytes 4718600 | tf_op jit(solution)/shard_map/ppermute | solution.py:58
  37.4 11.2 %collective-permute-start = (bf16[2,128,64]{2,1,0:T(8,128)(2,1)S(1)}, bf16[2,128,64]{2,1,0:T(8,128)(2,1)S(1)}, u32[]{:S(2)}, u32[]{:S(2)}) collective-permute-start(bf16[2,128,64]{2,1,0:T(8,128)(2,1)S(1)} %get-tuple-element.11), channel_id=1, source_target_pairs={{0,16},{16,32},{32,48},{48,64},{64,80},{80,96},{96,112},{112,128},... | collective-permute-start | bytes 98312 | tf_op jit(solution)/shard_map/ppermute | solution.py:334
  40.5 37.4 %collective-permute-start.10 = (bf16[3072,256]{1,0:T(8,128)(2,1)}, bf16[3072,256]{1,0:T(8,128)(2,1)}, u32[]{:S(2)}, u32[]{:S(2)}) collective-permute-start(bf16[3072,256]{1,0:T(8,128)(2,1)} %collective-permute-done.8.refs_5_), channel_id=1, source_target_pairs={{0,1},{1,0},{2,3},{3,2},{4,5},{5,4},{6,7},{7,6},{8,9},{9,8},{10,11... | collective-permute-start | bytes 4718600 | tf_op jit(solution)/shard_map/ppermute | solution.py:58
  43.9 36.1 %collective-permute-start.9 = (bf16[3072,256]{1,0:T(8,128)(2,1)}, bf16[3072,256]{1,0:T(8,128)(2,1)}, u32[]{:S(2)}, u32[]{:S(2)}) collective-permute-start(bf16[3072,256]{1,0:T(8,128)(2,1)} %collective-permute-done.5.refs_2_), channel_id=1, source_target_pairs={{0,3},{1,2},{2,1},{3,0},{4,7},{5,6},{6,5},{7,4},{8,11},{9,10},{10,... | collective-permute-start | bytes 4718600 | tf_op jit(solution)/shard_map/ppermute | solution.py:58
  48.6 6.0 %collective-permute-start.1 = (bf16[2,128,64]{2,1,0:T(8,128)(2,1)S(1)}, bf16[2,128,64]{2,1,0:T(8,128)(2,1)S(1)}, u32[]{:S(2)}, u32[]{:S(2)}) collective-permute-start(bf16[2,128,64]{2,1,0:T(8,128)(2,1)S(1)} %get-tuple-element.10), channel_id=1, source_target_pairs={{16,0},{32,16},{48,32},{64,48},{80,64},{96,80},{112,96},{128,112},... | collective-permute-start | bytes 98312 | tf_op jit(solution)/shard_map/ppermute | solution.py:335
  57.1 20.9 %all-to-all-start.1 = ((bf16[4,320,512]{2,1,0:T(8,128)(2,1)}), bf16[4,320,512]{2,1,0:T(8,128)(2,1)S(1)}, u32[]{:S(2)}, u32[]{:S(2)}) async-start(bf16[4,320,512]{2,1,0:T(8,128)(2,1)} %broadcast_in_dim.9), calls=%async_computation.1 | async-start | bytes 2621440 | tf_op jit(solution)/shard_map/all_to_all | solution.py:384
  106.1 24.5 %copy-start.7 = (f32[256,2]{0,1:T(2,128)S(1)}, f32[256,2]{0,1:T(2,128)}, u32[]{:S(2)}) copy-start(f32[256,2]{0,1:T(2,128)} %param.20) | copy-start | bytes 6148
  106.1 29.2 %copy-start.1 = (bf16[1024,128]{1,0:T(8,128)(2,1)S(1)}, bf16[1024,128]{1,0:T(8,128)(2,1)}, u32[]{:S(2)}) copy-start(bf16[1024,128]{1,0:T(8,128)(2,1)} %weight_ref.2) | copy-start | bytes 786436
  107.0 36.9 %all-to-all-start.3 = ((bf16[32,32,128]{2,1,0:T(8,128)(2,1)}), bf16[32,32,128]{2,1,0:T(8,128)(2,1)S(1)}, u32[]{:S(2)}, u32[]{:S(2)}) async-start(bf16[32,32,128]{2,1,0:T(8,128)(2,1)} %bitcast.6), calls=%async_computation.3 | async-start | bytes 524288 | tf_op jit(solution)/shard_map/all_to_all | solution.py:391
  121.7 9.2 %collective-permute-start.2 = (bf16[4,64,512]{2,1,0:T(8,128)(2,1)S(1)}, bf16[4,64,512]{2,1,0:T(8,128)(2,1)S(1)}, u32[]{:S(2)}, u32[]{:S(2)}) collective-permute-start(bf16[4,64,512]{2,1,0:T(8,128)(2,1)S(1)} %slice.16.own_ref), channel_id=1, source_target_pairs={{0,1},{1,0},{2,3},{3,2},{4,5},{5,4},{6,7},{7,6},{8,9},{9,8},{10,11... | collective-permute-start | bytes 786440 | tf_op jit(solution)/shard_map/ppermute | solution.py:58
  123.6 8.6 %collective-permute-start.3 = (bf16[4,64,512]{2,1,0:T(8,128)(2,1)S(1)}, bf16[4,64,512]{2,1,0:T(8,128)(2,1)S(1)}, u32[]{:S(2)}, u32[]{:S(2)}) collective-permute-start(bf16[4,64,512]{2,1,0:T(8,128)(2,1)S(1)} %slice.16.own_ref), channel_id=1, source_target_pairs={{0,3},{1,2},{2,1},{3,0},{4,7},{5,6},{6,5},{7,4},{8,11},{9,10},{10,... | collective-permute-start | bytes 786440 | tf_op jit(solution)/shard_map/ppermute | solution.py:58
  126.4 8.9 %collective-permute-start.4 = (bf16[4,64,512]{2,1,0:T(8,128)(2,1)S(1)}, bf16[4,64,512]{2,1,0:T(8,128)(2,1)S(1)}, u32[]{:S(2)}, u32[]{:S(2)}) collective-permute-start(bf16[4,64,512]{2,1,0:T(8,128)(2,1)S(1)} %slice.16.own_ref), channel_id=1, source_target_pairs={{0,2},{1,3},{2,0},{3,1},{4,6},{5,7},{6,4},{7,5},{8,10},{9,11},{10,... | collective-permute-start | bytes 786440 | tf_op jit(solution)/shard_map/ppermute | solution.py:58

commit v9 on v8

--- a/solution.py
+++ b/solution.py
@@ -58,30 +58,48 @@
     return lax.ppermute(x, PLANE, pairs)
 
 
-def pack_kernel(gate_ref, up_ref, down_ref, wa_ref, wb_ref, sems):
-    copies = [
-        (gate_ref.at[0], wa_ref.at[pl.ds(0, 2048)]),
-        (up_ref.at[0, pl.ds(0, 1024)], wa_ref.at[pl.ds(2048, 1024)]),
-        (up_ref.at[0, pl.ds(1024, 1024)], wb_ref.at[pl.ds(0, 1024)]),
-    ] + [
-        (down_ref.at[0, :, pl.ds(c * 256, 256)], wb_ref.at[pl.ds(1024 + c * 256, 256)])
-        for c in range(8)
+def pack_kernel(gate_ref, up_ref, down_ref, wa_ref, wb_ref, stage_ref, sems, out_sems):
+    second = [(up_ref.at[0, pl.ds(1024, 1024)], 0, 1024)] + [
+        (down_ref.at[0, :, pl.ds(c * 256, 256)], 1024 + c * 256, 256) for c in range(8)
     ]
-    copies = [pltpu.make_async_copy(s, d, sems.at[i]) for i, (s, d) in enumerate(copies)]
-    for copy in copies:
+    come = [
+        pltpu.make_async_copy(source, stage_ref.at[pl.ds(at, count)], sems.at[i])
+        for i, (source, at, count) in enumerate(second)
+    ]
+    leave = [
+        pltpu.make_async_copy(
+            stage_ref.at[pl.ds(at, count)], wb_ref.at[pl.ds(at, count)], out_sems.at[i]
+        )
+        for i, (_, at, count) in enumerate(second)
+    ]
+    first = [
+        pltpu.make_async_copy(gate_ref.at[0], wa_ref.at[pl.ds(0, 2048)], sems.at[9]),
+        pltpu.make_async_copy(
+            up_ref.at[0, pl.ds(0, 1024)], wa_ref.at[pl.ds(2048, 1024)], sems.at[10]
+        ),
+    ]
+    for copy in come + first:
         copy.start()
-    for copy in copies:
+    for arrival, departure in zip(come, leave):
+        arrival.wait()
+        departure.start()
+    for copy in first + leave:
         copy.wait()
 
 
 def pack(gate, up, down):
-    half = pltpu.VMEM((HALF_W, 256), jnp.bfloat16)
     return pl.pallas_call(
         pack_kernel,
-        out_shape=(half, half),
+        out_shape=(
+            pltpu.VMEM((HALF_W, 256), jnp.bfloat16), pltpu.HBM((HALF_W, 256), jnp.bfloat16)
+        ),
         in_specs=[IN_HBM] * 3,
-        out_specs=(VMEM, VMEM),
-        scratch_shapes=[pltpu.SemaphoreType.DMA((11,))],
+        out_specs=(VMEM, IN_HBM),
+        scratch_shapes=[
+            pltpu.VMEM((HALF_W, 256), jnp.bfloat16),
+            pltpu.SemaphoreType.DMA((11,)),
+            pltpu.SemaphoreType.DMA((9,)),
+        ],
         compiler_params=vmem_mib(8),
         name="pack",
     )(*(in_hbm(a) for a in (gate, up, down)))
@@ -392,9 +410,10 @@
     expert_out = combine(returned.reshape(EXPERTS * CAP, 128), slots, route_weights)
 
     heads = rows[:, 256:]
-    near = [swap(heads, partner) for partner in (NEAR_A, NEAR_B)]
+    one = swap(heads, NEAR_A)
     far = swap(heads, ACROSS)
-    mixer_out = project(heads, *near, far, out_weight)
+    two = swap(heads, NEAR_B)
+    mixer_out = project(heads, one, two, far, out_weight)
     return (mixer_out, expert_out)
 
 

time: 146 us -> 145 us (level)
  no operation moved by 1% of the time
where the time goes in v9:
time: 145 us; the launch traced here: 144 us
  starting transfers between devices  69.8 us (48%)
  waiting for transfers between devices  34.3 us (24%)
  blocking collectives  19.4 us (13%)
  Pallas kernels  16 us (11%)
  between operations  1.64 us (1%)
  local copies, waits for them, and re-layouts  1.63 us (1%)
  other arithmetic  1.57 us (1%)
    ppermute x9, starting transfers between devices, swap(): return lax.ppermute(x, PLANE, pairs)  30 us
    all_to_all x1, blocking collectives, local(): lax.all_to_all(partial, PLANE, 0, 0, tiled=True, axis_index_groups=WHOLE)  19.4 us
    all_to_all x1, waiting for transfers between devices, local(): lax.all_to_all(jnp.broadcast_to(payload[None], (4, *payload.shape)), PLAN...  17.1 us
    all_to_all x1, starting transfers between devices, local(): arrived = lax.all_to_all(outgoing, EP, 0, 0, tiled=True)  16.3 us
    all_to_all x1, starting transfers between devices, local(): returned = lax.all_to_all(result, EP, 0, 0, tiled=True)  14.7 us
    all_to_all x1, waiting for transfers between devices, local(): returned = lax.all_to_all(result, EP, 0, 0, tiled=True)  7.44 us
    pallas_call x1, Pallas kernels, ffn(): pl.pallas_call(ffn_kernel, out_shape=pltpu.HBM((16, ROWS_B, 128), jnp.bfl...  6.69 us
    ppermute x9, waiting for transfers between devices, swap(): return lax.ppermute(x, PLANE, pairs)  6.59 us
  transfers between devices with their start and end apart: 14, of which 6 were waited for; matrix products, arithmetic and copies ran while one was open for 2% of the time, Pallas kernels for 3%

profile of v9, /device:TPU:1, one launch (start us, length us, event | category | flops | bytes accessed | tf_op | source)
XLA Modules:
  0.0 144.3 jit_solution(949331272344459176)
XLA Ops:
  0.7 2.5 %pack.1 = (bf16[3072,256]{1,0:T(8,128)(2,1)S(1)}, bf16[3072,256]{1,0:T(8,128)(2,1)}) custom-call(bf16[1,2048,256]{2,1,0:T(8,128)(2,1)} %gate_ref.1, bf16[1,2048,256]{2,1,0:T(8,128)(2,1)} %up_ref.1, bf16[1,256,2048]{2,1,0:T(8,128)(2,1)} %down_ref.1), custom_call_target="tpu_custom_call" | custom-call | tf_op jit(solution)/shard_map/pack/pallas_call | solution.py:91
  3.2 0.0 copy-start.4
  3.2 0.0 copy-start.5
  3.2 5.6 %collective-permute-start.8 = (bf16[3072,256]{1,0:T(8,128)(2,1)}, bf16[3072,256]{1,0:T(8,128)(2,1)}, u32[]{:S(2)}, u32[]{:S(2)}) collective-permute-start(bf16[3072,256]{1,0:T(8,128)(2,1)} %get-tuple-element.8.refs_1_), channel_id=1, source_target_pairs={{0,3},{1,2},{2,1},{3,0},{4,7},{5,6},{6,5},{7,4},{8,11},{9,10},{10,... | collective-permute-start | bytes 4718600 | tf_op jit(solution)/shard_map/ppermute | solution.py:58
  8.8 1.9 %collective-permute-start.5 = (bf16[3072,256]{1,0:T(8,128)(2,1)S(1)}, bf16[3072,256]{1,0:T(8,128)(2,1)}, u32[]{:S(2)}, u32[]{:S(2)}) collective-permute-start(bf16[3072,256]{1,0:T(8,128)(2,1)S(1)} %get-tuple-element.7.refs_0_), channel_id=1, source_target_pairs={{0,1},{1,0},{2,3},{3,2},{4,5},{5,4},{6,7},{7,6},{8,9},{9,8},{10,11... | collective-permute-start | bytes 4718600 | tf_op jit(solution)/shard_map/ppermute | solution.py:58
  10.7 0.0 copy-done.2
  10.7 0.0 copy-done.3
  10.8 0.0 copy-done
  10.8 2.4 %prep.1 = (bf16[256,512]{1,0:T(8,128)(2,1)}, s32[256,128]{1,0:T(8,128)S(1)}) custom-call(bf16[256,2048]{1,0:T(8,128)(2,1)S(1)} %copy-done, f32[1,2048]{1,0:T(1,128)S(1)} %bitcast.11, s32[2,256]{1,0:T(2,128)S(1)} %bitcast.12), custom_call_target="tpu_custom_call" | custom-call | tf_op jit(solution)/shard_map/prep/pallas_call | solution.py:159
  13.1 16.3 %all-to-all-start = ((bf16[32,8,512]{2,1,0:T(8,128)(2,1)}), bf16[32,8,512]{2,1,0:T(8,128)(2,1)S(1)}, u32[]{:S(2)}, u32[]{:S(2)}) async-start(bf16[32,8,512]{2,1,0:T(8,128)(2,1)} %bitcast.2), calls=%async_computation | async-start | bytes 524288 | tf_op jit(solution)/shard_map/all_to_all | solution.py:395
  29.4 3.2 %collective-permute-start.6 = (bf16[3072,256]{1,0:T(8,128)(2,1)}, bf16[3072,256]{1,0:T(8,128)(2,1)}, u32[]{:S(2)}, u32[]{:S(2)}) collective-permute-start(bf16[3072,256]{1,0:T(8,128)(2,1)} %get-tuple-element.8.refs_1_), channel_id=1, source_target_pairs={{0,1},{1,0},{2,3},{3,2},{4,5},{5,4},{6,7},{7,6},{8,9},{9,8},{10,11... | collective-permute-start | bytes 4718600 | tf_op jit(solution)/shard_map/ppermute | solution.py:58
  32.7 3.8 %collective-permute-start.7 = (bf16[3072,256]{1,0:T(8,128)(2,1)S(1)}, bf16[3072,256]{1,0:T(8,128)(2,1)}, u32[]{:S(2)}, u32[]{:S(2)}) collective-permute-start(bf16[3072,256]{1,0:T(8,128)(2,1)S(1)} %get-tuple-element.7.refs_0_), channel_id=1, source_target_pairs={{0,3},{1,2},{2,1},{3,0},{4,7},{5,6},{6,5},{7,4},{8,11},{9,10},{10,... | collective-permute-start | bytes 4718600 | tf_op jit(solution)/shard_map/ppermute | solution.py:58
  36.5 0.0 copy-done.4
  36.5 0.1 dynamic-slice_bitcast_fusion
  36.7 3.1 %collective-permute-start = (bf16[2,128,64]{2,1,0:T(8,128)(2,1)S(1)}, bf16[2,128,64]{2,1,0:T(8,128)(2,1)S(1)}, u32[]{:S(2)}, u32[]{:S(2)}) collective-permute-start(bf16[2,128,64]{2,1,0:T(8,128)(2,1)S(1)} %get-tuple-element.11), channel_id=1, source_target_pairs={{0,16},{16,32},{32,48},{48,64},{64,80},{80,96},{96,112},{112,128},... | collective-permute-start | bytes 98312 | tf_op jit(solution)/shard_map/ppermute | solution.py:352
  39.8 0.0 collective-permute-done.8.refs_5_
  39.8 3.4 %collective-permute-start.10 = (bf16[3072,256]{1,0:T(8,128)(2,1)}, bf16[3072,256]{1,0:T(8,128)(2,1)}, u32[]{:S(2)}, u32[]{:S(2)}) collective-permute-start(bf16[3072,256]{1,0:T(8,128)(2,1)} %collective-permute-done.8.refs_5_), channel_id=1, source_target_pairs={{0,1},{1,0},{2,3},{3,2},{4,5},{5,4},{6,7},{7,6},{8,9},{9,8},{10,11... | collective-permute-start | bytes 4718600 | tf_op jit(solution)/shard_map/ppermute | solution.py:58
  43.2 0.0 collective-permute-done.5.refs_2_
  43.2 3.1 %collective-permute-start.9 = (bf16[3072,256]{1,0:T(8,128)(2,1)}, bf16[3072,256]{1,0:T(8,128)(2,1)}, u32[]{:S(2)}, u32[]{:S(2)}) collective-permute-start(bf16[3072,256]{1,0:T(8,128)(2,1)} %collective-permute-done.5.refs_2_), channel_id=1, source_target_pairs={{0,3},{1,2},{2,1},{3,0},{4,7},{5,6},{6,5},{7,4},{8,11},{9,10},{10,... | collective-permute-start | bytes 4718600 | tf_op jit(solution)/shard_map/ppermute | solution.py:58
  46.4 1.4 %fusion = (f32[768,64]{1,0:T(8,128)S(1)}, f32[768,64]{1,0:T(8,128)S(1)}) fusion(f32[768]{0:T(1024)S(1)} %add_convert_fusion, f32[64]{0:T(128)S(1)} %get-tuple-element.16, f32[64]{0:T(128)S(1)} %get-tuple-element.17), kind=kLoop, calls=%fused_computation.2 | loop fusion | flops 98304 | bytes 396800 | tf_op jit(solution)/shard_map/mul | solution.py:361
  47.8 0.0 collective-permute-done.low_ref
  47.8 1.9 %collective-permute-start.1 = (bf16[2,128,64]{2,1,0:T(8,128)(2,1)S(1)}, bf16[2,128,64]{2,1,0:T(8,128)(2,1)S(1)}, u32[]{:S(2)}, u32[]{:S(2)}) collective-permute-start(bf16[2,128,64]{2,1,0:T(8,128)(2,1)S(1)} %get-tuple-element.10), channel_id=1, source_target_pairs={{16,0},{32,16},{48,32},{64,48},{80,64},{96,80},{112,96},{128,112},... | collective-permute-start | bytes 98312 | tf_op jit(solution)/shard_map/ppermute | solution.py:353
  49.8 0.1 pad_maximum_fusion.kv_ref
  49.9 0.1 copy.17.q_ref
  50.6 3.2 %collective-permute-done.1.high_ref = bf16[2,128,64]{2,1,0:T(8,128)(2,1)S(1)} collective-permute-done((bf16[2,128,64]{2,1,0:T(8,128)(2,1)S(1)}, bf16[2,128,64]{2,1,0:T(8,128)(2,1)S(1)}, u32[]{:S(2)}, u32[]{:S(2)}) %collective-permute-start.1) | collective-permute-done | bytes 32800 | tf_op jit(solution)/shard_map/ppermute | solution.py:353
  53.8 1.3 attend.1
  55.1 0.0 all-to-all-done
  55.2 1.2 broadcast_in_dim.9
  56.4 3.7 %all-to-all-start.1 = ((bf16[4,320,512]{2,1,0:T(8,128)(2,1)}), bf16[4,320,512]{2,1,0:T(8,128)(2,1)S(1)}, u32[]{:S(2)}, u32[]{:S(2)}) async-start(bf16[4,320,512]{2,1,0:T(8,128)(2,1)} %broadcast_in_dim.9), calls=%async_computation.1 | async-start | bytes 2621440 | tf_op jit(solution)/shard_map/all_to_all | solution.py:402
  60.1 0.0 collective-permute-done.6.refs_3_
  60.1 0.0 collective-permute-done.7.refs_4_
  60.1 17.1 %all-to-all-done.1.x_ref = bf16[4,320,512]{2,1,0:T(8,128)(2,1)S(1)} async-done(((bf16[4,320,512]{2,1,0:T(8,128)(2,1)}), bf16[4,320,512]{2,1,0:T(8,128)(2,1)S(1)}, u32[]{:S(2)}, u32[]{:S(2)}) %all-to-all-start.1) | async-done | bytes 1310752 | tf_op jit(solution)/shard_map/all_to_all | solution.py:402
  77.2 0.0 collective-permute-done.10.refs_7_
  77.2 2.1 %collective-permute-done.9.refs_6_ = bf16[3072,256]{1,0:T(8,128)(2,1)} collective-permute-done((bf16[3072,256]{1,0:T(8,128)(2,1)}, bf16[3072,256]{1,0:T(8,128)(2,1)}, u32[]{:S(2)}, u32[]{:S(2)}) %collective-permute-start.9) | collective-permute-done | bytes 1572896 | tf_op jit(solution)/shard_map/ppermute | solution.py:58
  79.3 6.7 %ffn.1 = bf16[16,256,128]{2,1,0:T(8,128)(2,1)} custom-call(bf16[4,320,512]{2,1,0:T(8,128)(2,1)S(1)} %all-to-all-done.1.x_ref, bf16[3072,256]{1,0:T(8,128)(2,1)S(1)} %get-tuple-element.7.refs_0_, bf16[3072,256]{1,0:T(8,128)(2,1)} %get-tuple-element.8.refs_1_, bf16[3072,256]{1,0:T(8,128)(2,1)} %collective-permute-done.5.refs_2_, ...), custom_call_target="tpu_custom_call" | custom-call | tf_op jit(solution)/shard_map/ffn/pallas_call | solution.py:219
  86.0 19.4 %all_to_all.27.parts_ref = bf16[16,256,128]{2,1,0:T(8,128)(2,1)S(1)} all-to-all(bf16[16,256,128]{2,1,0:T(8,128)(2,1)} %ffn.1), channel_id=1, replica_groups={{0,1,2,3,4,5,6,7,8,9,10,11,12,13,14,15},{16,20,24,28,17,21,25,29,18,22,..., dimensions={0} | all-to-all | bytes 2097152 | tf_op jit(solution)/shard_map/all_to_all | solution.py:407
  105.4 0.8 total.1
  106.3 14.7 %all-to-all-start.3 = ((bf16[32,32,128]{2,1,0:T(8,128)(2,1)}), bf16[32,32,128]{2,1,0:T(8,128)(2,1)S(1)}, u32[]{:S(2)}, u32[]{:S(2)}) async-start(bf16[32,32,128]{2,1,0:T(8,128)(2,1)} %bitcast.6), calls=%async_computation.3 | async-start | bytes 524288 | tf_op jit(solution)/shard_map/all_to_all | solution.py:409
  121.0 1.9 %collective-permute-start.2 = (bf16[4,64,512]{2,1,0:T(8,128)(2,1)S(1)}, bf16[4,64,512]{2,1,0:T(8,128)(2,1)S(1)}, u32[]{:S(2)}, u32[]{:S(2)}) collective-permute-start(bf16[4,64,512]{2,1,0:T(8,128)(2,1)S(1)} %slice.16.own_ref), channel_id=1, source_target_pairs={{0,1},{1,0},{2,3},{3,2},{4,5},{5,4},{6,7},{7,6},{8,9},{9,8},{10,11... | collective-permute-start | bytes 786440 | tf_op jit(solution)/shard_map/ppermute | solution.py:58
  122.9 2.8 %collective-permute-start.3 = (bf16[4,64,512]{2,1,0:T(8,128)(2,1)S(1)}, bf16[4,64,512]{2,1,0:T(8,128)(2,1)S(1)}, u32[]{:S(2)}, u32[]{:S(2)}) collective-permute-start(bf16[4,64,512]{2,1,0:T(8,128)(2,1)S(1)} %slice.16.own_ref), channel_id=1, source_target_pairs={{0,3},{1,2},{2,1},{3,0},{4,7},{5,6},{6,5},{7,4},{8,11},{9,10},{10,... | collective-permute-start | bytes 786440 | tf_op jit(solution)/shard_map/ppermute | solution.py:58
  125.7 4.3 %collective-permute-start.4 = (bf16[4,64,512]{2,1,0:T(8,128)(2,1)S(1)}, bf16[4,64,512]{2,1,0:T(8,128)(2,1)S(1)}, u32[]{:S(2)}, u32[]{:S(2)}) collective-permute-start(bf16[4,64,512]{2,1,0:T(8,128)(2,1)S(1)} %slice.16.own_ref), channel_id=1, source_target_pairs={{0,2},{1,3},{2,0},{3,1},{4,6},{5,7},{6,4},{7,5},{8,10},{9,11},{10,... | collective-permute-start | bytes 786440 | tf_op jit(solution)/shard_map/ppermute | solution.py:58
  130.0 0.1 copy.18.weight_ref
  130.1 0.0 collective-permute-done.2.one_ref
  130.1 1.4 collective-permute-done.3.two_ref
  131.5 3.1 %collective-permute-done.4.far_ref = bf16[4,64,512]{2,1,0:T(8,128)(2,1)S(1)} collective-permute-done((bf16[4,64,512]{2,1,0:T(8,128)(2,1)S(1)}, bf16[4,64,512]{2,1,0:T(8,128)(2,1)S(1)}, u32[]{:S(2)}, u32[]{:S(2)}) %collective-permute-start.4) | collective-permute-done | bytes 262176 | tf_op jit(solution)/shard_map/ppermute | solution.py:58
  134.6 1.1 project.1
  135.7 7.4 %all-to-all-done.3 = bf16[32,32,128]{2,1,0:T(8,128)(2,1)S(1)} async-done(((bf16[32,32,128]{2,1,0:T(8,128)(2,1)}), bf16[32,32,128]{2,1,0:T(8,128)(2,1)S(1)}, u32[]{:S(2)}, u32[]{:S(2)}) %all-to-all-start.3) | async-done | bytes 262176 | tf_op jit(solution)/shard_map/all_to_all | solution.py:409
  143.2 1.1 combine.1
  (15 shorter events, 0.1 us)
Async XLA Ops:
  0.6 10.1 %copy-start.2 = (f32[2048]{0:T(1024)S(1)}, f32[2048]{0:T(1024)}, u32[]{:S(2)}) copy-start(f32[2048]{0:T(1024)} %param.18) | copy-start | bytes 24580
  0.6 10.1 %copy-start.3 = (s32[256,2]{0,1:T(2,128)S(1)}, s32[256,2]{0,1:T(2,128)}, u32[]{:S(2)}) copy-start(s32[256,2]{0,1:T(2,128)} %param.19) | copy-start | bytes 6148
  0.7 10.1 %copy-start = (bf16[256,2048]{1,0:T(8,128)(2,1)S(1)}, bf16[256,2048]{1,0:T(8,128)(2,1)}, u32[]{:S(2)}) copy-start(bf16[256,2048]{1,0:T(8,128)(2,1)} %x_ref.1) | copy-start | bytes 3145732
  3.2 33.3 %copy-start.4 = (bf16[512,256]{1,0:T(8,128)(2,1)S(1)}, bf16[512,256]{1,0:T(8,128)(2,1)}, u32[]{:S(2)}) copy-start(bf16[512,256]{1,0:T(8,128)(2,1)} %param.14) | copy-start | bytes 786436
  3.2 33.3 %copy-start.5 = (bf16[512,256]{1,0:T(8,128)(2,1)S(1)}, bf16[512,256]{1,0:T(8,128)(2,1)}, u32[]{:S(2)}) copy-start(bf16[512,256]{1,0:T(8,128)(2,1)} %param.13) | copy-start | bytes 786436
  3.2 36.6 %collective-permute-start.8 = (bf16[3072,256]{1,0:T(8,128)(2,1)}, bf16[3072,256]{1,0:T(8,128)(2,1)}, u32[]{:S(2)}, u32[]{:S(2)}) collective-permute-start(bf16[3072,256]{1,0:T(8,128)(2,1)} %get-tuple-element.8.refs_1_), channel_id=1, source_target_pairs={{0,3},{1,2},{2,1},{3,0},{4,7},{5,6},{6,5},{7,4},{8,11},{9,10},{10,... | collective-permute-start | bytes 4718600 | tf_op jit(solution)/shard_map/ppermute | solution.py:58
  8.8 34.4 %collective-permute-start.5 = (bf16[3072,256]{1,0:T(8,128)(2,1)S(1)}, bf16[3072,256]{1,0:T(8,128)(2,1)}, u32[]{:S(2)}, u32[]{:S(2)}) collective-permute-start(bf16[3072,256]{1,0:T(8,128)(2,1)S(1)} %get-tuple-element.7.refs_0_), channel_id=1, source_target_pairs={{0,1},{1,0},{2,3},{3,2},{4,5},{5,4},{6,7},{7,6},{8,9},{9,8},{10,11... | collective-permute-start | bytes 4718600 | tf_op jit(solution)/shard_map/ppermute | solution.py:58
  13.1 36.7 %copy-start.6 = (bf16[512,64]{0,1:T(8,128)(2,1)S(1)}, bf16[512,64]{0,1:T(8,128)(2,1)}, u32[]{:S(2)}) copy-start(bf16[512,64]{0,1:T(8,128)(2,1)} %param.12) | copy-start | bytes 196612
  13.1 42.0 %all-to-all-start = ((bf16[32,8,512]{2,1,0:T(8,128)(2,1)}), bf16[32,8,512]{2,1,0:T(8,128)(2,1)S(1)}, u32[]{:S(2)}, u32[]{:S(2)}) async-start(bf16[32,8,512]{2,1,0:T(8,128)(2,1)} %bitcast.2), calls=%async_computation | async-start | bytes 524288 | tf_op jit(solution)/shard_map/all_to_all | solution.py:395
  29.4 30.7 %collective-permute-start.6 = (bf16[3072,256]{1,0:T(8,128)(2,1)}, bf16[3072,256]{1,0:T(8,128)(2,1)}, u32[]{:S(2)}, u32[]{:S(2)}) collective-permute-start(bf16[3072,256]{1,0:T(8,128)(2,1)} %get-tuple-element.8.refs_1_), channel_id=1, source_target_pairs={{0,1},{1,0},{2,3},{3,2},{4,5},{5,4},{6,7},{7,6},{8,9},{9,8},{10,11... | collective-permute-start | bytes 4718600 | tf_op jit(solution)/shard_map/ppermute | solution.py:58
  32.7 27.5 %collective-permute-start.7 = (bf16[3072,256]{1,0:T(8,128)(2,1)S(1)}, bf16[3072,256]{1,0:T(8,128)(2,1)}, u32[]{:S(2)}, u32[]{:S(2)}) collective-permute-start(bf16[3072,256]{1,0:T(8,128)(2,1)S(1)} %get-tuple-element.7.refs_0_), channel_id=1, source_target_pairs={{0,3},{1,2},{2,1},{3,0},{4,7},{5,6},{6,5},{7,4},{8,11},{9,10},{10,... | collective-permute-start | bytes 4718600 | tf_op jit(solution)/shard_map/ppermute | solution.py:58
  36.7 11.2 %collective-permute-start = (bf16[2,128,64]{2,1,0:T(8,128)(2,1)S(1)}, bf16[2,128,64]{2,1,0:T(8,128)(2,1)S(1)}, u32[]{:S(2)}, u32[]{:S(2)}) collective-permute-start(bf16[2,128,64]{2,1,0:T(8,128)(2,1)S(1)} %get-tuple-element.11), channel_id=1, source_target_pairs={{0,16},{16,32},{32,48},{48,64},{64,80},{80,96},{96,112},{112,128},... | collective-permute-start | bytes 98312 | tf_op jit(solution)/shard_map/ppermute | solution.py:352
  39.8 37.4 %collective-permute-start.10 = (bf16[3072,256]{1,0:T(8,128)(2,1)}, bf16[3072,256]{1,0:T(8,128)(2,1)}, u32[]{:S(2)}, u32[]{:S(2)}) collective-permute-start(bf16[3072,256]{1,0:T(8,128)(2,1)} %collective-permute-done.8.refs_5_), channel_id=1, source_target_pairs={{0,1},{1,0},{2,3},{3,2},{4,5},{5,4},{6,7},{7,6},{8,9},{9,8},{10,11... | collective-permute-start | bytes 4718600 | tf_op jit(solution)/shard_map/ppermute | solution.py:58
  43.2 36.1 %collective-permute-start.9 = (bf16[3072,256]{1,0:T(8,128)(2,1)}, bf16[3072,256]{1,0:T(8,128)(2,1)}, u32[]{:S(2)}, u32[]{:S(2)}) collective-permute-start(bf16[3072,256]{1,0:T(8,128)(2,1)} %collective-permute-done.5.refs_2_), channel_id=1, source_target_pairs={{0,3},{1,2},{2,1},{3,0},{4,7},{5,6},{6,5},{7,4},{8,11},{9,10},{10,... | collective-permute-start | bytes 4718600 | tf_op jit(solution)/shard_map/ppermute | solution.py:58
  47.8 6.0 %collective-permute-start.1 = (bf16[2,128,64]{2,1,0:T(8,128)(2,1)S(1)}, bf16[2,128,64]{2,1,0:T(8,128)(2,1)S(1)}, u32[]{:S(2)}, u32[]{:S(2)}) collective-permute-start(bf16[2,128,64]{2,1,0:T(8,128)(2,1)S(1)} %get-tuple-element.10), channel_id=1, source_target_pairs={{16,0},{32,16},{48,32},{64,48},{80,64},{96,80},{112,96},{128,112},... | collective-permute-start | bytes 98312 | tf_op jit(solution)/shard_map/ppermute | solution.py:353
  56.4 20.9 %all-to-all-start.1 = ((bf16[4,320,512]{2,1,0:T(8,128)(2,1)}), bf16[4,320,512]{2,1,0:T(8,128)(2,1)S(1)}, u32[]{:S(2)}, u32[]{:S(2)}) async-start(bf16[4,320,512]{2,1,0:T(8,128)(2,1)} %broadcast_in_dim.9), calls=%async_computation.1 | async-start | bytes 2621440 | tf_op jit(solution)/shard_map/all_to_all | solution.py:402
  105.4 24.5 %copy-start.7 = (f32[256,2]{0,1:T(2,128)S(1)}, f32[256,2]{0,1:T(2,128)}, u32[]{:S(2)}) copy-start(f32[256,2]{0,1:T(2,128)} %param.20) | copy-start | bytes 6148
  105.4 29.2 %copy-start.1 = (bf16[1024,128]{1,0:T(8,128)(2,1)S(1)}, bf16[1024,128]{1,0:T(8,128)(2,1)}, u32[]{:S(2)}) copy-start(bf16[1024,128]{1,0:T(8,128)(2,1)} %weight_ref.2) | copy-start | bytes 786436
  106.3 36.9 %all-to-all-start.3 = ((bf16[32,32,128]{2,1,0:T(8,128)(2,1)}), bf16[32,32,128]{2,1,0:T(8,128)(2,1)S(1)}, u32[]{:S(2)}, u32[]{:S(2)}) async-start(bf16[32,32,128]{2,1,0:T(8,128)(2,1)} %bitcast.6), calls=%async_computation.3 | async-start | bytes 524288 | tf_op jit(solution)/shard_map/all_to_all | solution.py:409
  121.0 9.2 %collective-permute-start.2 = (bf16[4,64,512]{2,1,0:T(8,128)(2,1)S(1)}, bf16[4,64,512]{2,1,0:T(8,128)(2,1)S(1)}, u32[]{:S(2)}, u32[]{:S(2)}) collective-permute-start(bf16[4,64,512]{2,1,0:T(8,128)(2,1)S(1)} %slice.16.own_ref), channel_id=1, source_target_pairs={{0,1},{1,0},{2,3},{3,2},{4,5},{5,4},{6,7},{7,6},{8,9},{9,8},{10,11... | collective-permute-start | bytes 786440 | tf_op jit(solution)/shard_map/ppermute | solution.py:58
  122.9 8.6 %collective-permute-start.3 = (bf16[4,64,512]{2,1,0:T(8,128)(2,1)S(1)}, bf16[4,64,512]{2,1,0:T(8,128)(2,1)S(1)}, u32[]{:S(2)}, u32[]{:S(2)}) collective-permute-start(bf16[4,64,512]{2,1,0:T(8,128)(2,1)S(1)} %slice.16.own_ref), channel_id=1, source_target_pairs={{0,3},{1,2},{2,1},{3,0},{4,7},{5,6},{6,5},{7,4},{8,11},{9,10},{10,... | collective-permute-start | bytes 786440 | tf_op jit(solution)/shard_map/ppermute | solution.py:58
  125.7 8.9 %collective-permute-start.4 = (bf16[4,64,512]{2,1,0:T(8,128)(2,1)S(1)}, bf16[4,64,512]{2,1,0:T(8,128)(2,1)S(1)}, u32[]{:S(2)}, u32[]{:S(2)}) collective-permute-start(bf16[4,64,512]{2,1,0:T(8,128)(2,1)S(1)} %slice.16.own_ref), channel_id=1, source_target_pairs={{0,2},{1,3},{2,0},{3,1},{4,6},{5,7},{6,4},{7,5},{8,10},{9,11},{10,... | collective-permute-start | bytes 786440 | tf_op jit(solution)/shard_map/ppermute | solution.py:58

commit v10 on v9

--- a/solution.py
+++ b/solution.py
@@ -219,7 +219,7 @@
     return pl.pallas_call(
         ffn_kernel,
         out_shape=pltpu.HBM((16, ROWS_B, 128), jnp.bfloat16),
-        in_specs=[VMEM] + [ANY] * 8,
+        in_specs=[VMEM, ANY] + [IN_HBM] * 7,
         out_specs=IN_HBM,
         scratch_shapes=[
             pltpu.VMEM((ROWS_B, D), jnp.float32),
@@ -230,7 +230,7 @@
         ],
         compiler_params=vmem_mib(24),
         name="ffn",
-    )(resident(x), *weights)
+    )(resident(x), weights[0], *(in_hbm(a) for a in weights[1:]))
 
 
 def total_kernel(parts_ref, out_ref):
@@ -389,8 +389,8 @@
     wa, wb = pack(gate_weight, up_weight, down_weight)
     one_a = swap(wa, NEAR_A)
     two_b = swap(wb, NEAR_B)
+    two_a = swap(wa, NEAR_B)
     one_b = swap(wb, NEAR_A)
-    two_a = swap(wa, NEAR_B)
     outgoing, slots = prepare(expert_input, norm_gain, routes)
     arrived = lax.all_to_all(outgoing, EP, 0, 0, tiled=True)
     far_a = swap(one_a, NEAR_B)
@@ -410,10 +410,9 @@
     expert_out = combine(returned.reshape(EXPERTS * CAP, 128), slots, route_weights)
 
     heads = rows[:, 256:]
-    one = swap(heads, NEAR_A)
+    near = [swap(heads, partner) for partner in (NEAR_A, NEAR_B)]
     far = swap(heads, ACROSS)
-    two = swap(heads, NEAR_B)
-    mixer_out = project(heads, one, two, far, out_weight)
+    mixer_out = project(heads, *near, far, out_weight)
     return (mixer_out, expert_out)
 
 

time: 145 us -> 145 us (level)
  no operation moved by 1% of the time
where the time goes in v10:
time: 145 us; the launch traced here: 144 us
  starting transfers between devices  69.8 us (48%)
  waiting for transfers between devices  34.3 us (24%)
  blocking collectives  19.4 us (13%)
  Pallas kernels  16 us (11%)
  between operations  1.64 us (1%)
  local copies, waits for them, and re-layouts  1.63 us (1%)
  other arithmetic  1.57 us (1%)
    ppermute x9, starting transfers between devices, swap(): return lax.ppermute(x, PLANE, pairs)  30 us
    all_to_all x1, blocking collectives, local(): lax.all_to_all(partial, PLANE, 0, 0, tiled=True, axis_index_groups=WHOLE)  19.4 us
    all_to_all x1, waiting for transfers between devices, local(): lax.all_to_all(jnp.broadcast_to(payload[None], (4, *payload.shape)), PLAN...  17.1 us
    all_to_all x1, starting transfers between devices, local(): arrived = lax.all_to_all(outgoing, EP, 0, 0, tiled=True)  16.3 us
    all_to_all x1, starting transfers between devices, local(): returned = lax.all_to_all(result, EP, 0, 0, tiled=True)  14.7 us
    all_to_all x1, waiting for transfers between devices, local(): returned = lax.all_to_all(result, EP, 0, 0, tiled=True)  7.44 us
    pallas_call x1, Pallas kernels, ffn(): pl.pallas_call(ffn_kernel, out_shape=pltpu.HBM((16, ROWS_B, 128), jnp.bfl...  6.69 us
    ppermute x9, waiting for transfers between devices, swap(): return lax.ppermute(x, PLANE, pairs)  6.59 us
  transfers between devices with their start and end apart: 14, of which 6 were waited for; matrix products, arithmetic and copies ran while one was open for 2% of the time, Pallas kernels for 3%

profile of v10, /device:TPU:1, one launch (start us, length us, event | category | flops | bytes accessed | tf_op | source)
XLA Modules:
  0.0 144.3 jit_solution(949331272344459176)
XLA Ops:
  0.7 2.5 %pack.1 = (bf16[3072,256]{1,0:T(8,128)(2,1)S(1)}, bf16[3072,256]{1,0:T(8,128)(2,1)}) custom-call(bf16[1,2048,256]{2,1,0:T(8,128)(2,1)} %gate_ref.1, bf16[1,2048,256]{2,1,0:T(8,128)(2,1)} %up_ref.1, bf16[1,256,2048]{2,1,0:T(8,128)(2,1)} %down_ref.1), custom_call_target="tpu_custom_call" | custom-call | tf_op jit(solution)/shard_map/pack/pallas_call | solution.py:91
  3.2 0.0 copy-start.4
  3.2 0.0 copy-start.5
  3.2 5.6 %collective-permute-start.8 = (bf16[3072,256]{1,0:T(8,128)(2,1)}, bf16[3072,256]{1,0:T(8,128)(2,1)}, u32[]{:S(2)}, u32[]{:S(2)}) collective-permute-start(bf16[3072,256]{1,0:T(8,128)(2,1)} %get-tuple-element.8.refs_1_), channel_id=1, source_target_pairs={{0,3},{1,2},{2,1},{3,0},{4,7},{5,6},{6,5},{7,4},{8,11},{9,10},{10,... | collective-permute-start | bytes 4718600 | tf_op jit(solution)/shard_map/ppermute | solution.py:58
  8.8 1.9 %collective-permute-start.5 = (bf16[3072,256]{1,0:T(8,128)(2,1)S(1)}, bf16[3072,256]{1,0:T(8,128)(2,1)}, u32[]{:S(2)}, u32[]{:S(2)}) collective-permute-start(bf16[3072,256]{1,0:T(8,128)(2,1)S(1)} %get-tuple-element.7.refs_0_), channel_id=1, source_target_pairs={{0,1},{1,0},{2,3},{3,2},{4,5},{5,4},{6,7},{7,6},{8,9},{9,8},{10,11... | collective-permute-start | bytes 4718600 | tf_op jit(solution)/shard_map/ppermute | solution.py:58
  10.7 0.0 copy-done.2
  10.7 0.0 copy-done.3
  10.8 0.0 copy-done
  10.8 2.4 %prep.1 = (bf16[256,512]{1,0:T(8,128)(2,1)}, s32[256,128]{1,0:T(8,128)S(1)}) custom-call(bf16[256,2048]{1,0:T(8,128)(2,1)S(1)} %copy-done, f32[1,2048]{1,0:T(1,128)S(1)} %bitcast.11, s32[2,256]{1,0:T(2,128)S(1)} %bitcast.12), custom_call_target="tpu_custom_call" | custom-call | tf_op jit(solution)/shard_map/prep/pallas_call | solution.py:159
  13.1 16.3 %all-to-all-start = ((bf16[32,8,512]{2,1,0:T(8,128)(2,1)}), bf16[32,8,512]{2,1,0:T(8,128)(2,1)S(1)}, u32[]{:S(2)}, u32[]{:S(2)}) async-start(bf16[32,8,512]{2,1,0:T(8,128)(2,1)} %bitcast.2), calls=%async_computation | async-start | bytes 524288 | tf_op jit(solution)/shard_map/all_to_all | solution.py:395
  29.4 3.2 %collective-permute-start.6 = (bf16[3072,256]{1,0:T(8,128)(2,1)}, bf16[3072,256]{1,0:T(8,128)(2,1)}, u32[]{:S(2)}, u32[]{:S(2)}) collective-permute-start(bf16[3072,256]{1,0:T(8,128)(2,1)} %get-tuple-element.8.refs_1_), channel_id=1, source_target_pairs={{0,1},{1,0},{2,3},{3,2},{4,5},{5,4},{6,7},{7,6},{8,9},{9,8},{10,11... | collective-permute-start | bytes 4718600 | tf_op jit(solution)/shard_map/ppermute | solution.py:58
  32.7 3.8 %collective-permute-start.7 = (bf16[3072,256]{1,0:T(8,128)(2,1)S(1)}, bf16[3072,256]{1,0:T(8,128)(2,1)}, u32[]{:S(2)}, u32[]{:S(2)}) collective-permute-start(bf16[3072,256]{1,0:T(8,128)(2,1)S(1)} %get-tuple-element.7.refs_0_), channel_id=1, source_target_pairs={{0,3},{1,2},{2,1},{3,0},{4,7},{5,6},{6,5},{7,4},{8,11},{9,10},{10,... | collective-permute-start | bytes 4718600 | tf_op jit(solution)/shard_map/ppermute | solution.py:58
  36.5 0.0 copy-done.4
  36.5 0.1 dynamic-slice_bitcast_fusion
  36.7 3.1 %collective-permute-start = (bf16[2,128,64]{2,1,0:T(8,128)(2,1)S(1)}, bf16[2,128,64]{2,1,0:T(8,128)(2,1)S(1)}, u32[]{:S(2)}, u32[]{:S(2)}) collective-permute-start(bf16[2,128,64]{2,1,0:T(8,128)(2,1)S(1)} %get-tuple-element.11), channel_id=1, source_target_pairs={{0,16},{16,32},{32,48},{48,64},{64,80},{80,96},{96,112},{112,128},... | collective-permute-start | bytes 98312 | tf_op jit(solution)/shard_map/ppermute | solution.py:352
  39.8 0.0 collective-permute-done.8.refs_5_
  39.8 3.4 %collective-permute-start.10 = (bf16[3072,256]{1,0:T(8,128)(2,1)}, bf16[3072,256]{1,0:T(8,128)(2,1)}, u32[]{:S(2)}, u32[]{:S(2)}) collective-permute-start(bf16[3072,256]{1,0:T(8,128)(2,1)} %collective-permute-done.8.refs_5_), channel_id=1, source_target_pairs={{0,1},{1,0},{2,3},{3,2},{4,5},{5,4},{6,7},{7,6},{8,9},{9,8},{10,11... | collective-permute-start | bytes 4718600 | tf_op jit(solution)/shard_map/ppermute | solution.py:58
  43.2 0.0 collective-permute-done.5.refs_2_
  43.2 3.1 %collective-permute-start.9 = (bf16[3072,256]{1,0:T(8,128)(2,1)}, bf16[3072,256]{1,0:T(8,128)(2,1)}, u32[]{:S(2)}, u32[]{:S(2)}) collective-permute-start(bf16[3072,256]{1,0:T(8,128)(2,1)} %collective-permute-done.5.refs_2_), channel_id=1, source_target_pairs={{0,3},{1,2},{2,1},{3,0},{4,7},{5,6},{6,5},{7,4},{8,11},{9,10},{10,... | collective-permute-start | bytes 4718600 | tf_op jit(solution)/shard_map/ppermute | solution.py:58
  46.4 1.4 %fusion = (f32[768,64]{1,0:T(8,128)S(1)}, f32[768,64]{1,0:T(8,128)S(1)}) fusion(f32[768]{0:T(1024)S(1)} %add_convert_fusion, f32[64]{0:T(128)S(1)} %get-tuple-element.16, f32[64]{0:T(128)S(1)} %get-tuple-element.17), kind=kLoop, calls=%fused_computation.2 | loop fusion | flops 98304 | bytes 396800 | tf_op jit(solution)/shard_map/mul | solution.py:361
  47.8 0.0 collective-permute-done.low_ref
  47.8 1.9 %collective-permute-start.1 = (bf16[2,128,64]{2,1,0:T(8,128)(2,1)S(1)}, bf16[2,128,64]{2,1,0:T(8,128)(2,1)S(1)}, u32[]{:S(2)}, u32[]{:S(2)}) collective-permute-start(bf16[2,128,64]{2,1,0:T(8,128)(2,1)S(1)} %get-tuple-element.10), channel_id=1, source_target_pairs={{16,0},{32,16},{48,32},{64,48},{80,64},{96,80},{112,96},{128,112},... | collective-permute-start | bytes 98312 | tf_op jit(solution)/shard_map/ppermute | solution.py:353
  49.8 0.1 pad_maximum_fusion.kv_ref
  49.9 0.1 copy.17.q_ref
  50.6 3.2 %collective-permute-done.1.high_ref = bf16[2,128,64]{2,1,0:T(8,128)(2,1)S(1)} collective-permute-done((bf16[2,128,64]{2,1,0:T(8,128)(2,1)S(1)}, bf16[2,128,64]{2,1,0:T(8,128)(2,1)S(1)}, u32[]{:S(2)}, u32[]{:S(2)}) %collective-permute-start.1) | collective-permute-done | bytes 32800 | tf_op jit(solution)/shard_map/ppermute | solution.py:353
  53.8 1.3 attend.1
  55.1 0.0 all-to-all-done
  55.2 1.2 broadcast_in_dim.9
  56.4 3.7 %all-to-all-start.1 = ((bf16[4,320,512]{2,1,0:T(8,128)(2,1)}), bf16[4,320,512]{2,1,0:T(8,128)(2,1)S(1)}, u32[]{:S(2)}, u32[]{:S(2)}) async-start(bf16[4,320,512]{2,1,0:T(8,128)(2,1)} %broadcast_in_dim.9), calls=%async_computation.1 | async-start | bytes 2621440 | tf_op jit(solution)/shard_map/all_to_all | solution.py:402
  60.1 0.0 collective-permute-done.6.refs_3_
  60.1 0.0 collective-permute-done.7.refs_4_
  60.1 17.1 %all-to-all-done.1.x_ref = bf16[4,320,512]{2,1,0:T(8,128)(2,1)S(1)} async-done(((bf16[4,320,512]{2,1,0:T(8,128)(2,1)}), bf16[4,320,512]{2,1,0:T(8,128)(2,1)S(1)}, u32[]{:S(2)}, u32[]{:S(2)}) %all-to-all-start.1) | async-done | bytes 1310752 | tf_op jit(solution)/shard_map/all_to_all | solution.py:402
  77.2 0.0 collective-permute-done.10.refs_7_
  77.2 2.1 %collective-permute-done.9.refs_6_ = bf16[3072,256]{1,0:T(8,128)(2,1)} collective-permute-done((bf16[3072,256]{1,0:T(8,128)(2,1)}, bf16[3072,256]{1,0:T(8,128)(2,1)}, u32[]{:S(2)}, u32[]{:S(2)}) %collective-permute-start.9) | collective-permute-done | bytes 1572896 | tf_op jit(solution)/shard_map/ppermute | solution.py:58
  79.3 6.7 %ffn.1 = bf16[16,256,128]{2,1,0:T(8,128)(2,1)} custom-call(bf16[4,320,512]{2,1,0:T(8,128)(2,1)S(1)} %all-to-all-done.1.x_ref, bf16[3072,256]{1,0:T(8,128)(2,1)S(1)} %get-tuple-element.7.refs_0_, bf16[3072,256]{1,0:T(8,128)(2,1)} %get-tuple-element.8.refs_1_, bf16[3072,256]{1,0:T(8,128)(2,1)} %collective-permute-done.5.refs_2_, ...), custom_call_target="tpu_custom_call" | custom-call | tf_op jit(solution)/shard_map/ffn/pallas_call | solution.py:219
  86.0 19.4 %all_to_all.27.parts_ref = bf16[16,256,128]{2,1,0:T(8,128)(2,1)S(1)} all-to-all(bf16[16,256,128]{2,1,0:T(8,128)(2,1)} %ffn.1), channel_id=1, replica_groups={{0,1,2,3,4,5,6,7,8,9,10,11,12,13,14,15},{16,20,24,28,17,21,25,29,18,22,..., dimensions={0} | all-to-all | bytes 2097152 | tf_op jit(solution)/shard_map/all_to_all | solution.py:407
  105.4 0.8 total.1
  106.3 14.7 %all-to-all-start.3 = ((bf16[32,32,128]{2,1,0:T(8,128)(2,1)}), bf16[32,32,128]{2,1,0:T(8,128)(2,1)S(1)}, u32[]{:S(2)}, u32[]{:S(2)}) async-start(bf16[32,32,128]{2,1,0:T(8,128)(2,1)} %bitcast.6), calls=%async_computation.3 | async-start | bytes 524288 | tf_op jit(solution)/shard_map/all_to_all | solution.py:409
  121.0 1.9 %collective-permute-start.2 = (bf16[4,64,512]{2,1,0:T(8,128)(2,1)S(1)}, bf16[4,64,512]{2,1,0:T(8,128)(2,1)S(1)}, u32[]{:S(2)}, u32[]{:S(2)}) collective-permute-start(bf16[4,64,512]{2,1,0:T(8,128)(2,1)S(1)} %slice.16.own_ref), channel_id=1, source_target_pairs={{0,1},{1,0},{2,3},{3,2},{4,5},{5,4},{6,7},{7,6},{8,9},{9,8},{10,11... | collective-permute-start | bytes 786440 | tf_op jit(solution)/shard_map/ppermute | solution.py:58
  122.9 2.8 %collective-permute-start.3 = (bf16[4,64,512]{2,1,0:T(8,128)(2,1)S(1)}, bf16[4,64,512]{2,1,0:T(8,128)(2,1)S(1)}, u32[]{:S(2)}, u32[]{:S(2)}) collective-permute-start(bf16[4,64,512]{2,1,0:T(8,128)(2,1)S(1)} %slice.16.own_ref), channel_id=1, source_target_pairs={{0,3},{1,2},{2,1},{3,0},{4,7},{5,6},{6,5},{7,4},{8,11},{9,10},{10,... | collective-permute-start | bytes 786440 | tf_op jit(solution)/shard_map/ppermute | solution.py:58
  125.7 4.3 %collective-permute-start.4 = (bf16[4,64,512]{2,1,0:T(8,128)(2,1)S(1)}, bf16[4,64,512]{2,1,0:T(8,128)(2,1)S(1)}, u32[]{:S(2)}, u32[]{:S(2)}) collective-permute-start(bf16[4,64,512]{2,1,0:T(8,128)(2,1)S(1)} %slice.16.own_ref), channel_id=1, source_target_pairs={{0,2},{1,3},{2,0},{3,1},{4,6},{5,7},{6,4},{7,5},{8,10},{9,11},{10,... | collective-permute-start | bytes 786440 | tf_op jit(solution)/shard_map/ppermute | solution.py:58
  130.0 0.1 copy.18.weight_ref
  130.1 0.0 collective-permute-done.2.one_ref
  130.1 1.4 collective-permute-done.3.two_ref
  131.5 3.1 %collective-permute-done.4.far_ref = bf16[4,64,512]{2,1,0:T(8,128)(2,1)S(1)} collective-permute-done((bf16[4,64,512]{2,1,0:T(8,128)(2,1)S(1)}, bf16[4,64,512]{2,1,0:T(8,128)(2,1)S(1)}, u32[]{:S(2)}, u32[]{:S(2)}) %collective-permute-start.4) | collective-permute-done | bytes 262176 | tf_op jit(solution)/shard_map/ppermute | solution.py:58
  134.6 1.1 project.1
  135.7 7.4 %all-to-all-done.3 = bf16[32,32,128]{2,1,0:T(8,128)(2,1)S(1)} async-done(((bf16[32,32,128]{2,1,0:T(8,128)(2,1)}), bf16[32,32,128]{2,1,0:T(8,128)(2,1)S(1)}, u32[]{:S(2)}, u32[]{:S(2)}) %all-to-all-start.3) | async-done | bytes 262176 | tf_op jit(solution)/shard_map/all_to_all | solution.py:409
  143.2 1.1 combine.1
  (15 shorter events, 0.1 us)
Async XLA Ops:
  0.6 10.1 %copy-start.2 = (f32[2048]{0:T(1024)S(1)}, f32[2048]{0:T(1024)}, u32[]{:S(2)}) copy-start(f32[2048]{0:T(1024)} %param.18) | copy-start | bytes 24580
  0.6 10.1 %copy-start.3 = (s32[256,2]{0,1:T(2,128)S(1)}, s32[256,2]{0,1:T(2,128)}, u32[]{:S(2)}) copy-start(s32[256,2]{0,1:T(2,128)} %param.19) | copy-start | bytes 6148
  0.7 10.1 %copy-start = (bf16[256,2048]{1,0:T(8,128)(2,1)S(1)}, bf16[256,2048]{1,0:T(8,128)(2,1)}, u32[]{:S(2)}) copy-start(bf16[256,2048]{1,0:T(8,128)(2,1)} %x_ref.1) | copy-start | bytes 3145732
  3.2 33.3 %copy-start.4 = (bf16[512,256]{1,0:T(8,128)(2,1)S(1)}, bf16[512,256]{1,0:T(8,128)(2,1)}, u32[]{:S(2)}) copy-start(bf16[512,256]{1,0:T(8,128)(2,1)} %param.14) | copy-start | bytes 786436
  3.2 33.3 %copy-start.5 = (bf16[512,256]{1,0:T(8,128)(2,1)S(1)}, bf16[512,256]{1,0:T(8,128)(2,1)}, u32[]{:S(2)}) copy-start(bf16[512,256]{1,0:T(8,128)(2,1)} %param.13) | copy-start | bytes 786436
  3.2 36.6 %collective-permute-start.8 = (bf16[3072,256]{1,0:T(8,128)(2,1)}, bf16[3072,256]{1,0:T(8,128)(2,1)}, u32[]{:S(2)}, u32[]{:S(2)}) collective-permute-start(bf16[3072,256]{1,0:T(8,128)(2,1)} %get-tuple-element.8.refs_1_), channel_id=1, source_target_pairs={{0,3},{1,2},{2,1},{3,0},{4,7},{5,6},{6,5},{7,4},{8,11},{9,10},{10,... | collective-permute-start | bytes 4718600 | tf_op jit(solution)/shard_map/ppermute | solution.py:58
  8.8 34.4 %collective-permute-start.5 = (bf16[3072,256]{1,0:T(8,128)(2,1)S(1)}, bf16[3072,256]{1,0:T(8,128)(2,1)}, u32[]{:S(2)}, u32[]{:S(2)}) collective-permute-start(bf16[3072,256]{1,0:T(8,128)(2,1)S(1)} %get-tuple-element.7.refs_0_), channel_id=1, source_target_pairs={{0,1},{1,0},{2,3},{3,2},{4,5},{5,4},{6,7},{7,6},{8,9},{9,8},{10,11... | collective-permute-start | bytes 4718600 | tf_op jit(solution)/shard_map/ppermute | solution.py:58
  13.1 36.7 %copy-start.6 = (bf16[512,64]{0,1:T(8,128)(2,1)S(1)}, bf16[512,64]{0,1:T(8,128)(2,1)}, u32[]{:S(2)}) copy-start(bf16[512,64]{0,1:T(8,128)(2,1)} %param.12) | copy-start | bytes 196612
  13.1 42.0 %all-to-all-start = ((bf16[32,8,512]{2,1,0:T(8,128)(2,1)}), bf16[32,8,512]{2,1,0:T(8,128)(2,1)S(1)}, u32[]{:S(2)}, u32[]{:S(2)}) async-start(bf16[32,8,512]{2,1,0:T(8,128)(2,1)} %bitcast.2), calls=%async_computation | async-start | bytes 524288 | tf_op jit(solution)/shard_map/all_to_all | solution.py:395
  29.4 30.7 %collective-permute-start.6 = (bf16[3072,256]{1,0:T(8,128)(2,1)}, bf16[3072,256]{1,0:T(8,128)(2,1)}, u32[]{:S(2)}, u32[]{:S(2)}) collective-permute-start(bf16[3072,256]{1,0:T(8,128)(2,1)} %get-tuple-element.8.refs_1_), channel_id=1, source_target_pairs={{0,1},{1,0},{2,3},{3,2},{4,5},{5,4},{6,7},{7,6},{8,9},{9,8},{10,11... | collective-permute-start | bytes 4718600 | tf_op jit(solution)/shard_map/ppermute | solution.py:58
  32.7 27.5 %collective-permute-start.7 = (bf16[3072,256]{1,0:T(8,128)(2,1)S(1)}, bf16[3072,256]{1,0:T(8,128)(2,1)}, u32[]{:S(2)}, u32[]{:S(2)}) collective-permute-start(bf16[3072,256]{1,0:T(8,128)(2,1)S(1)} %get-tuple-element.7.refs_0_), channel_id=1, source_target_pairs={{0,3},{1,2},{2,1},{3,0},{4,7},{5,6},{6,5},{7,4},{8,11},{9,10},{10,... | collective-permute-start | bytes 4718600 | tf_op jit(solution)/shard_map/ppermute | solution.py:58
  36.7 11.2 %collective-permute-start = (bf16[2,128,64]{2,1,0:T(8,128)(2,1)S(1)}, bf16[2,128,64]{2,1,0:T(8,128)(2,1)S(1)}, u32[]{:S(2)}, u32[]{:S(2)}) collective-permute-start(bf16[2,128,64]{2,1,0:T(8,128)(2,1)S(1)} %get-tuple-element.11), channel_id=1, source_target_pairs={{0,16},{16,32},{32,48},{48,64},{64,80},{80,96},{96,112},{112,128},... | collective-permute-start | bytes 98312 | tf_op jit(solution)/shard_map/ppermute | solution.py:352
  39.8 37.4 %collective-permute-start.10 = (bf16[3072,256]{1,0:T(8,128)(2,1)}, bf16[3072,256]{1,0:T(8,128)(2,1)}, u32[]{:S(2)}, u32[]{:S(2)}) collective-permute-start(bf16[3072,256]{1,0:T(8,128)(2,1)} %collective-permute-done.8.refs_5_), channel_id=1, source_target_pairs={{0,1},{1,0},{2,3},{3,2},{4,5},{5,4},{6,7},{7,6},{8,9},{9,8},{10,11... | collective-permute-start | bytes 4718600 | tf_op jit(solution)/shard_map/ppermute | solution.py:58
  43.2 36.1 %collective-permute-start.9 = (bf16[3072,256]{1,0:T(8,128)(2,1)}, bf16[3072,256]{1,0:T(8,128)(2,1)}, u32[]{:S(2)}, u32[]{:S(2)}) collective-permute-start(bf16[3072,256]{1,0:T(8,128)(2,1)} %collective-permute-done.5.refs_2_), channel_id=1, source_target_pairs={{0,3},{1,2},{2,1},{3,0},{4,7},{5,6},{6,5},{7,4},{8,11},{9,10},{10,... | collective-permute-start | bytes 4718600 | tf_op jit(solution)/shard_map/ppermute | solution.py:58
  47.8 6.0 %collective-permute-start.1 = (bf16[2,128,64]{2,1,0:T(8,128)(2,1)S(1)}, bf16[2,128,64]{2,1,0:T(8,128)(2,1)S(1)}, u32[]{:S(2)}, u32[]{:S(2)}) collective-permute-start(bf16[2,128,64]{2,1,0:T(8,128)(2,1)S(1)} %get-tuple-element.10), channel_id=1, source_target_pairs={{16,0},{32,16},{48,32},{64,48},{80,64},{96,80},{112,96},{128,112},... | collective-permute-start | bytes 98312 | tf_op jit(solution)/shard_map/ppermute | solution.py:353
  56.4 20.9 %all-to-all-start.1 = ((bf16[4,320,512]{2,1,0:T(8,128)(2,1)}), bf16[4,320,512]{2,1,0:T(8,128)(2,1)S(1)}, u32[]{:S(2)}, u32[]{:S(2)}) async-start(bf16[4,320,512]{2,1,0:T(8,128)(2,1)} %broadcast_in_dim.9), calls=%async_computation.1 | async-start | bytes 2621440 | tf_op jit(solution)/shard_map/all_to_all | solution.py:402
  105.4 24.5 %copy-start.7 = (f32[256,2]{0,1:T(2,128)S(1)}, f32[256,2]{0,1:T(2,128)}, u32[]{:S(2)}) copy-start(f32[256,2]{0,1:T(2,128)} %param.20) | copy-start | bytes 6148
  105.4 29.2 %copy-start.1 = (bf16[1024,128]{1,0:T(8,128)(2,1)S(1)}, bf16[1024,128]{1,0:T(8,128)(2,1)}, u32[]{:S(2)}) copy-start(bf16[1024,128]{1,0:T(8,128)(2,1)} %weight_ref.2) | copy-start | bytes 786436
  106.3 36.9 %all-to-all-start.3 = ((bf16[32,32,128]{2,1,0:T(8,128)(2,1)}), bf16[32,32,128]{2,1,0:T(8,128)(2,1)S(1)}, u32[]{:S(2)}, u32[]{:S(2)}) async-start(bf16[32,32,128]{2,1,0:T(8,128)(2,1)} %bitcast.6), calls=%async_computation.3 | async-start | bytes 524288 | tf_op jit(solution)/shard_map/all_to_all | solution.py:409
  121.0 9.2 %collective-permute-start.2 = (bf16[4,64,512]{2,1,0:T(8,128)(2,1)S(1)}, bf16[4,64,512]{2,1,0:T(8,128)(2,1)S(1)}, u32[]{:S(2)}, u32[]{:S(2)}) collective-permute-start(bf16[4,64,512]{2,1,0:T(8,128)(2,1)S(1)} %slice.16.own_ref), channel_id=1, source_target_pairs={{0,1},{1,0},{2,3},{3,2},{4,5},{5,4},{6,7},{7,6},{8,9},{9,8},{10,11... | collective-permute-start | bytes 786440 | tf_op jit(solution)/shard_map/ppermute | solution.py:58
  122.9 8.6 %collective-permute-start.3 = (bf16[4,64,512]{2,1,0:T(8,128)(2,1)S(1)}, bf16[4,64,512]{2,1,0:T(8,128)(2,1)S(1)}, u32[]{:S(2)}, u32[]{:S(2)}) collective-permute-start(bf16[4,64,512]{2,1,0:T(8,128)(2,1)S(1)} %slice.16.own_ref), channel_id=1, source_target_pairs={{0,3},{1,2},{2,1},{3,0},{4,7},{5,6},{6,5},{7,4},{8,11},{9,10},{10,... | collective-permute-start | bytes 786440 | tf_op jit(solution)/shard_map/ppermute | solution.py:58
  125.7 8.9 %collective-permute-start.4 = (bf16[4,64,512]{2,1,0:T(8,128)(2,1)S(1)}, bf16[4,64,512]{2,1,0:T(8,128)(2,1)S(1)}, u32[]{:S(2)}, u32[]{:S(2)}) collective-permute-start(bf16[4,64,512]{2,1,0:T(8,128)(2,1)S(1)} %slice.16.own_ref), channel_id=1, source_target_pairs={{0,2},{1,3},{2,0},{3,1},{4,6},{5,7},{6,4},{7,5},{8,10},{9,11},{10,... | collective-permute-start | bytes 786440 | tf_op jit(solution)/shard_map/ppermute | solution.py:58
